TPU v7x, 128 devices: a whole 4x4x4 slice. The times are simulated.
128 devices in a mesh: ep: 32 (over z, y, core), tp: 4 (over x).
Axes of the slice: x: 4, y: 4, z: 4, core: 2. Of those that a mesh axis runs over, the one named last changes fastest.
Arguments:
- sequence_entry_features: bfloat16 [49152, 4096], P('ep', 'tp'), may hold values from -6 to 6
- sequence_exit_gating: bfloat16 [49152, 4096], P('ep', 'tp'), may hold values from -6 to 6
- memory_insert_clusters: bfloat16 [49152, 1024], P('ep', 'tp'), may hold values from -6 to 6
- memory_query_clusters: bfloat16 [49152, 1024], P('ep', 'tp'), may hold values from -6 to 6
- interval_presoftplus: bfloat16 [49152, 64], P('ep', 'tp'), may hold values from -4 to 4
- entry_filter_taps: bfloat16 [4, 4096], P(None, 'tp'), may hold values from -3 to 3
- insert_filter_taps: bfloat16 [4, 1024], P(None, 'tp'), may hold values from -3 to 3
- query_filter_taps: bfloat16 [4, 1024], P(None, 'tp'), may hold values from -3 to 3
- interval_offset: float32 [64], P('tp'), may hold values from -6 to -1
- head_fading_exponent: float32 [64], P('tp'), may hold values from -8 to -1
- skip_connection_factor: float32 [64], P('tp'), may hold values from 0.1 to 1.9
- spike_fading_exponent: float32 [49152, 64], P('ep', 'tp'), may hold values from -1 to 0
- cluster_scaling_vector: float32 [4096], P('tp'), may hold values from 0.1 to 1.9
- sequence_exit_projection: bfloat16 [4096, 2048], P('tp'), may hold values from -0.09375 to 0.09375
- specialist_sample_slice: bfloat16 [16384, 2048], P(('ep', 'tp')), may hold values from -6 to 6
- specialist_scaling_vector: float32 [2048], replicated, may hold values from 0.1 to 1.9
- chosen_specialists: int32 [16384, 4], P(('ep', 'tp')), may hold values from 0 to 31, all different within a row; in each aligned block of 128 rows (0 to 127, 128 to 255, ...) at most 20 rows name the same one
- dispatcher_affinity_matrix: float32 [16384, 4], P(('ep', 'tp')), may hold values from -4 to 4
- gating_projection: bfloat16 [32, 2048, 2048], P('ep', None, 'tp'), may hold values from -0.5 to 0.5
- expand_projection: bfloat16 [32, 2048, 2048], P('ep', None, 'tp'), may hold values from -0.5 to 0.5
- shrink_projection: bfloat16 [32, 2048, 2048], P('ep', 'tp'), may hold values from -0.03125 to 0.03125
Outputs:
- mixed: bfloat16 [49152, 2048], P(('ep', 'tp'))
- moe_out: bfloat16 [16384, 2048], P(('ep', 'tp'))
Inputs may be any that keep to these rules, and one draw needn't show every extreme that they name: `chosen_specialists`: in each aligned block of 128 rows (the rows of one device) no expert is named by more than 20 rows, a bound that some block reaches; the 4 experts of a row differ.
All inputs are finite; a program needn't handle non-finite values.
Results may differ from a plain program's by a relative error of at most 0.015.
Values may be sent and summed in bfloat16 or wider, within the bound.
A program may use at most 192 MiB of HBM per device.

v0:
```python
import jax
import jax.numpy as jnp
from jax import lax
from jax.sharding import Mesh
from jax.sharding import PartitionSpec as P

HEAD = 64
STATE = 128
SPAN = 128
EP = ("ep_0", "ep_1", "ep_2")
EP_TP = ("ep_0", "ep_1", "ep_2", "tp")


norm_eps = 1e-05
clamp_top = 7.0
sigmoid_sharp = 1.702
highest = lax.Precision.HIGHEST


def passed_along(block, axis, distance):
    devices = range(lax.axis_size(axis))
    route = [(i - distance, i) for i in devices if i - distance in devices]
    return lax.ppermute(block, axis, route)


def neutral_like(value, identity):
    return jax.tree.map(
        lambda part, zero: jnp.zeros_like(part) + jnp.asarray(zero, part.dtype), value, identity
    )


def entering_2(value, axes, combine, identity):
    before = start = neutral_like(value, identity)
    running = value
    for axis in reversed(axes):
        size, mine = (lax.axis_size(axis), lax.axis_index(axis))
        pieces = jax.tree.map(
            lambda part, kind: lax.all_gather(part.astype(kind), axis),
            running,
            (jnp.bfloat16, jnp.bfloat16),
        )
        inside, running = (start, start)
        for k in range(size):
            passed = k < mine
            running = combine(
                running, jax.tree.map(lambda part, own: part[k].astype(own.dtype), pieces, value)
            )
            inside = jax.tree.map(lambda new, old: jnp.where(passed, new, old), running, inside)
        before = combine(inside, before)
    return before


def laid_out(tiles, dim):
    lengths = list(tiles.shape[1:])
    lengths[dim] *= tiles.shape[0]
    return jnp.moveaxis(tiles, 0, dim).reshape(lengths)


def copy_for_each(value, axis):
    size = lax.axis_size(axis)
    return lax.all_to_all(
        jnp.broadcast_to(value[None], (size, *value.shape)), axis, 0, 0, tiled=True
    )


def gather_directly(value, axis, dim):
    return laid_out(copy_for_each(value, axis), dim)


def causal_conv(values, previous, kernel):
    length = values.shape[0]
    joined = jnp.concatenate([previous, values], axis=0).astype(jnp.float32)
    summed = jnp.zeros(values.shape, jnp.float32)
    for offset in range(kernel.shape[0]):
        summed = summed + joined[offset : offset + length] * kernel[offset].astype(jnp.float32)
    return jax.nn.silu(summed)


def combine_states(earlier, latter):
    return (earlier[0] * latter[1][:, :, None, None] + latter[0], earlier[1] * latter[1])


def mixer_half(
    sequence_entry_features,
    sequence_exit_gating,
    memory_insert_clusters,
    memory_query_clusters,
    interval_presoftplus,
    entry_filter_taps,
    insert_filter_taps,
    query_filter_taps,
    interval_offset,
    head_fading_exponent,
    skip_connection_factor,
    spike_fading_exponent,
    cluster_scaling_vector,
    sequence_exit_projection,
):
    tok_rows = sequence_entry_features.shape[0]
    local_heads = interval_offset.shape[0]
    local_groups = memory_insert_clusters.shape[1] // STATE
    per_group = local_heads // local_groups
    group_cols = per_group * HEAD
    rim_rows = entry_filter_taps.shape[0] - 1
    inner_cols = sequence_entry_features.shape[1]
    state_cols = memory_insert_clusters.shape[1]
    last_rows = jnp.concatenate(
        [
            sequence_entry_features[tok_rows - rim_rows :],
            memory_insert_clusters[tok_rows - rim_rows :],
            memory_query_clusters[tok_rows - rim_rows :],
        ],
        axis=1,
    )
    before = passed_along(last_rows, EP, 1)
    seq_x = causal_conv(sequence_entry_features, before[:, :inner_cols], entry_filter_taps)
    seq_b = causal_conv(
        memory_insert_clusters, before[:, inner_cols : inner_cols + state_cols], insert_filter_taps
    )
    seq_c = causal_conv(
        memory_query_clusters, before[:, inner_cols + state_cols :], query_filter_taps
    )
    discretization_interval = jax.nn.softplus(
        interval_presoftplus.astype(jnp.float32) + interval_offset
    )
    fading_exponent = (
        spike_fading_exponent - jnp.exp(head_fading_exponent) * discretization_interval
    )
    blocks = tok_rows // SPAN
    scaled = (
        seq_x.reshape(tok_rows, local_heads, HEAD) * discretization_interval[:, :, None]
    ).reshape(blocks, SPAN, local_groups, per_group, HEAD)
    keys_b = seq_b.reshape(blocks, SPAN, local_groups, STATE)
    query_c = seq_c.reshape(blocks, SPAN, local_groups, STATE)
    cumulative = jnp.cumsum(fading_exponent.reshape(blocks, SPAN, local_groups, per_group), axis=1)
    causal = jnp.tril(jnp.ones((SPAN, SPAN), bool))[None, :, :, None, None]
    weight = jnp.exp(jnp.where(causal, cumulative[:, :, None] - cumulative[:, None, :], -jnp.inf))
    scores = jnp.einsum("ctgn,csgn->ctsg", query_c, keys_b, precision=highest)
    within = jnp.einsum("ctsge,csgep->ctgep", scores[..., None] * weight, scaled, precision=highest)
    block_end = cumulative[:, -1]
    block_state = jnp.einsum(
        "csgn,csgep->cgepn",
        keys_b,
        scaled * jnp.exp(block_end[:, None] - cumulative)[..., None],
        precision=highest,
    )

    def advance(running, pieces):
        new_state, factor = pieces
        return (running * factor[:, :, None, None] + new_state, running)

    own_state, before_block = lax.scan(
        advance, jnp.zeros(block_state.shape[1:], jnp.float32), (block_state, jnp.exp(block_end))
    )
    start_log = jnp.cumsum(block_end, axis=0) - block_end
    own_decay = jnp.exp(jnp.sum(block_end, axis=0))
    entering = entering_2(
        (own_state, own_decay),
        EP,
        combine_states,
        (jnp.zeros_like(own_state), jnp.ones_like(own_decay)),
    )[0]
    full_prev = before_block + jnp.exp(start_log)[:, :, :, None, None] * entering[None]
    carried = (
        jnp.einsum("ctgn,cgepn->ctgep", query_c, full_prev, precision=highest)
        * jnp.exp(cumulative)[..., None]
    )
    mixer_y = (within + carried).reshape(tok_rows, local_heads, HEAD) + seq_x.reshape(
        tok_rows, local_heads, HEAD
    ) * skip_connection_factor[:, None]
    gated_y = mixer_y.reshape(tok_rows, local_groups, group_cols) * jax.nn.silu(
        sequence_exit_gating.astype(jnp.float32)
    ).reshape(tok_rows, local_groups, group_cols)
    normed = gated_y * lax.rsqrt(jnp.mean(gated_y * gated_y, axis=2, keepdims=True) + norm_eps)
    normed = (normed.reshape(tok_rows, inner_cols) * cluster_scaling_vector).astype(jnp.bfloat16)
    return lax.psum_scatter(
        jnp.dot(normed, sequence_exit_projection, preferred_element_type=jnp.float32).astype(
            jnp.bfloat16
        ),
        "tp",
        scatter_dimension=0,
        tiled=True,
    )


def experts_half(
    specialist_sample_slice,
    specialist_scaling_vector,
    chosen_specialists,
    dispatcher_affinity_matrix,
    gating_projection,
    expand_projection,
    shrink_projection,
):
    tok_rows = specialist_sample_slice.shape[0]
    feature_count = specialist_sample_slice.shape[1]
    top_count = chosen_specialists.shape[1]
    experts = lax.axis_size(EP)
    groups_tp = lax.axis_size("tp")
    capacity = tok_rows * top_count * 5 // (4 * experts)
    as_float = specialist_sample_slice.astype(jnp.float32)
    centred = as_float - jnp.mean(as_float, axis=1, keepdims=True)
    normed = (
        centred
        * lax.rsqrt(jnp.mean(centred * centred, axis=1, keepdims=True) + norm_eps)
        * specialist_scaling_vector
    ).astype(jnp.bfloat16)
    route_weight = jnp.exp(dispatcher_affinity_matrix) / jnp.sum(
        jnp.exp(dispatcher_affinity_matrix), axis=1, keepdims=True
    )
    flat_routes = chosen_specialists.reshape(-1)
    onehot = (flat_routes[:, None] == jnp.arange(experts, dtype=jnp.int32)[None, :]).astype(
        jnp.int32
    )
    position = jnp.sum(onehot * (jnp.cumsum(onehot, axis=0) - 1), axis=1)
    target = flat_routes * capacity + position
    token_ids = jnp.arange(tok_rows * top_count, dtype=jnp.int32) // top_count
    source_table = jnp.full((experts * capacity,), tok_rows, jnp.int32).at[target].set(token_ids)
    padded = jnp.concatenate([normed, jnp.zeros((1, feature_count), jnp.bfloat16)], axis=0)
    outgoing = padded[source_table].reshape(experts, capacity, feature_count)
    arrived = lax.all_to_all(outgoing, EP, split_axis=0, concat_axis=0, tiled=True)
    shard_rows = gather_directly(arrived, "tp", 0)
    rows_in = shard_rows.reshape(-1, feature_count)
    gate_h = jnp.dot(rows_in, gating_projection[0], preferred_element_type=jnp.float32)
    up_h = jnp.dot(rows_in, expand_projection[0], preferred_element_type=jnp.float32)
    clipped = jnp.minimum(gate_h, clamp_top)
    hidden_act = (
        (
            clipped
            * jax.nn.sigmoid(sigmoid_sharp * clipped)
            * (jnp.clip(up_h, -clamp_top, clamp_top) + 1.0)
        )
        .astype(jnp.bfloat16)
        .reshape(shard_rows.shape[0], capacity, -1)
    )
    hidden_act = hidden_act.reshape(groups_tp * experts * capacity, -1)
    summed = lax.psum_scatter(
        jnp.dot(hidden_act, shrink_projection[0], preferred_element_type=jnp.float32).astype(
            jnp.bfloat16
        ),
        "tp",
        scatter_dimension=0,
        tiled=True,
    )
    returned = lax.all_to_all(
        summed.reshape(experts, capacity, feature_count),
        EP,
        split_axis=0,
        concat_axis=0,
        tiled=True,
    )
    slot_out = returned.reshape(experts * capacity, feature_count)[target].reshape(
        tok_rows, top_count, feature_count
    )
    combined = jnp.einsum("tk,tkd->td", route_weight, slot_out.astype(jnp.float32))
    return combined.astype(jnp.bfloat16)


def body(
    sequence_entry_features,
    sequence_exit_gating,
    memory_insert_clusters,
    memory_query_clusters,
    interval_presoftplus,
    entry_filter_taps,
    insert_filter_taps,
    query_filter_taps,
    interval_offset,
    head_fading_exponent,
    skip_connection_factor,
    spike_fading_exponent,
    cluster_scaling_vector,
    sequence_exit_projection,
    specialist_sample_slice,
    specialist_scaling_vector,
    chosen_specialists,
    dispatcher_affinity_matrix,
    gating_projection,
    expand_projection,
    shrink_projection,
):
    mixed = mixer_half(
        sequence_entry_features,
        sequence_exit_gating,
        memory_insert_clusters,
        memory_query_clusters,
        interval_presoftplus,
        entry_filter_taps,
        insert_filter_taps,
        query_filter_taps,
        interval_offset,
        head_fading_exponent,
        skip_connection_factor,
        spike_fading_exponent,
        cluster_scaling_vector,
        sequence_exit_projection,
    )
    moe_out = experts_half(
        specialist_sample_slice,
        specialist_scaling_vector,
        chosen_specialists,
        dispatcher_affinity_matrix,
        gating_projection,
        expand_projection,
        shrink_projection,
    )
    return (mixed, moe_out)


def solution(mesh):
    split = Mesh(mesh.devices.reshape(4, 4, 2, mesh.shape["tp"]), ("ep_0", "ep_1", "ep_2", "tp"))
    return jax.shard_map(
        body,
        mesh=split,
        in_specs=(
            P(EP, "tp"),
            P(EP, "tp"),
            P(EP, "tp"),
            P(EP, "tp"),
            P(EP, "tp"),
            P(None, "tp"),
            P(None, "tp"),
            P(None, "tp"),
            P("tp"),
            P("tp"),
            P("tp"),
            P(EP, "tp"),
            P("tp"),
            P("tp", None),
            P(EP_TP, None),
            P(),
            P(EP_TP, None),
            P(EP_TP, None),
            P(EP, None, "tp"),
            P(EP, None, "tp"),
            P(EP, "tp", None),
        ),
        out_specs=(P(EP_TP, None), P(EP_TP, None)),
        check_vma=False,
    )
```

profile of v0, /device:TPU:0, one launch (start us, length us, event | category | flops | bytes accessed | tf_op | source)
XLA Modules:
  0.0 563.0 jit_solution(11998925609202190352)
XLA Ops:
  10.5 2.1 collective-permute-start
  14.3 1.2 convert_reduce_fusion
  15.5 1.3 fusion.56
  17.1 1.2 reduce-window.6
  19.2 2.4 scatter_custom_fusion
  21.7 1.4 fusion.58
  23.2 4.1 gather_fusion
  27.3 5.2 reshape.290
  32.5 9.4 %all-to-all-start = ((bf16[32,20,2048]{2,1,0:T(8,128)(2,1)}), bf16[32,20,2048]{2,1,0:T(8,128)(2,1)}, u32[]{:S(2)}, u32[]{:S(2)}) async-start(bf16[32,20,2048]{2,1,0:T(8,128)(2,1)} %reshape.290), calls=%async_computation.1 | async-start | bytes 6291456 | tf_op jit(solution)/shard_map/all_to_all | solution.py:221
  42.1 2.1 copy.67
  44.2 1.8 fusion.100
  46.0 1.3 copy-done.5
  47.4 2.5 fusion.98
  50.5 1.3 subtract_exponential_fusion.1
  51.9 1.8 all-gather.2
  53.7 30.3 %all_gather.27 = bf16[4,2,8]{2,1,0:T(2,128)(2,1)S(1)} all-gather(bf16[1,2,8]{2,1,0:T(2,128)(2,1)S(1)} %fusion.86), channel_id=1, replica_groups=mesh['ep_0'=4,'ep_1'=4,'ep_2'=2,'tp'=4] {'ep_1'}, dimensions={0}, use_global_device_ids=true | all-gather | bytes 160 | tf_op jit(solution)/shard_map/all_gather | solution.py:38
  85.1 4.6 copy.60
  89.8 2.3 copy.71
  93.8 3.5 maximum_convert_fusion
  97.3 2.9 copy-done.2
  100.2 7.5 %divide_multiply_fusion = f32[1536,1024]{0,1:T(8,128)} fusion(f32[1539,1024]{0,1:T(8,128)S(1)} %maximum_convert_fusion, f32[1024]{0:T(1024)S(1)} %bitcast.206, f32[1024]{0:T(1024)S(1)} %bitcast.209, f32[1024]{0:T(1024)S(1)} %bitcast.203, f32[1024]{0:T(1024)S(1)} %bitcast.200), kind=kLoop, calls=%fused_computation.43 | loop fusion | flops 17301504 | bytes 31473664 | tf_op jit(solution)/shard_map/jit(silu)/mul | solution.py:76
  107.7 8.5 %reshape.281 = f32[12,128,2,8,64]{1,0,4,3,2:T(8,128)} reshape(f32[1536,1024]{0,1:T(8,128)} %divide_multiply_fusion) | data formatting | bytes 12582912 | tf_op jit(solution)/shard_map/reshape | solution.py:131
  116.2 1.5 fusion.99
  117.7 1.5 copy.62
  120.1 2.8 divide_multiply_fusion.2
  122.9 2.9 reshape.282
  125.8 11.2 %broadcast_multiply_fusion = (f32[12,128,2,8,64]{1,0,4,3,2:T(8,128)}, f32[12,128,2,8,64]{1,0,4,3,2:T(8,128)}) fusion(f32[12,128,2,8]{1,0,3,2:T(8,128)S(1)} %copy.71, f32[12,128,2,8,64]{1,0,4,3,2:T(8,128)} %reshape.281, f32[12,128,2,8]{1,0,3,2:T(8,128)S(1)} %copy-done.10), kind=kLoop, calls=%fused_computation.47 | loop fusion | flops 3145728 | bytes 19070976 | tf_op jit(solution)/shard_map/mul | solution.py:144
  136.9 12.1 %fusion.16 = f32[12,2,8,64,128]{4,3,2,1,0:T(8,128)} fusion(f32[12,128,2,8,64]{1,0,4,3,2:T(8,128)} %get-tuple-element.77, f32[12,128,2,128,1]{3,2,1,0,4:T(2,128)S(1)} %bitcast.196), kind=kOutput, calls=%fused_computation.32 | convolution fusion | flops 2415919104 | bytes 14155776 | tf_op jit(solution)/shard_map/csgn,csgep->cgepn/dot_general | solution.py:141
  149.1 4.9 copy.85
  154.0 7.2 %broadcast_in_dim.26 = bf16[4,32,20,2048]{3,1,2,0:T(8,128)(2,1)} broadcast(bf16[32,20,2048]{2,0,1:T(8,128)(2,1)} %copy.85), dimensions={1,2,3} | broadcast | bytes 13107200 | tf_op jit(solution)/shard_map/broadcast_in_dim | solution.py:62
  161.2 6.0 %all-to-all-start.1 = ((bf16[4,32,20,2048]{3,1,2,0:T(8,128)(2,1)}), bf16[4,32,20,2048]{3,1,2,0:T(8,128)(2,1)}, u32[]{:S(2)}, u32[]{:S(2)}) async-start(bf16[4,32,20,2048]{3,1,2,0:T(8,128)(2,1)} %broadcast_in_dim.26), calls=%async_computation.2 | async-start | bytes 20971520 | tf_op jit(solution)/shard_map/all_to_all | solution.py:61
  167.2 32.7 %while.13 = (s32[]{:T(128)}, f32[2,8,64,128]{3,2,1,0:T(8,128)S(1)}, f32[12,2,8,64,128]{4,3,2,1,0:T(8,128)}, f32[12,2,8]{2,0,1:T(8,128)}, f32[12,2,8,64,128]{4,3,2,1,0:T(8,128)}, /*index=5*/s32[]{:T(128)}, s32[]{:T(128)}) while((s32[]{:T(128)}, f32[2,8,64,128]{3,2,1,0:T(8,128)S(1)}, f32[12,2,8,64,128]{4,3,2,1,0:T(8,128)}, ...), condition=%wide.region_2.3_spmd.clone, body=%wide.region_1.2_spmd.clone.sunk | while | flops 524291 | bytes 2621740 | solution.py:152
  171.5 1.2 bitcast_add_fusion.3
  200.0 2.2 all-gather.1
  203.3 24.7 %all-gather.6.cloned.1.call-done = bf16[4,2,8,64,128]{4,3,2,1,0:T(8,128)(2,1)} async-done(((bf16[1,2,8,64,128]{4,3,2,1,0:T(8,128)(2,1)}), bf16[4,2,8,64,128]{4,3,2,1,0:T(8,128)(2,1)}) %all-gather.6.cloned.1.call-update) | async-done | bytes 1048592 | tf_op jit(solution)/shard_map/all_gather | solution.py:38
  228.0 2.2 fusion.65
  230.3 52.8 %all-to-all-done.1 = bf16[4,32,20,2048]{3,1,2,0:T(8,128)(2,1)} async-done(((bf16[4,32,20,2048]{3,1,2,0:T(8,128)(2,1)}), bf16[4,32,20,2048]{3,1,2,0:T(8,128)(2,1)}, u32[]{:S(2)}, u32[]{:S(2)}) %all-to-all-start.1) | async-done | bytes 10485792 | tf_op jit(solution)/shard_map/all_to_all | solution.py:61
  283.1 14.6 %copy.86 = bf16[4,32,20,2048]{3,2,1,0:T(8,128)(2,1)} copy(bf16[4,32,20,2048]{3,1,2,0:T(8,128)(2,1)} %all-to-all-done.1) | data formatting | bytes 20971520 | tf_op jit(solution)/shard_map/all_to_all | solution.py:61
  297.7 16.5 %reshape_reshape.3 = bf16[2560,2048]{1,0:T(8,128)(2,1)} reshape(bf16[4,32,20,2048]{3,2,1,0:T(8,128)(2,1)} %copy.86) | data formatting | bytes 20971520 | tf_op jit(solution)/shard_map/reshape;reshape | solution.py:223
  314.1 10.4 %convolution_clamp_fusion = f32[2560,512]{1,0:T(8,128)} fusion(bf16[2560,2048]{1,0:T(8,128)(2,1)} %reshape_reshape.3, bf16[1,2048,512]{2,1,0:T(8,128)(2,1)} %param.42), kind=kOutput, calls=%fused_computation.45 | convolution fusion | flops 5370019840 | bytes 17825792 | tf_op jit(solution)/shard_map/dot_general | solution.py:225
  324.5 18.5 %convolution_convert_fusion = bf16[2560,2048]{1,0:T(8,128)(2,1)} fusion(f32[2560,512]{1,0:T(8,128)} %convolution_clamp_fusion, bf16[2560,2048]{1,0:T(8,128)(2,1)} %reshape_reshape.3, bf16[1,512,2048]{2,1,0:T(8,128)(2,1)S(1)} %copy-done, bf16[1,2048,512]{2,1,0:T(8,128)(2,1)} %param.41), kind=kOutput, calls=%fused_computation.11 | convolution fusion | flops 10754457600 | bytes 30408704 | tf_op jit(solution)/shard_map/dot_general | solution.py:238
  343.2 9.3 %all_gather.28 = bf16[4,2,8]{2,1,0:T(2,128)(2,1)} all-gather(bf16[1,2,8]{2,1,0:T(2,128)(2,1)S(1)} %fusion.83), channel_id=1, replica_groups=mesh['ep_0'=4,'ep_1'=4,'ep_2'=2,'tp'=4] {'ep_0'}, dimensions={0}, use_global_device_ids=true | all-gather | bytes 160 | tf_op jit(solution)/shard_map/all_gather | solution.py:38
  352.5 1.4 copy.68
  354.8 2.3 copy.77
  357.1 4.9 copy.79
  365.2 2.1 divide_multiply_fusion.1
  367.2 2.1 reshape.283
  369.3 5.9 %fusion.49 = f32[12,128,128,2]{1,2,3,0:T(8,128)} fusion(f32[12,128,2,128]{3,2,1,0:T(2,128)S(1)} %reshape.283, f32[12,128,2,128]{3,2,1,0:T(2,128)} %reshape.282), kind=kOutput, calls=%fused_computation.80 | convolution fusion | flops 603979776 | bytes 4718592 | tf_op jit(solution)/shard_map/ctgn,csgn->ctsg/dot_general | solution.py:138
  375.3 3.1 copy.66
  378.5 29.6 %fusion = f32[12,2,8,64,128]{4,3,2,1,0:T(8,128)} fusion(f32[12,128,2,8,64]{1,0,4,3,2:T(8,128)} %get-tuple-element.78, f32[12,128,2,8]{1,3,2,0:T(8,128)S(1)} %copy-done.11, f32[12,128,128,2]{2,1,3,0:T(8,128)} %copy.66, pred[128,128]{1,0:T(8,128)(4,1)S(1)} %iota_compare_fusion.2), kind=kOutput, calls=%fused_computation.6 | convolution fusion | flops 2425356288 | bytes 14270464 | tf_op jit(solution)/shard_map/ctsge,csgep->ctgep/dot_general | solution.py:139
  408.2 2.4 fusion.64
  410.6 9.0 %fusion.15 = f32[12,128,2,8,64]{1,4,3,2,0:T(8,128)S(1)} fusion(f32[12,2,8,64,128]{4,3,2,1,0:T(8,128)} %fusion, f32[12,128,2,8]{1,3,2,0:T(8,128)S(1)} %copy.77, f32[12,2,8,64,128]{4,3,2,1,0:T(8,128)} %get-tuple-element.30, f32[2,8,64,128]{3,2,1,0:T(8,128)S(1)} %fusion.64, f32[12,2,8]{2,1,0:T(2,128)S(1)} %copy.75, f32[12,128,2,128,1]{3,2,1,0,4:T(2,128)S(1)} %bitcast.197), kind=kOutput, calls=%fused_computation.31 | convolution fusion | flops 2422210560 | bytes 21070592 | tf_op jit(solution)/shard_map/ctgn,cgepn->ctgep/dot_general | solution.py:165
  419.6 7.9 %copy.78 = f32[12,128,2,8,64]{1,0,4,3,2:T(8,128)} copy(f32[12,128,2,8,64]{1,4,3,2,0:T(8,128)S(1)} %fusion.15) | data formatting | bytes 12582912 | tf_op jit(solution)/shard_map/add | solution.py:168
  427.5 8.8 %reshape.286 = f32[1536,2,512]{0,2,1:T(8,128)} reshape(f32[12,128,2,8,64]{1,0,4,3,2:T(8,128)} %copy.78) | data formatting | bytes 12582912 | tf_op jit(solution)/shard_map/reshape | solution.py:168
  436.3 18.9 %multiply_reduce_fusion = f32[1536,2]{0,1:T(2,128)S(1)} fusion(f32[1536,2,512]{0,2,1:T(8,128)} %reshape.286, f32[2,512]{1,0:T(2,128)S(1)} %copy-done.18, bf16[1536,1024]{0,1:T(8,128)(2,1)} %copy.79, f32[1024]{0:T(1024)S(1)} %bitcast.207, f32[1539,1024]{0,1:T(8,128)} %copy-done.2, f32[1024]{0:T(1024)S(1)} %bitcast.210, f32[1024]{0:T(1024)S(1)} %bitcast.204, ...), kind=kLoop, calls=%fused_computation.35 | loop fusion | flops 33027072 | bytes 34635776 | tf_op jit(solution)/shard_map/reduce_sum | solution.py:174
  455.2 18.1 %fusion.11 = bf16[1536,1024]{0,1:T(8,128)(2,1)S(1)} fusion(f32[128,8,12,128]{3,2,1,0:T(8,128)S(1)} %bitcast.195, f32[1024]{0:T(1024)S(1)} %copy-done.34, f32[1536,2]{0,1:T(2,128)S(1)} %add_rsqrt_fusion, f32[1024]{0:T(1024)S(1)} %mul.586, bf16[1536,1024]{0,1:T(8,128)(2,1)S(1)} %copy-done.4, f32[1024]{0:T(1024)S(1)} %bitcast.208, f32[1539,1024]{0,1:T(8,128)} %copy-done.2, ...), kind=kLoop, calls=%fused_computation.22 | loop fusion | flops 34603008 | bytes 37785600 | tf_op jit(solution)/shard_map/convert_element_type | solution.py:175
  473.3 9.0 %convolution_convert_fusion.1 = bf16[1536,2048]{1,0:T(8,128)(2,1)} fusion(bf16[1536,1024]{0,1:T(8,128)(2,1)S(1)} %fusion.11, bf16[1024,2048]{1,0:T(8,128)(2,1)S(1)} %copy-done.44), kind=kOutput, calls=%fused_computation.14 | convolution fusion | flops 6445596672 | bytes 13631488 | tf_op jit(solution)/shard_map/dot_general | solution.py:177
  482.4 5.2 reshape.291
  487.6 4.8 all-to-all-start.2
  492.6 41.8 %all-to-all-done.2 = bf16[32,20,2048]{2,1,0:T(8,128)(2,1)} async-done(((bf16[32,20,2048]{2,1,0:T(8,128)(2,1)}), bf16[32,20,2048]{2,1,0:T(8,128)(2,1)}, u32[]{:S(2)}, u32[]{:S(2)}) %all-to-all-start.2) | async-done | bytes 2621472 | tf_op jit(solution)/shard_map/all_to_all | solution.py:245
  534.4 5.2 reshape.292
  539.6 7.5 %gather_fusion.1 = bf16[512,2048]{1,0:T(8,128)(2,1)} fusion(bf16[640,2048]{1,0:T(8,128)(2,1)} %reshape.292, s32[1024]{0:T(1024)S(1)} %pad_clamp_fusion), kind=kCustom, calls=%fused_computation.1 | custom fusion | bytes 4196352 | tf_op jit(solution)/shard_map/gather | solution.py:252
  547.1 4.1 reshape.293
  551.2 2.8 fusion.101
  (199 shorter events, 48.1 us)
Async XLA Ops:
  8.0 316.5 %copy-start = (bf16[1,512,2048]{2,1,0:T(8,128)(2,1)S(1)}, bf16[1,512,2048]{2,1,0:T(8,128)(2,1)}, u32[]{:S(2)}) copy-start(bf16[1,512,2048]{2,1,0:T(8,128)(2,1)} %param.43) | copy-start | bytes 6291460
  10.5 82.3 %collective-permute-start = (bf16[3,1536]{0,1:T(8,128)(2,1)S(1)}, bf16[3,1536]{0,1:T(8,128)(2,1)}, u32[]{:S(2)}, u32[]{:S(2)}) collective-permute-start(bf16[3,1536]{0,1:T(8,128)(2,1)S(1)} %copy.59), channel_id=1, source_target_pairs={{0,4},{4,8},{8,12},{12,16},{16,20},{20,24},{24,28},{28,32},{32,36}... | collective-permute-start | bytes 27656 | tf_op jit(solution)/shard_map/ppermute | solution.py:23
  18.7 0.6 copy-start.29
  27.3 14.6 %copy-start.45 = (f32[16]{0:T(128)S(1)}, f32[16]{0:T(128)}, u32[]{:S(2)}) copy-start(f32[16]{0:T(128)} %param.32) | copy-start | bytes 196
  27.3 14.7 %copy-start.12 = (f32[1536,16]{0,1:T(8,128)S(1)}, f32[1536,16]{0,1:T(8,128)}, u32[]{:S(2)}) copy-start(f32[1536,16]{0,1:T(8,128)} %param.34) | copy-start | bytes 294916
  27.3 14.7 %copy-start.14 = (bf16[1536,16]{0,1:T(8,128)(2,1)S(1)}, bf16[1536,16]{0,1:T(8,128)(2,1)}, u32[]{:S(2)}) copy-start(bf16[1536,16]{0,1:T(8,128)(2,1)} %param.27) | copy-start | bytes 147460
  27.3 14.7 %copy-start.43 = (f32[16]{0:T(128)S(1)}, f32[16]{0:T(128)}, u32[]{:S(2)}) copy-start(f32[16]{0:T(128)} %param.31) | copy-start | bytes 196
  32.5 116.6 %all-to-all-start = ((bf16[32,20,2048]{2,1,0:T(8,128)(2,1)}), bf16[32,20,2048]{2,1,0:T(8,128)(2,1)}, u32[]{:S(2)}, u32[]{:S(2)}) async-start(bf16[32,20,2048]{2,1,0:T(8,128)(2,1)} %reshape.290), calls=%async_computation.1 | async-start | bytes 6291456 | tf_op jit(solution)/shard_map/all_to_all | solution.py:221
  42.1 7.8 %copy-start.15 = (bf16[4,1024]{1,0:T(4,128)(2,1)S(1)}, bf16[4,1024]{1,0:T(4,128)(2,1)}, u32[]{:S(2)}) copy-start(bf16[4,1024]{1,0:T(4,128)(2,1)} %param.28) | copy-start | bytes 24580
  42.1 7.8 %copy-start.32 = (bf16[4,256]{1,0:T(4,128)(2,1)S(1)}, bf16[4,256]{1,0:T(4,128)(2,1)}, u32[]{:S(2)}) copy-start(bf16[4,256]{1,0:T(4,128)(2,1)} %param.29) | copy-start | bytes 6148
  46.0 1.3 copy-start.5
  83.9 13.4 %copy-start.16 = (bf16[4,2,8]{2,1,0:T(2,128)(2,1)}, bf16[4,2,8]{2,1,0:T(2,128)(2,1)S(1)}, u32[]{:S(2)}) copy-start(bf16[4,2,8]{2,1,0:T(2,128)(2,1)S(1)} %all_gather.27) | copy-start | bytes 388
  97.3 2.9 copy-start.2
  107.7 11.5 %copy-start.8 = (bf16[1536,256]{1,0:T(8,128)(2,1)S(1)}, bf16[1536,256]{1,0:T(8,128)(2,1)}, u32[]{:S(2)}) copy-start(bf16[1536,256]{1,0:T(8,128)(2,1)} %param.25) | copy-start | bytes 2359300
  120.1 5.7 %copy-start.10 = (f32[12,128,2,8]{1,0,3,2:T(8,128)S(1)}, f32[12,128,2,8]{1,0,3,2:T(8,128)}, u32[]{:S(2)}) copy-start(f32[12,128,2,8]{1,0,3,2:T(8,128)} %copy.61) | copy-start | bytes 294916
  125.8 11.2 %copy-start.7 = (f32[12,128,2,128]{3,2,1,0:T(2,128)S(1)}, f32[12,128,2,128]{3,2,1,0:T(2,128)}, u32[]{:S(2)}) copy-start(f32[12,128,2,128]{3,2,1,0:T(2,128)} %reshape.282) | copy-start | bytes 4718596
  161.2 121.9 %all-to-all-start.1 = ((bf16[4,32,20,2048]{3,1,2,0:T(8,128)(2,1)}), bf16[4,32,20,2048]{3,1,2,0:T(8,128)(2,1)}, u32[]{:S(2)}, u32[]{:S(2)}) async-start(bf16[4,32,20,2048]{3,1,2,0:T(8,128)(2,1)} %broadcast_in_dim.26), calls=%async_computation.2 | async-start | bytes 20971520 | tf_op jit(solution)/shard_map/all_to_all | solution.py:61
  167.2 60.8 %all-gather.6.cloned.1.call-start = ((), (), s32[]{:S(2)}) async-start(), calls=%async_computation.5 | async-start | bytes 1310720 | tf_op jit(solution)/shard_map/all_gather | solution.py:38
  167.2 35.0 %copy-start.21 = (f32[2,8]{1,0:T(2,128)S(1)}, f32[2,8]{1,0:T(2,128)}, u32[]{:S(2)}) copy-start(f32[2,8]{1,0:T(2,128)} %get-tuple-element.108) | copy-start | bytes 196
  167.2 35.0 %copy-start.35 = (f32[2,8]{1,0:T(2,128)S(1)}, f32[2,8]{1,0:T(2,128)}, u32[]{:S(2)}) copy-start(f32[2,8]{1,0:T(2,128)} %fusion.91) | copy-start | bytes 196
  167.2 36.0 %copy-start.17 = (bf16[4,2,8]{2,1,0:T(2,128)(2,1)S(1)}, bf16[4,2,8]{2,1,0:T(2,128)(2,1)}, u32[]{:S(2)}) copy-start(bf16[4,2,8]{2,1,0:T(2,128)(2,1)} %copy-done.16) | copy-start | bytes 388
  167.2 60.7 %copy-start.19 = (f32[2,8]{1,0:T(2,128)S(1)}, f32[2,8]{1,0:T(2,128)}, u32[]{:S(2)}) copy-start(f32[2,8]{1,0:T(2,128)} %get-tuple-element.96) | copy-start | bytes 196
  203.2 204.9 %all-gather.8.cloned.1.call-start = ((), (), s32[]{:S(2)}) async-start(), calls=%async_computation.6 | async-start | bytes 1310720 | tf_op jit(solution)/shard_map/all_gather | solution.py:38
  203.3 94.4 %copy-start.23 = (f32[2,8]{1,0:T(2,128)}, f32[2,8]{1,0:T(2,128)S(1)}, u32[]{:S(2)}) copy-start(f32[2,8]{1,0:T(2,128)S(1)} %get-tuple-element.97) | copy-start | bytes 196
  203.3 94.4 %copy-start.25 = (f32[2,8]{1,0:T(2,128)}, f32[2,8]{1,0:T(2,128)S(1)}, u32[]{:S(2)}) copy-start(f32[2,8]{1,0:T(2,128)S(1)} %get-tuple-element.98) | copy-start | bytes 196
  203.3 94.4 %copy-start.27 = (f32[2,8]{1,0:T(2,128)}, f32[2,8]{1,0:T(2,128)S(1)}, u32[]{:S(2)}) copy-start(f32[2,8]{1,0:T(2,128)S(1)} %get-tuple-element.99) | copy-start | bytes 196
  230.2 252.1 %reduce-scatter.5.cloned.1.call-start = ((), (), s32[]{:S(2)}) async-start(), calls=%async_computation.8 | async-start | bytes 13107200 | tf_op jit(solution)/shard_map/reduce_scatter | solution.py:237
  343.1 9.5 %copy-start.6 = (f32[12,128,2,8]{3,0,1,2:T(8,128)S(1)}, f32[12,128,2,8]{3,0,1,2:T(8,128)}, u32[]{:S(2)}) copy-start(f32[12,128,2,8]{3,0,1,2:T(8,128)} %copy-done.5) | copy-start | bytes 294916
  343.1 10.9 %copy-start.46 = (f32[16]{0:T(128)S(1)}, f32[16]{0:T(128)}, u32[]{:S(2)}) copy-start(f32[16]{0:T(128)} %param.33) | copy-start | bytes 196
  343.1 14.1 %copy-start.13 = (f32[12,2,8]{2,0,1:T(8,128)S(1)}, f32[12,2,8]{2,0,1:T(8,128)}, u32[]{:S(2)}) copy-start(f32[12,2,8]{2,0,1:T(8,128)} %get-tuple-element.79) | copy-start | bytes 2308
  343.1 21.9 %copy-start.9 = (bf16[1536,256]{1,0:T(8,128)(2,1)S(1)}, bf16[1536,256]{1,0:T(8,128)(2,1)}, u32[]{:S(2)}) copy-start(bf16[1536,256]{1,0:T(8,128)(2,1)} %param.26) | copy-start | bytes 2359300
  343.1 212.0 %reduce-scatter.3.cloned.1.call-start = ((), (), s32[]{:S(2)}) async-start(), calls=%async_computation.7 | async-start | bytes 7864320 | tf_op jit(solution)/shard_map/reduce_scatter | solution.py:176
  353.9 8.1 %copy-start.33 = (bf16[4,2,8]{2,1,0:T(2,128)(2,1)S(1)}, bf16[4,2,8]{2,1,0:T(2,128)(2,1)}, u32[]{:S(2)}) copy-start(bf16[4,2,8]{2,1,0:T(2,128)(2,1)} %all_gather.28) | copy-start | bytes 388
  367.2 11.1 %copy-start.11 = (f32[12,128,2,8]{1,3,2,0:T(8,128)S(1)}, f32[12,128,2,8]{1,3,2,0:T(8,128)}, u32[]{:S(2)}) copy-start(f32[12,128,2,8]{1,3,2,0:T(8,128)} %copy.68) | copy-start | bytes 294916
  378.4 29.7 %copy-start.20 = (f32[2,8]{1,0:T(2,128)S(1)}, f32[2,8]{1,0:T(2,128)}, u32[]{:S(2)}) copy-start(f32[2,8]{1,0:T(2,128)} %get-tuple-element.96) | copy-start | bytes 196
  378.4 29.7 %copy-start.22 = (f32[2,8]{1,0:T(2,128)S(1)}, f32[2,8]{1,0:T(2,128)}, u32[]{:S(2)}) copy-start(f32[2,8]{1,0:T(2,128)} %get-tuple-element.108) | copy-start | bytes 196
  378.4 29.7 %copy-start.24 = (f32[2,8]{1,0:T(2,128)S(1)}, f32[2,8]{1,0:T(2,128)}, u32[]{:S(2)}) copy-start(f32[2,8]{1,0:T(2,128)} %copy-done.23) | copy-start | bytes 196
  378.4 29.7 %copy-start.26 = (f32[2,8]{1,0:T(2,128)S(1)}, f32[2,8]{1,0:T(2,128)}, u32[]{:S(2)}) copy-start(f32[2,8]{1,0:T(2,128)} %copy-done.25) | copy-start | bytes 196
  378.4 29.7 %copy-start.28 = (f32[2,8]{1,0:T(2,128)S(1)}, f32[2,8]{1,0:T(2,128)}, u32[]{:S(2)}) copy-start(f32[2,8]{1,0:T(2,128)} %copy-done.27) | copy-start | bytes 196
  378.4 29.7 %copy-start.36 = (f32[2,8]{1,0:T(2,128)S(1)}, f32[2,8]{1,0:T(2,128)}, u32[]{:S(2)}) copy-start(f32[2,8]{1,0:T(2,128)} %fusion.91) | copy-start | bytes 196
  378.4 29.7 %copy-start.37 = (f32[2,8]{1,0:T(2,128)S(1)}, f32[2,8]{1,0:T(2,128)}, u32[]{:S(2)}) copy-start(f32[2,8]{1,0:T(2,128)} %get-tuple-element.75) | copy-start | bytes 196
  378.4 29.7 %copy-start.38 = (f32[2,8]{1,0:T(2,128)S(1)}, f32[2,8]{1,0:T(2,128)}, u32[]{:S(2)}) copy-start(f32[2,8]{1,0:T(2,128)} %get-tuple-element.76) | copy-start | bytes 196
  378.4 29.7 %copy-start.39 = (f32[2,8]{1,0:T(2,128)S(1)}, f32[2,8]{1,0:T(2,128)}, u32[]{:S(2)}) copy-start(f32[2,8]{1,0:T(2,128)} %get-tuple-element.93) | copy-start | bytes 196
  378.4 29.7 %copy-start.40 = (f32[2,8]{1,0:T(2,128)S(1)}, f32[2,8]{1,0:T(2,128)}, u32[]{:S(2)}) copy-start(f32[2,8]{1,0:T(2,128)} %get-tuple-element.94) | copy-start | bytes 196
  378.4 29.7 %copy-start.41 = (f32[2,8]{1,0:T(2,128)S(1)}, f32[2,8]{1,0:T(2,128)}, u32[]{:S(2)}) copy-start(f32[2,8]{1,0:T(2,128)} %get-tuple-element.95) | copy-start | bytes 196
  378.5 29.7 %copy-start.42 = (f32[2,8]{1,0:T(2,128)S(1)}, f32[2,8]{1,0:T(2,128)}, u32[]{:S(2)}) copy-start(f32[2,8]{1,0:T(2,128)} %multiply_bitcast_fusion) | copy-start | bytes 196
  427.5 8.8 %copy-start.18 = (f32[2,512]{1,0:T(2,128)S(1)}, f32[2,512]{1,0:T(2,128)}, u32[]{:S(2)}) copy-start(f32[2,512]{1,0:T(2,128)} %mul.591) | copy-start | bytes 12292
  436.3 18.9 %copy-start.3 = (f32[12,128,2,8,64]{1,0,4,3,2:T(8,128)S(1)}, f32[12,128,2,8,64]{1,0,4,3,2:T(8,128)}, u32[]{:S(2)}) copy-start(f32[12,128,2,8,64]{1,0,4,3,2:T(8,128)} %copy.78) | copy-start | bytes 18874372
  436.3 18.9 %copy-start.4 = (bf16[1536,1024]{0,1:T(8,128)(2,1)S(1)}, bf16[1536,1024]{0,1:T(8,128)(2,1)}, u32[]{:S(2)}) copy-start(bf16[1536,1024]{0,1:T(8,128)(2,1)} %copy.79) | copy-start | bytes 9437188
  436.3 18.9 %copy-start.34 = (f32[1024]{0:T(1024)S(1)}, f32[1024]{0:T(1024)}, u32[]{:S(2)}) copy-start(f32[1024]{0:T(1024)} %param.35) | copy-start | bytes 12292
  455.2 18.1 %copy-start.44 = (bf16[1024,2048]{1,0:T(8,128)(2,1)S(1)}, bf16[1024,2048]{1,0:T(8,128)(2,1)}, u32[]{:S(2)}) copy-start(bf16[1024,2048]{1,0:T(8,128)(2,1)} %param.36) | copy-start | bytes 12582916
  482.3 10.1 %copy-start.31 = (f32[128,4]{0,1:T(4,128)S(1)}, f32[128,4]{0,1:T(4,128)}, u32[]{:S(2)}) copy-start(f32[128,4]{0,1:T(4,128)} %param.40) | copy-start | bytes 6148
  482.3 10.3 %copy-start.30 = (s32[512,1]{0,1:T(1,128)S(1)}, s32[512,1]{0,1:T(1,128)}, u32[]{:S(2)}) copy-start(s32[512,1]{0,1:T(1,128)} %copy-done.29) | copy-start | bytes 6148
  487.6 46.8 %all-to-all-start.2 = ((bf16[32,20,2048]{2,1,0:T(8,128)(2,1)}), bf16[32,20,2048]{2,1,0:T(8,128)(2,1)}, u32[]{:S(2)}, u32[]{:S(2)}) async-start(bf16[32,20,2048]{2,1,0:T(8,128)(2,1)} %reshape.291), calls=%async_computation.4 | async-start | bytes 6291456 | tf_op jit(solution)/shard_map/all_to_all | solution.py:245
  539.6 15.5 %copy-start.1 = (bf16[1,512,2048]{2,1,0:T(8,128)(2,1)S(1)}, bf16[1,512,2048]{2,1,0:T(8,128)(2,1)}, u32[]{:S(2)}) copy-start(bf16[1,512,2048]{2,1,0:T(8,128)(2,1)} %param.43) | copy-start | bytes 6291460
Sparse Core Ops, SparseCore 0:
  203.3 24.6 all-gather.5
  230.4 24.6 all-gather.7
Sparse Core Ops, SparseCore 1:
  343.2 94.8 reduce-scatter.4
  482.4 59.3 reduce-scatter.2
where the time goes:
time: 572 us; the launch traced here: 563 us
  local copies, waits for them, and re-layouts  153 us (27%)
  waiting for transfers between devices  119 us (21%)
  other arithmetic  110 us (19%)
  matrix products  97.5 us (17%)
  blocking collectives  43.6 us (8%)
  starting transfers between devices  22.4 us (4%)
  between operations  16.6 us (3%)
    all_to_all x1, waiting for transfers between devices, copy_for_each(): lax.all_to_all(jnp.broadcast_to(value[None], (size, *value.shape)), axis,...  52.8 us
    all_gather x4, blocking collectives, entering_2(): lax.all_gather(part.astype(kind), axis)  43.6 us
    all_to_all x1, waiting for transfers between devices, experts_half(): lax.all_to_all(summed.reshape(experts, capacity, feature_count), EP, spli...  41.8 us
    dot_general x1, matrix products, mixer_half(): jnp.einsum('ctsge,csgep->ctgep', scores[..., None] * weight, scaled, prec...  29.6 us
    all_gather x2, waiting for transfers between devices, entering_2(): lax.all_gather(part.astype(kind), axis)  24.7 us
    reduce_sum x1, other arithmetic, mixer_half(): jnp.mean(gated_y * gated_y, axis=2, keepdims=True) + norm_eps  18.9 us
    dot_general x1, matrix products, experts_half(): jnp.dot(hidden_act, shrink_projection[0], preferred_element_type=jnp.floa...  18.5 us
    convert_element_type x1, other arithmetic, mixer_half(): (normed.reshape(tok_rows, inner_cols) * cluster_scaling_vector).astype(jn...  18.1 us
  transfers between devices with their start and end apart: 8, of which 3 were waited for; matrix products, arithmetic and copies ran while one was open for 61% of the time, Pallas kernels for 0%

commit v1 on v0

v1 whole, which is shorter than its diff:
```python
import functools

import jax
import jax.numpy as jnp
from jax import lax
from jax.experimental import pallas as pl
from jax.experimental.pallas import tpu as pltpu
from jax.sharding import Mesh
from jax.sharding import PartitionSpec as P


HEAD = 64
STATE = 128
SPAN = 128
PAIR = 2 * HEAD
CAP = 20
LATE = 8
EARLY = CAP - LATE
ROW_TILE = 256
EP = ("ep_0", "ep_1", "ep_2")
EP_TP = ("ep_0", "ep_1", "ep_2", "tp")

norm_eps = 1e-05
clamp_top = 7.0
sigmoid_sharp = 1.702
LOG2E = 1.4426950408889634
HIGHEST = lax.Precision.HIGHEST
f32 = jnp.float32
bf16 = jnp.bfloat16


def silu(v):
    half = 0.5 * v
    return half + half * jnp.tanh(half)


def mm(a, b):
    return jnp.dot(a, b, preferred_element_type=f32)


def mm_last(a, b):
    return lax.dot_general(a, b, (((1,), (1,)), ((), ())), preferred_element_type=f32)


def lanes_below(shape, limit):
    return lax.broadcasted_iota(jnp.int32, shape, 1) < limit


def params(*sem):
    return pltpu.CompilerParams(dimension_semantics=sem, vmem_limit_bytes=60 * 1024 * 1024)


def cost(flops, nbytes):
    return pl.CostEstimate(flops=int(flops), bytes_accessed=int(nbytes), transcendentals=0)


def expand_heads(row, heads):
    low = lanes_below((1, PAIR), HEAD)
    return [
        jnp.where(low, row[:, 2 * p : 2 * p + 1], row[:, 2 * p + 1 : 2 * p + 2])
        for p in range(heads // 2)
    ]


def states_kernel(
    x_ref, b_ref, c_ref, halo_ref, taps_ref, dtp_ref, spike_ref, off_ref, fade_ref,
    xs_ref, bs_ref, cs_ref, row_ref, state_ref, total_ref, send_ref, buf,
):
    step = pl.program_id(0)
    inner = x_ref.shape[1]
    group = b_ref.shape[1]
    heads = dtp_ref.shape[0]
    groups = group // STATE
    pairs = heads // groups // 2

    @pl.when(step == 0)
    def _():
        buf[0:8, :] = halo_ref[...].astype(f32)
        state_ref[...] = jnp.zeros_like(state_ref)
        total_ref[...] = jnp.zeros_like(total_ref)

    taps = taps_ref[...].astype(f32)
    for ref, out, base in ((x_ref, xs_ref, 0), (b_ref, bs_ref, inner), (c_ref, cs_ref, inner + group)):
        for j in range(0, ref.shape[1], 128):
            at = base + j
            cols = slice(at, at + 128)
            new = ref[:, j : j + 128].astype(f32)
            buf[8 : 8 + SPAN, cols] = new
            acc = new * taps[3:4, cols]
            for k in range(3):
                acc = acc + buf[5 + k : 5 + k + SPAN, cols] * taps[k : k + 1, cols]
            out[:, j : j + 128] = silu(acc).astype(bf16)
    buf[0:8, :] = buf[SPAN : SPAN + 8, :]

    pre = dtp_ref[...].astype(f32) + off_ref[...]
    dt = jnp.maximum(pre, 0.0) + jnp.log1p(jnp.exp(-jnp.abs(pre)))
    log_decay = (spike_ref[...] - jnp.exp(fade_ref[...]) * dt) * LOG2E
    upto = (
        lax.broadcasted_iota(jnp.int32, (SPAN, SPAN), 0)
        <= lax.broadcasted_iota(jnp.int32, (SPAN, SPAN), 1)
    ).astype(f32)
    cum = jnp.dot(log_decay, upto, precision=HIGHEST, preferred_element_type=f32)
    rows = cum - jnp.log2(dt)
    row_ref[0:heads, :] = rows
    row_ref[heads : 2 * heads, :] = cum
    factor = jnp.exp2(cum[:, SPAN - 1 : SPAN] - rows)
    end = jnp.concatenate([cum, jnp.zeros((128 - heads, SPAN), f32)], axis=0).T[SPAN - 1 : SPAN, 0:heads]
    total_ref[...] = total_ref[...] + jnp.concatenate(expand_heads(end, heads), axis=1)
    low = lanes_below((STATE, PAIR), HEAD)
    shrink = expand_heads(jnp.exp2(end), heads)
    for g in range(groups):
        bt = bs_ref[:, g * STATE : (g + 1) * STATE].astype(f32).T
        for p in range(pairs):
            q = g * pairs + p
            cols = slice(q * PAIR, (q + 1) * PAIR)
            left = jnp.concatenate(
                [bt * factor[2 * q : 2 * q + 1, :], bt * factor[2 * q + 1 : 2 * q + 2, :]], axis=0
            ).astype(bf16)
            res = mm(left, xs_ref[:, cols])
            state_ref[:, cols] = state_ref[:, cols] * shrink[q] + jnp.where(low, res[:STATE], res[STATE:])

    @pl.when(step == pl.num_programs(0) - 1)
    def _():
        put_message(send_ref, state_ref[...], total_ref[0:1, :])


def put_message(ref, state, total):
    hi = total.astype(bf16).astype(f32)
    mid = (total - hi).astype(bf16).astype(f32)
    low = total - hi - mid
    ref[0:STATE, :] = state.astype(bf16)
    ref[STATE : STATE + 16, :] = jnp.concatenate(
        [hi, mid, low, jnp.zeros((13, total.shape[1]), f32)], axis=0
    ).astype(bf16)


def prefix_kernel(msg_ref, own_ref, total_ref, own_out, total_out, send_ref):
    tail = msg_ref[STATE : STATE + 16, :].astype(f32)
    came = msg_ref[0:STATE, :].astype(f32)
    decay = tail[0:1] + tail[1:2] + tail[2:3]
    own = own_ref[0] + jnp.exp2(total_ref[0:1, :]) * came
    total = total_ref[0:1, :] + decay
    own_out[0] = own
    own_out[1] = own_ref[1] + jnp.exp2(total_ref[1:2, :]) * came
    total_out[...] = jnp.concatenate([total, total_ref[1:2, :] + decay], axis=0)
    put_message(send_ref, own, total)


def first_kernel(msg_ref, state_ref, total_ref, own_out, total_out, send_ref):
    tail = msg_ref[STATE : STATE + 16, :].astype(f32)
    came = msg_ref[0:STATE, :].astype(f32)
    decay = tail[0:1] + tail[1:2] + tail[2:3]
    own = state_ref[...] + jnp.exp2(total_ref[0:1, :]) * came
    total = total_ref[0:1, :] + decay
    own_out[0] = own
    own_out[1] = came
    total_out[...] = jnp.concatenate([total, decay], axis=0)
    put_message(send_ref, own, total)


def last_kernel(msg_ref, own_ref, total_ref, out_ref):
    out_ref[...] = own_ref[...] + jnp.exp2(total_ref[1:2, :]) * msg_ref[0:STATE, :].astype(f32)


def shifted(value, distance):
    return lax.ppermute(value, EP, [(i, i + distance) for i in range(lax.axis_size(EP) - distance)])


def entering_state(state, total, message):
    inner = state.shape[1]
    own_shape = [
        jax.ShapeDtypeStruct((2, STATE, inner), f32),
        jax.ShapeDtypeStruct((2, inner), f32),
        jax.ShapeDtypeStruct(message.shape, bf16),
    ]
    distance, ep = 1, lax.axis_size(EP)
    own = state
    while distance < ep:
        message = shifted(message, distance)
        last = 2 * distance >= ep
        if last:
            whole = pl.BlockSpec((None, STATE, inner), lambda i: (1, 0, 0))
            return pl.pallas_call(
                last_kernel,
                grid=(1,),
                in_specs=[
                    pl.BlockSpec(message.shape, lambda i: (0, 0)),
                    whole,
                    pl.BlockSpec((2, inner), lambda i: (0, 0)),
                ],
                out_specs=pl.BlockSpec((STATE, inner), lambda i: (0, 0)),
                out_shape=jax.ShapeDtypeStruct((STATE, inner), f32),
                compiler_params=params("arbitrary"),
                cost_estimate=cost(1e9, 2e6),
                name="last",
            )(message, own, total)
        own, total, message = pl.pallas_call(
            first_kernel if distance == 1 else prefix_kernel,
            out_shape=own_shape,
            compiler_params=params(),
            cost_estimate=cost(1e9, 3e6),
            name="prefix",
        )(message, own, total)
        distance *= 2


def mixer_kernel(
    xs_ref, bs_ref, cs_ref, z_ref, row_ref, enter_ref, skip_ref, gain_ref, w_ref,
    out_ref, state, gated, normed,
):
    step = pl.program_id(0)
    inner = xs_ref.shape[1]
    group = bs_ref.shape[1]
    heads = row_ref.shape[0] // 2
    groups = group // STATE
    pairs = heads // groups // 2
    wide = inner // groups

    @pl.when(step == 0)
    def _():
        state[...] = enter_ref[...]

    mask = lax.broadcasted_iota(jnp.int32, (SPAN, SPAN), 0) >= lax.broadcasted_iota(
        jnp.int32, (SPAN, SPAN), 1
    )
    low = lanes_below((STATE, PAIR), HEAD)
    rows = row_ref[0:heads, :]
    cum = jnp.concatenate(
        [row_ref[heads : 2 * heads, :], jnp.zeros((128 - heads, SPAN), f32)], axis=0
    ).T
    factor = jnp.exp2(row_ref[heads : 2 * heads, SPAN - 1 : SPAN] - rows)
    shrink = expand_heads(jnp.exp2(cum[SPAN - 1 : SPAN, 0:heads]), heads)
    for g in range(groups):
        gcols = slice(g * STATE, (g + 1) * STATE)
        bt = bs_ref[:, gcols].astype(f32).T
        cmat = cs_ref[:, gcols]
        c32 = cmat.astype(f32)
        scores = mm_last(cmat, bs_ref[:, gcols])
        squares = jnp.zeros((SPAN, PAIR), f32)
        for p in range(pairs):
            q = g * pairs + p
            cols = slice(q * PAIR, (q + 1) * PAIR)
            lefts, downs = [], []
            for h in (2 * q, 2 * q + 1):
                col = jnp.broadcast_to(cum[:, h : h + 1], (SPAN, SPAN))
                decay = jnp.exp2(jnp.where(mask, col - rows[h : h + 1, :], -1e30))
                lefts.append(
                    jnp.concatenate([(scores * decay).astype(bf16), (c32 * jnp.exp2(col)).astype(bf16)], axis=1)
                )
                downs.append((bt * factor[h : h + 1, :]).astype(bf16))
            xp = xs_ref[:, cols]
            sp = state[:, cols]
            res = mm(jnp.concatenate(lefts, axis=0), jnp.concatenate([xp, sp.astype(bf16)], axis=0))
            add = mm(jnp.concatenate(downs, axis=0), xp)
            state[:, cols] = sp * shrink[q] + jnp.where(low, add[:STATE], add[STATE:])
            y = jnp.where(low, res[:SPAN], res[SPAN:]) + xp.astype(f32) * skip_ref[:, cols]
            y = y * silu(z_ref[:, cols].astype(f32))
            gated[:, cols] = y
            squares = squares + y * y
        scale = lax.rsqrt(jnp.sum(squares, axis=1, keepdims=True) * (1.0 / wide) + norm_eps)
        wcols = slice(g * wide, (g + 1) * wide)
        normed[:, wcols] = (gated[:, wcols] * scale * gain_ref[:, wcols]).astype(bf16)
    out_ref[...] = mm(normed[...], w_ref[...]).astype(bf16)


def mixer_half(
    features, gating, insert, query, presoftplus, entry_taps, insert_taps, query_taps,
    offset, fading, skip, spike, gain, projection,
):
    rows, inner = features.shape
    group = insert.shape[1]
    heads = offset.shape[0]
    width = projection.shape[1]
    every = inner + 2 * group
    last = jnp.concatenate([a[rows - 8 :] for a in (features, insert, query)], axis=1)
    halo = shifted(last, 1)
    taps = jnp.concatenate([entry_taps, insert_taps, query_taps], axis=1)
    steps = rows // SPAN

    def block(n):
        return pl.BlockSpec((SPAN, n), lambda i: (i, 0))

    def whole(*shape):
        return pl.BlockSpec(shape, lambda i: (0,) * len(shape))

    def across(n):
        return pl.BlockSpec((n, SPAN), lambda i: (0, i))

    xs, bs, cs, row, state, total, message = pl.pallas_call(
        states_kernel,
        grid=(steps,),
        in_specs=[
            block(inner), block(group), block(group), whole(8, every), whole(4, every),
            across(heads), across(heads), whole(heads, 1), whole(heads, 1),
        ],
        out_specs=[
            block(inner), block(group), block(group), across(2 * heads),
            whole(STATE, inner), whole(1, inner), whole(STATE + 16, inner),
        ],
        out_shape=[
            jax.ShapeDtypeStruct((rows, inner), bf16),
            jax.ShapeDtypeStruct((rows, group), bf16),
            jax.ShapeDtypeStruct((rows, group), bf16),
            jax.ShapeDtypeStruct((2 * heads, rows), f32),
            jax.ShapeDtypeStruct((STATE, inner), f32),
            jax.ShapeDtypeStruct((1, inner), f32),
            jax.ShapeDtypeStruct((STATE + 16, inner), bf16),
        ],
        scratch_shapes=[pltpu.VMEM((SPAN + 8, every), f32)],
        compiler_params=params("arbitrary"),
        cost_estimate=cost(8e9, 1e7),
        name="states",
    )(
        features, insert, query, halo, taps, presoftplus.T, spike.T,
        offset.reshape(heads, 1), fading.reshape(heads, 1),
    )
    entering = entering_state(state, total, message)
    partial = pl.pallas_call(
        mixer_kernel,
        grid=(steps,),
        in_specs=[
            block(inner), block(group), block(group), block(inner), across(2 * heads),
            whole(STATE, inner), whole(1, inner), whole(1, inner), whole(inner, width),
        ],
        out_specs=block(width),
        out_shape=jax.ShapeDtypeStruct((rows, width), bf16),
        scratch_shapes=[
            pltpu.VMEM((STATE, inner), f32),
            pltpu.VMEM((SPAN, inner), f32),
            pltpu.VMEM((SPAN, inner), bf16),
        ],
        compiler_params=params("arbitrary"),
        cost_estimate=cost(2e10, 2e7),
        name="mixer",
    )(
        xs, bs, cs, gating, row, entering,
        jnp.repeat(skip, HEAD).reshape(1, inner), gain.reshape(1, inner), projection,
    )
    return lax.psum_scatter(partial, "tp", scatter_dimension=0, tiled=True)


FIRST = 16
SECOND = 40
OTHERS = 36


def second_slot(inside):
    other = inside < OTHERS
    return (
        jnp.where(other, inside // EARLY + 1, 0),
        jnp.where(other, inside % EARLY + LATE, inside - OTHERS + FIRST),
    )


def expert_of(rows, first, per, experts):
    at = lax.broadcasted_iota(jnp.int32, (rows, experts), 0) + first
    return (at // per == lax.broadcasted_iota(jnp.int32, (rows, experts), 1)).astype(bf16)


def route_kernel(x_ref, gain_ref, pick_ref, score_ref, token_ref, first_ref):
    tokens, width = x_ref.shape
    experts = first_ref.shape[0] // FIRST
    x = x_ref[...].astype(f32)
    x = x - jnp.mean(x, axis=1, keepdims=True)
    x = x * lax.rsqrt(jnp.mean(x * x, axis=1, keepdims=True) + norm_eps) * gain_ref[...]
    normed = x.astype(bf16)
    token_ref[:, 0:width] = normed
    weight = jnp.exp(score_ref[...])
    weight = weight / jnp.sum(weight, axis=0, keepdims=True)
    lane = lax.broadcasted_iota(jnp.int32, (experts, tokens), 0)
    taken = jnp.zeros((experts, tokens), f32)
    dense = jnp.zeros((experts, tokens), f32)
    for k in range(pick_ref.shape[0]):
        hit = pick_ref[k : k + 1, :] == lane
        taken = jnp.where(hit, 1.0, taken)
        dense = jnp.where(hit, weight[k : k + 1, :], dense)
    earlier = (
        lax.broadcasted_iota(jnp.int32, (tokens, tokens), 0)
        < lax.broadcasted_iota(jnp.int32, (tokens, tokens), 1)
    ).astype(bf16)
    slot = jnp.where(taken > 0, mm(taken.astype(bf16), earlier), -1.0)
    token_ref[:, width : width + 128] = jnp.concatenate(
        [slot, dense, jnp.zeros((128 - 2 * experts, tokens), f32)], axis=0
    ).T.astype(bf16)
    rows = experts * FIRST
    spread = mm(expert_of(rows, 0, FIRST, experts), slot.astype(bf16))
    wanted = lax.broadcasted_iota(jnp.int32, (rows, 1), 0) % FIRST
    first_ref[...] = mm((spread == wanted.astype(f32)).astype(bf16), normed).astype(bf16)


def second_kernel(table_ref, apart_ref, out_ref, *, experts):
    width = table_ref.shape[1] - 128
    rows = out_ref.shape[0]
    first = pl.program_id(0) * rows
    spread = mm_last(expert_of(rows, first, SECOND, experts), table_ref[:, width : width + experts])
    at = lax.broadcasted_iota(jnp.int32, (rows, 1), 0) + first
    block, wanted = second_slot(at % SECOND)
    hit = (spread == wanted.astype(f32)) & (apart_ref[...] == block)
    out_ref[...] = mm(hit.astype(bf16), table_ref[:, 0:width]).astype(bf16)


def expert_kernel(x_ref, gate_ref, up_ref, down_ref, out_ref):
    x = x_ref[...]
    g = jnp.minimum(mm(x, gate_ref[...]), clamp_top)
    u = jnp.clip(mm(x, up_ref[...]), -clamp_top, clamp_top) + 1.0
    act = g * (0.5 + 0.5 * jnp.tanh((0.5 * sigmoid_sharp) * g)) * u
    out_ref[...] = mm(act.astype(bf16), down_ref[...]).astype(bf16)


def expert(rows_in, gate, up, down):
    rows, width = rows_in.shape
    hidden = gate.shape[2]
    return pl.pallas_call(
        expert_kernel,
        grid=(rows // ROW_TILE,),
        in_specs=[
            pl.BlockSpec((ROW_TILE, width), lambda i: (i, 0)),
            pl.BlockSpec((None, width, hidden), lambda i: (0, 0, 0)),
            pl.BlockSpec((None, width, hidden), lambda i: (0, 0, 0)),
            pl.BlockSpec((None, hidden, width), lambda i: (0, 0, 0)),
        ],
        out_specs=pl.BlockSpec((ROW_TILE, width), lambda i: (i, 0)),
        out_shape=jax.ShapeDtypeStruct((rows, width), bf16),
        compiler_params=params("arbitrary"),
        cost_estimate=cost(6 * rows * width * hidden, 3 * 2 * width * hidden + 4 * rows * width),
        name="expert",
    )(rows_in, gate, up, down)


def gather_kernel(table_ref, apart_ref, back_ref, out_ref, pick, *, experts):
    rows = back_ref.shape[0]

    @pl.when(pl.program_id(0) == 0)
    def _():
        chosen = expert_of(rows, 0, SECOND, experts)
        table = table_ref[...]
        slot = mm_last(table[:, 0:experts], chosen)
        weight = mm_last(table[:, experts : 2 * experts], chosen)
        block, wanted = second_slot(lax.broadcasted_iota(jnp.int32, (1, rows), 1) % SECOND)
        hit = (slot == wanted.astype(f32)) & (apart_ref[...] == block)
        pick[...] = jnp.where(hit, weight, 0.0).astype(bf16)

    out_ref[...] = mm(pick[...], back_ref[...]).astype(bf16)


def final_kernel(table_ref, back_ref, sum_ref, out_ref, *, experts):
    rows = back_ref.shape[0]
    table = table_ref[...]
    chosen = expert_of(rows, 0, FIRST, experts)
    slot = mm_last(table[:, 0:experts], chosen)
    weight = mm_last(table[:, experts : 2 * experts], chosen)
    at = lax.broadcasted_iota(jnp.int32, (1, rows), 1) % FIRST
    own = mm(jnp.where(slot == at.astype(f32), weight, 0.0).astype(bf16), back_ref[...])
    out_ref[...] = (own + sum_ref[...].astype(f32)).astype(bf16)


def exchanged(value):
    return lax.all_to_all(value, EP, split_axis=0, concat_axis=0, tiled=True)


def experts_half(sample, gain, pick, score, gate, up, down):
    tokens, width = sample.shape
    experts = lax.axis_size(EP)
    blocks = lax.axis_size("tp")
    every = width + 128
    own, first_out = pl.pallas_call(
        route_kernel,
        out_shape=[
            jax.ShapeDtypeStruct((tokens, every), bf16),
            jax.ShapeDtypeStruct((experts * FIRST, width), bf16),
        ],
        compiler_params=params(),
        cost_estimate=cost(1e9, 3e6),
        name="route",
    )(sample, gain.reshape(1, width), pick.T, score.T)
    apart = (jnp.arange(blocks * tokens, dtype=jnp.int32) // tokens - lax.axis_index("tp")) % blocks
    table = lax.all_gather(own, "tp", axis=0, tiled=True)
    first_in = exchanged(first_out.reshape(experts, FIRST, width))
    late_rows = lax.all_gather(first_in[:, :LATE], "tp", axis=0, tiled=True).reshape(-1, width)

    count = experts * SECOND
    tile = count // 4
    second_out = pl.pallas_call(
        functools.partial(second_kernel, experts=experts),
        grid=(count // tile,),
        in_specs=[
            pl.BlockSpec((blocks * tokens, every), lambda i: (0, 0)),
            pl.BlockSpec((1, blocks * tokens), lambda i: (0, 0)),
        ],
        out_specs=pl.BlockSpec((tile, width), lambda i: (i, 0)),
        out_shape=jax.ShapeDtypeStruct((count, width), bf16),
        compiler_params=params("arbitrary"),
        cost_estimate=cost(3.2e9, 1e7),
        name="second",
    )(table, apart.reshape(1, -1))
    second_in = exchanged(second_out.reshape(experts, SECOND, width))

    late_part = expert(late_rows, gate, up, down)
    own_part = expert(first_in[:, LATE:].reshape(-1, width), gate, up, down)
    late_sum = lax.psum_scatter(
        late_part.reshape(blocks * experts, LATE, width), "tp", scatter_dimension=0, tiled=True
    )
    second_part = expert(second_in.reshape(count, width), gate, up, down)
    second_back = exchanged(second_part.reshape(experts, SECOND, width))
    first_back = exchanged(
        jnp.concatenate([late_sum, own_part.reshape(experts, FIRST - LATE, width)], axis=1)
    )
    col_tile = 512
    second_mix = pl.pallas_call(
        functools.partial(gather_kernel, experts=experts),
        grid=(width // col_tile,),
        in_specs=[
            pl.BlockSpec((blocks * tokens, 128), lambda i: (0, width // 128)),
            pl.BlockSpec((blocks * tokens, 1), lambda i: (0, 0)),
            pl.BlockSpec((count, col_tile), lambda i: (0, i)),
        ],
        out_specs=pl.BlockSpec((blocks * tokens, col_tile), lambda i: (0, i)),
        out_shape=jax.ShapeDtypeStruct((blocks * tokens, width), bf16),
        scratch_shapes=[pltpu.VMEM((blocks * tokens, count), bf16)],
        compiler_params=params("arbitrary"),
        cost_estimate=cost(3.2e9, 1e7),
        name="gather",
    )(table, apart.reshape(-1, 1), second_back.reshape(count, width))
    second_sum = lax.psum_scatter(second_mix, "tp", scatter_dimension=0, tiled=True)
    return pl.pallas_call(
        functools.partial(final_kernel, experts=experts),
        grid=(1,),
        in_specs=[
            pl.BlockSpec((tokens, 128), lambda i: (0, width // 128)),
            pl.BlockSpec((experts * FIRST, width), lambda i: (0, 0)),
            pl.BlockSpec((tokens, width), lambda i: (0, 0)),
        ],
        out_specs=pl.BlockSpec((tokens, width), lambda i: (0, 0)),
        out_shape=jax.ShapeDtypeStruct((tokens, width), bf16),
        compiler_params=params("arbitrary"),
        cost_estimate=cost(2e8, 2e6),
        name="final",
    )(own, first_back.reshape(experts * FIRST, width), second_sum)


def body(*args):
    moe_out = experts_half(*args[14:])
    mixed = mixer_half(*args[:14])
    return (mixed, moe_out)


def solution(mesh):
    split = Mesh(mesh.devices.reshape(4, 4, 2, mesh.shape["tp"]), ("ep_0", "ep_1", "ep_2", "tp"))
    return jax.shard_map(
        body,
        mesh=split,
        in_specs=(
            P(EP, "tp"),
            P(EP, "tp"),
            P(EP, "tp"),
            P(EP, "tp"),
            P(EP, "tp"),
            P(None, "tp"),
            P(None, "tp"),
            P(None, "tp"),
            P("tp"),
            P("tp"),
            P("tp"),
            P(EP, "tp"),
            P("tp"),
            P("tp", None),
            P(EP_TP, None),
            P(),
            P(EP_TP, None),
            P(EP_TP, None),
            P(EP, None, "tp"),
            P(EP, None, "tp"),
            P(EP, "tp", None),
        ),
        out_specs=(P(EP_TP, None), P(EP_TP, None)),
        check_vma=False,
    )
```

time: 572 us -> 397 us (0.69); the launches traced: 563 us -> 395 us
  local copies, waits for them, and re-layouts: 153 us -> 9.19 us
  Pallas kernels: 0 us -> 105 us
  other arithmetic: 110 us -> 5.22 us
  matrix products: 97.5 us -> 0 us
  waiting for transfers between devices: 119 us -> 180 us
  starting transfers between devices: 22.4 us -> 45 us
  blocking collectives: 43.6 us -> 36.9 us
    pallas_call x0 -> x14, Pallas kernels: none -> 105 us  [the longest x3 31.7 us: expert(): pl.pallas_call(expert_kernel, grid=(rows // ROW_TILE,), in_specs=[pl.Bloc...]
    dot_general x8 -> x0, matrix products: 97.5 us -> none  [the longest x1 29.6 us: mixer_half(): jnp.einsum('ctsge,csgep->ctgep', scores[..., None] * weight, scaled, prec...]
    all_gather x4 -> x0, blocking collectives: 43.6 us -> none  [entering_2(): lax.all_gather(part.astype(kind), axis)]
    reshape x9 -> x2, local copies, waits for them, and re-layouts: 44.1 us -> 1.36 us  [the longest x1 0.68 us: mixer_half(): offset.reshape(heads, 1)]
    all_to_all x0 -> x1, blocking collectives: none -> 36.9 us  [exchanged(): return lax.all_to_all(value, EP, split_axis=0, concat_axis=0, tiled=True)]
    mul x11 -> x0, other arithmetic: 28.8 us -> none  [the longest x3 12.3 us: causal_conv(): return jax.nn.silu(summed)]
    convert_element_type x14 -> x0, other arithmetic: 28.5 us -> none  [the longest x1 18.1 us: mixer_half(): (normed.reshape(tok_rows, inner_cols) * cluster_scaling_vector).astype(jn...]
    ppermute x1 -> x6, starting transfers between devices: 2.07 us -> 29.3 us  [shifted(): lax.ppermute(value, EP, [(i, i + distance) for i in range(lax.axis_size(E...]
  transfers between devices with their start and end apart: 8 -> 14, of which waited for: 3 -> 10; matrix products, arithmetic and copies ran while one was open for 61% -> 2% of each run, Pallas kernels for 0% -> 26%
where the time goes in v1:
time: 397 us; the launch traced here: 395 us
  waiting for transfers between devices  180 us (45%)
  Pallas kernels  105 us (26%)
  starting transfers between devices  45 us (11%)
  blocking collectives  36.9 us (9%)
  between operations  14 us (4%)
  local copies, waits for them, and re-layouts  9.19 us (2%)
  other arithmetic  5.22 us (1%)
    all_to_all x3, waiting for transfers between devices, exchanged(): return lax.all_to_all(value, EP, split_axis=0, concat_axis=0, tiled=True)  111 us
    all_to_all x1, blocking collectives, exchanged(): return lax.all_to_all(value, EP, split_axis=0, concat_axis=0, tiled=True)  36.9 us
    all_gather x1, waiting for transfers between devices, experts_half(): lax.all_gather(first_in[:, :LATE], 'tp', axis=0, tiled=True)  33.5 us
    pallas_call x3, Pallas kernels, expert(): pl.pallas_call(expert_kernel, grid=(rows // ROW_TILE,), in_specs=[pl.Bloc...  31.7 us
    ppermute x6, starting transfers between devices, shifted(): lax.ppermute(value, EP, [(i, i + distance) for i in range(lax.axis_size(E...  29.3 us
    pallas_call x1, Pallas kernels, mixer_half(): pl.pallas_call(mixer_kernel, grid=(steps,), in_specs=[block(inner), block...  24.4 us
    ppermute x6, waiting for transfers between devices, shifted(): lax.ppermute(value, EP, [(i, i + distance) for i in range(lax.axis_size(E...  20.4 us
    pallas_call x1, Pallas kernels, mixer_half(): pl.pallas_call(states_kernel, grid=(steps,), in_specs=[block(inner), bloc...  15.9 us
  transfers between devices with their start and end apart: 14, of which 10 were waited for; matrix products, arithmetic and copies ran while one was open for 2% of the time, Pallas kernels for 26%

profile of v1, /device:TPU:0, one launch (start us, length us, event | category | flops | bytes accessed | tf_op | source)
XLA Modules:
  0.0 395.4 jit_solution(6360446089520664527)
XLA Ops:
  7.2 0.0 all-gather.5.cloned.1.call-start
  7.2 3.6 route.1
  10.8 0.0 all-gather.5.cloned.1.call-update
  10.8 0.0 all-gather.3.cloned.1.call-start
  10.9 36.9 %all_to_all.20 = bf16[32,16,2048]{2,1,0:T(8,128)(2,1)S(1)} all-to-all(bf16[32,16,2048]{2,1,0:T(8,128)(2,1)} %bitcast.24), channel_id=1, replica_groups=mesh['ep_0'=4,'ep_1'=4,'ep_2'=2,'tp'=4] {'ep_0','ep_1','ep_2'}, dimensions={0} | all-to-all | bytes 4194304 | tf_op jit(solution)/shard_map/all_to_all | solution.py:458
  47.8 1.5 fusion.7
  49.3 0.0 all-gather.3.cloned.1.call-update
  49.3 0.6 and_select_fusion.apart_ref
  49.9 7.4 %second.1 = bf16[1280,2048]{1,0:T(8,128)(2,1)} custom-call(bf16[512,2176]{1,0:T(8,128)(2,1)} %all-gather.5.cloned.1.call-done.table_ref, s32[1,512]{1,0:T(1,128)} %and_select_fusion.apart_ref), custom_call_target="tpu_custom_call" | custom-call | flops 3200000000 | bytes 10000000 | tf_op jit(solution)/shard_map/second/pallas_call | solution.py:483
  57.3 4.9 %all-to-all-start.2 = ((bf16[32,40,2048]{2,1,0:T(8,128)(2,1)}), bf16[32,40,2048]{2,1,0:T(8,128)(2,1)}, u32[]{:S(2)}, u32[]{:S(2)}) async-start(bf16[32,40,2048]{2,1,0:T(8,128)(2,1)} %bitcast.21), calls=%async_computation.4 | async-start | bytes 10485760 | tf_op jit(solution)/shard_map/all_to_all | solution.py:458
  62.3 0.0 reduce-scatter.6.cloned.1.call-start
  62.3 33.5 %all-gather.3.cloned.1.call-done = bf16[128,8,2048]{2,1,0:T(8,128)(2,1)} async-done(((bf16[32,8,2048]{2,1,0:T(8,128)(2,1)}), bf16[128,8,2048]{2,1,0:T(8,128)(2,1)}) %all-gather.3.cloned.1.call-update) | async-done | bytes 4194320 | tf_op jit(solution)/shard_map/all_gather | solution.py:479
  95.8 11.8 %expert.3 = bf16[1024,2048]{1,0:T(8,128)(2,1)} custom-call(bf16[1024,2048]{1,0:T(8,128)(2,1)} %bitcast.27, bf16[1,2048,512]{2,1,0:T(8,128)(2,1)} %gate_ref.5, bf16[1,2048,512]{2,1,0:T(8,128)(2,1)} %up_ref.5, bf16[1,512,2048]{2,1,0:T(8,128)(2,1)} %down_ref.5), custom_call_target="tpu_custom_call" | custom-call | flops 6442450944 | bytes 14680064 | tf_op jit(solution)/shard_map/expert/pallas_call | solution.py:413
  107.6 0.0 reduce-scatter.6.cloned.1.call-update
  107.7 20.5 %all-to-all-done.2 = bf16[32,40,2048]{2,1,0:T(8,128)(2,1)} async-done(((bf16[32,40,2048]{2,1,0:T(8,128)(2,1)}), bf16[32,40,2048]{2,1,0:T(8,128)(2,1)}, u32[]{:S(2)}, u32[]{:S(2)}) %all-to-all-start.2) | async-done | bytes 5242912 | tf_op jit(solution)/shard_map/all_to_all | solution.py:458
  128.1 13.8 %expert.5 = bf16[1280,2048]{1,0:T(8,128)(2,1)} custom-call(bf16[1280,2048]{1,0:T(8,128)(2,1)} %bitcast.15.x_ref, bf16[1,2048,512]{2,1,0:T(8,128)(2,1)} %gate_ref.5, bf16[1,2048,512]{2,1,0:T(8,128)(2,1)} %up_ref.5, bf16[1,512,2048]{2,1,0:T(8,128)(2,1)} %down_ref.5), custom_call_target="tpu_custom_call" | custom-call | flops 8053063680 | bytes 16777216 | tf_op jit(solution)/shard_map/expert/pallas_call | solution.py:413
  142.0 0.0 copy-start.4
  142.0 0.0 copy-start.1
  142.0 0.0 copy-start.2
  142.0 5.0 %all-to-all-start.3 = ((bf16[32,40,2048]{2,1,0:T(8,128)(2,1)}), bf16[32,40,2048]{2,1,0:T(8,128)(2,1)}, u32[]{:S(2)}, u32[]{:S(2)}) async-start(bf16[32,40,2048]{2,1,0:T(8,128)(2,1)} %bitcast.20), calls=%async_computation.5 | async-start | bytes 10485760 | tf_op jit(solution)/shard_map/all_to_all | solution.py:458
  147.1 0.0 reduce-scatter.8.cloned.1.call-start
  147.2 2.0 collective-permute-start
  149.2 0.7 copy.25.off_ref
  149.9 0.7 copy.26.fade_ref
  150.5 0.8 add_select_fusion.apart_ref
  151.4 0.6 pad_maximum_fusion.2.taps_ref
  152.0 61.0 %all-to-all-done.3 = bf16[32,40,2048]{2,1,0:T(8,128)(2,1)} async-done(((bf16[32,40,2048]{2,1,0:T(8,128)(2,1)}), bf16[32,40,2048]{2,1,0:T(8,128)(2,1)}, u32[]{:S(2)}, u32[]{:S(2)}) %all-to-all-start.3) | async-done | bytes 5242912 | tf_op jit(solution)/shard_map/all_to_all | solution.py:458
  212.9 7.3 %gather.1 = bf16[512,2048]{1,0:T(8,128)(2,1)} custom-call(bf16[512,2176]{1,0:T(8,128)(2,1)} %all-gather.5.cloned.1.call-done.table_ref, s32[512,1]{1,0:T(8,128)} %add_select_fusion.apart_ref, bf16[1280,2048]{1,0:T(8,128)(2,1)} %bitcast.17.back_ref), custom_call_target="tpu_custom_call" | custom-call | flops 3200000000 | bytes 10000000 | tf_op jit(solution)/shard_map/gather/pallas_call | solution.py:509
  220.3 0.0 reduce-scatter.8.cloned.1.call-update
  220.3 0.0 reduce-scatter.4.cloned.1.call-start
  220.4 0.6 copy-done.12
  221.0 15.9 %states.1 = (bf16[1536,1024]{1,0:T(8,128)(2,1)}, bf16[1536,256]{1,0:T(8,128)(2,1)}, bf16[1536,256]{1,0:T(8,128)(2,1)}, f32[32,1536]{1,0:T(8,128)}, f32[128,1024]...) custom-call(bf16[1536,1024]{1,0:T(8,128)(2,1)} %x_ref.2, bf16[1536,256]{1,0:T(8,128)(2,1)} %b_ref.1, ...), custom_call_target="tpu_custom_call" | custom-call | flops 8000000000 | bytes 10000000 | tf_op jit(solution)/shard_map/states/pallas_call | solution.py:289
  236.8 1.3 collective-permute-start.1
  238.1 1.4 collective-permute-done.1.msg_ref
  239.5 0.7 copy-done.11
  240.3 2.3 prefix.4
  242.6 6.6 %collective-permute-start.2 = (bf16[144,1024]{1,0:T(8,128)(2,1)}, bf16[144,1024]{1,0:T(8,128)(2,1)S(1)}, u32[]{:S(2)}, u32[]{:S(2)}) collective-permute-start(bf16[144,1024]{1,0:T(8,128)(2,1)} %get-tuple-element.30), channel_id=1, source_target_pairs={{0,8},{4,12},{8,16},{12,20},{16,24},{20,28},{24,32},{28,36},{32,40... | collective-permute-start | bytes 884744 | tf_op jit(solution)/shard_map/ppermute | solution.py:166
  249.1 4.5 %collective-permute-done.2.msg_ref = bf16[144,1024]{1,0:T(8,128)(2,1)S(1)} collective-permute-done((bf16[144,1024]{1,0:T(8,128)(2,1)}, bf16[144,1024]{1,0:T(8,128)(2,1)S(1)}, u32[]{:S(2)}, u32[]{:S(2)}) %collective-permute-start.2) | collective-permute-done | bytes 294944 | tf_op jit(solution)/shard_map/ppermute | solution.py:166
  253.7 0.7 copy-done.7
  254.4 2.5 prefix.5
  256.9 5.5 %collective-permute-start.3 = (bf16[144,1024]{1,0:T(8,128)(2,1)}, bf16[144,1024]{1,0:T(8,128)(2,1)S(1)}, u32[]{:S(2)}, u32[]{:S(2)}) collective-permute-start(bf16[144,1024]{1,0:T(8,128)(2,1)} %get-tuple-element.33), channel_id=1, source_target_pairs={{0,16},{4,20},{8,24},{12,28},{16,32},{20,36},{24,40},{28,44},{32,4... | collective-permute-start | bytes 884744 | tf_op jit(solution)/shard_map/ppermute | solution.py:166
  262.4 6.4 %collective-permute-done.3.msg_ref = bf16[144,1024]{1,0:T(8,128)(2,1)S(1)} collective-permute-done((bf16[144,1024]{1,0:T(8,128)(2,1)}, bf16[144,1024]{1,0:T(8,128)(2,1)S(1)}, u32[]{:S(2)}, u32[]{:S(2)}) %collective-permute-start.3) | collective-permute-done | bytes 294944 | tf_op jit(solution)/shard_map/ppermute | solution.py:166
  268.8 0.7 copy-done.8
  269.5 2.5 prefix.6
  272.0 7.3 %collective-permute-start.4 = (bf16[144,1024]{1,0:T(8,128)(2,1)}, bf16[144,1024]{1,0:T(8,128)(2,1)S(1)}, u32[]{:S(2)}, u32[]{:S(2)}) collective-permute-start(bf16[144,1024]{1,0:T(8,128)(2,1)} %get-tuple-element.36), channel_id=1, source_target_pairs={{0,32},{4,36},{8,40},{12,44},{16,48},{20,52},{24,56},{28,60},{32,6... | collective-permute-start | bytes 884744 | tf_op jit(solution)/shard_map/ppermute | solution.py:166
  279.4 4.5 %collective-permute-done.4.msg_ref = bf16[144,1024]{1,0:T(8,128)(2,1)S(1)} collective-permute-done((bf16[144,1024]{1,0:T(8,128)(2,1)}, bf16[144,1024]{1,0:T(8,128)(2,1)S(1)}, u32[]{:S(2)}, u32[]{:S(2)}) %collective-permute-start.4) | collective-permute-done | bytes 294944 | tf_op jit(solution)/shard_map/ppermute | solution.py:166
  283.9 0.7 copy-done.9
  284.6 2.5 prefix.7
  287.1 6.7 %collective-permute-start.5 = (bf16[144,1024]{1,0:T(8,128)(2,1)}, bf16[144,1024]{1,0:T(8,128)(2,1)S(1)}, u32[]{:S(2)}, u32[]{:S(2)}) collective-permute-start(bf16[144,1024]{1,0:T(8,128)(2,1)} %get-tuple-element.39), channel_id=1, source_target_pairs={{0,64},{4,68},{8,72},{12,76},{16,80},{20,84},{24,88},{28,92},{32,9... | collective-permute-start | bytes 884744 | tf_op jit(solution)/shard_map/ppermute | solution.py:166
  293.8 0.1 broadcast_in_dim.3
  293.9 0.7 reshape_reshape.3.skip_ref
  294.5 3.6 collective-permute-done.5.msg_ref
  298.1 0.7 copy-done.10
  298.8 2.0 last.1.enter_ref
  300.8 24.4 %mixer.1 = bf16[1536,2048]{1,0:T(8,128)(2,1)} custom-call(bf16[1536,1024]{1,0:T(8,128)(2,1)} %get-tuple-element.23.xs_ref, bf16[1536,256]{1,0:T(8,128)(2,1)} %get-tuple-element.24.bs_ref, bf16[1536,256]{1,0:T(8,128)(2,1)} %get-tuple-element.25.cs_ref, bf16[1536,1024]{1,0:T(8,128)(2,1)} %z_ref.1, f32[32,1536]{1,0:T(8,128)} %get-tuple-element.26.row_ref, ...), custom_call_target="tpu_custom_call" | custom-call | flops 20000000000 | bytes 20000000 | tf_op jit(solution)/shard_map/mixer/pallas_call | solution.py:318
  325.2 0.0 reduce-scatter.4.cloned.1.call-update
  325.3 6.1 %expert.4 = bf16[256,2048]{1,0:T(8,128)(2,1)} custom-call(bf16[256,2048]{1,0:T(8,128)(2,1)} %get-tuple-element.45.x_ref, bf16[1,2048,512]{2,1,0:T(8,128)(2,1)} %gate_ref.5, bf16[1,2048,512]{2,1,0:T(8,128)(2,1)} %up_ref.5, bf16[1,512,2048]{2,1,0:T(8,128)(2,1)} %down_ref.5), custom_call_target="tpu_custom_call" | custom-call | flops 1610612736 | bytes 8388608 | tf_op jit(solution)/shard_map/expert/pallas_call | solution.py:413
  331.3 3.2 pad_maximum_fusion
  334.5 5.6 %all-to-all-start.1 = ((bf16[32,16,2048]{2,1,0:T(8,128)(2,1)}), bf16[32,16,2048]{2,1,0:T(8,128)(2,1)S(1)}, u32[]{:S(2)}, u32[]{:S(2)}) async-start(bf16[32,16,2048]{2,1,0:T(8,128)(2,1)} %pad_maximum_fusion), calls=%async_computation.3 | async-start | bytes 4194304 | tf_op jit(solution)/shard_map/all_to_all | solution.py:458
  340.1 0.0 reduce-scatter.8.cloned.1.call-done.sum_ref
  340.1 30.0 %all-to-all-done.1 = bf16[32,16,2048]{2,1,0:T(8,128)(2,1)S(1)} async-done(((bf16[32,16,2048]{2,1,0:T(8,128)(2,1)}), bf16[32,16,2048]{2,1,0:T(8,128)(2,1)S(1)}, u32[]{:S(2)}, u32[]{:S(2)}) %all-to-all-start.1) | async-done | bytes 2097184 | tf_op jit(solution)/shard_map/all_to_all | solution.py:458
  370.2 1.4 copy-done
  371.6 3.1 final.1
  374.7 14.2 %reduce-scatter.4.cloned.1.call-done = bf16[384,2048]{1,0:T(8,128)(2,1)} async-done(((bf16[1536,2048]{1,0:T(8,128)(2,1)}), bf16[384,2048]{1,0:T(8,128)(2,1)}) %reduce-scatter.4.cloned.1.call-update) | async-done | bytes 1572880 | tf_op jit(solution)/shard_map/reduce_scatter | solution.py:339
  (26 shorter events, 0.1 us)
Async XLA Ops:
  7.2 42.7 %all-gather.5.cloned.1.call-start = ((), (), s32[]{:S(2)}) async-start(), calls=%async_computation.10 | async-start | bytes 2785280 | tf_op jit(solution)/shard_map/all_gather | solution.py:477
  10.8 85.0 %all-gather.3.cloned.1.call-start = ((), (), s32[]{:S(2)}) async-start(), calls=%async_computation.8 | async-start | bytes 5242880 | tf_op jit(solution)/shard_map/all_gather | solution.py:479
  57.3 70.8 %all-to-all-start.2 = ((bf16[32,40,2048]{2,1,0:T(8,128)(2,1)}), bf16[32,40,2048]{2,1,0:T(8,128)(2,1)}, u32[]{:S(2)}, u32[]{:S(2)}) async-start(bf16[32,40,2048]{2,1,0:T(8,128)(2,1)} %bitcast.21), calls=%async_computation.4 | async-start | bytes 10485760 | tf_op jit(solution)/shard_map/all_to_all | solution.py:458
  62.3 269.1 %reduce-scatter.6.cloned.1.call-start = ((), (), s32[]{:S(2)}) async-start(), calls=%async_computation.9 | async-start | bytes 5242880 | tf_op jit(solution)/shard_map/reduce_scatter | solution.py:500
  142.0 5.2 %slice-start = ((bf16[1536,1024]{1,0:T(8,128)(2,1)}), bf16[8,1024]{1,0:T(8,128)(2,1)S(1)}, s32[]{:S(2)}) async-start(bf16[1536,1024]{1,0:T(8,128)(2,1)} %x_ref.2), calls=%async_computation.12 | async-start | bytes 32768 | tf_op jit(solution)/shard_map/slice | solution.py:275
  142.0 5.2 %slice-start.1 = ((bf16[1536,256]{1,0:T(8,128)(2,1)}), bf16[8,256]{1,0:T(8,128)(2,1)S(1)}, s32[]{:S(2)}) async-start(bf16[1536,256]{1,0:T(8,128)(2,1)} %b_ref.1), calls=%async_computation.13 | async-start | bytes 8192 | tf_op jit(solution)/shard_map/slice | solution.py:275
  142.0 5.2 %slice-start.2 = ((bf16[1536,256]{1,0:T(8,128)(2,1)}), bf16[8,256]{1,0:T(8,128)(2,1)S(1)}, s32[]{:S(2)}) async-start(bf16[1536,256]{1,0:T(8,128)(2,1)} %c_ref.1), calls=%async_computation.14 | async-start | bytes 8192 | tf_op jit(solution)/shard_map/slice | solution.py:275
  142.0 7.2 %copy-start.4 = (f32[16]{0:T(128)S(1)}, f32[16]{0:T(128)}, u32[]{:S(2)}) copy-start(f32[16]{0:T(128)} %param.29) | copy-start | bytes 196
  142.0 7.9 %copy-start.5 = (f32[16]{0:T(128)S(1)}, f32[16]{0:T(128)}, u32[]{:S(2)}) copy-start(f32[16]{0:T(128)} %param.30) | copy-start | bytes 196
  142.0 9.4 %copy-start.1 = (bf16[4,1024]{1,0:T(4,128)(2,1)S(1)}, bf16[4,1024]{1,0:T(4,128)(2,1)}, u32[]{:S(2)}) copy-start(bf16[4,1024]{1,0:T(4,128)(2,1)} %param.26) | copy-start | bytes 24580
  142.0 9.4 %copy-start.2 = (bf16[4,256]{1,0:T(4,128)(2,1)S(1)}, bf16[4,256]{1,0:T(4,128)(2,1)}, u32[]{:S(2)}) copy-start(bf16[4,256]{1,0:T(4,128)(2,1)} %param.28) | copy-start | bytes 6148
  142.0 9.4 %copy-start.3 = (bf16[4,256]{1,0:T(4,128)(2,1)S(1)}, bf16[4,256]{1,0:T(4,128)(2,1)}, u32[]{:S(2)}) copy-start(bf16[4,256]{1,0:T(4,128)(2,1)} %param.27) | copy-start | bytes 6148
  142.0 70.9 %all-to-all-start.3 = ((bf16[32,40,2048]{2,1,0:T(8,128)(2,1)}), bf16[32,40,2048]{2,1,0:T(8,128)(2,1)}, u32[]{:S(2)}, u32[]{:S(2)}) async-start(bf16[32,40,2048]{2,1,0:T(8,128)(2,1)} %bitcast.20), calls=%async_computation.5 | async-start | bytes 10485760 | tf_op jit(solution)/shard_map/all_to_all | solution.py:458
  147.1 193.0 %reduce-scatter.8.cloned.1.call-start = ((), (), s32[]{:S(2)}) async-start(), calls=%async_computation.11 | async-start | bytes 2621440 | tf_op jit(solution)/shard_map/reduce_scatter | solution.py:524
  147.2 73.2 %collective-permute-start = (bf16[8,1536]{1,0:T(8,128)(2,1)S(1)}, bf16[8,1536]{1,0:T(8,128)(2,1)S(1)}, u32[]{:S(2)}, u32[]{:S(2)}) collective-permute-start(bf16[8,1536]{1,0:T(8,128)(2,1)S(1)} %pad_maximum_fusion.1), channel_id=1, source_target_pairs={{0,4},{4,8},{8,12},{12,16},{16,20},{20,24},{24,28},{28,32},{32,36}... | collective-permute-start | bytes 73736 | tf_op jit(solution)/shard_map/ppermute | solution.py:166
  220.3 168.6 %reduce-scatter.4.cloned.1.call-start = ((), (), s32[]{:S(2)}) async-start(), calls=%async_computation.7 | async-start | bytes 7864320 | tf_op jit(solution)/shard_map/reduce_scatter | solution.py:339
  220.4 0.6 copy-start.12
  236.8 2.7 collective-permute-start.1
  239.5 0.7 copy-start.11
  242.6 11.1 %collective-permute-start.2 = (bf16[144,1024]{1,0:T(8,128)(2,1)}, bf16[144,1024]{1,0:T(8,128)(2,1)S(1)}, u32[]{:S(2)}, u32[]{:S(2)}) collective-permute-start(bf16[144,1024]{1,0:T(8,128)(2,1)} %get-tuple-element.30), channel_id=1, source_target_pairs={{0,8},{4,12},{8,16},{12,20},{16,24},{20,28},{24,32},{28,36},{32,40... | collective-permute-start | bytes 884744 | tf_op jit(solution)/shard_map/ppermute | solution.py:166
  253.7 0.7 copy-start.7
  256.9 11.9 %collective-permute-start.3 = (bf16[144,1024]{1,0:T(8,128)(2,1)}, bf16[144,1024]{1,0:T(8,128)(2,1)S(1)}, u32[]{:S(2)}, u32[]{:S(2)}) collective-permute-start(bf16[144,1024]{1,0:T(8,128)(2,1)} %get-tuple-element.33), channel_id=1, source_target_pairs={{0,16},{4,20},{8,24},{12,28},{16,32},{20,36},{24,40},{28,44},{32,4... | collective-permute-start | bytes 884744 | tf_op jit(solution)/shard_map/ppermute | solution.py:166
  268.8 0.7 copy-start.8
  269.5 24.3 %copy-start.6 = (f32[16]{0:T(128)S(1)}, f32[16]{0:T(128)}, u32[]{:S(2)}) copy-start(f32[16]{0:T(128)} %param.31) | copy-start | bytes 196
  272.0 11.9 %collective-permute-start.4 = (bf16[144,1024]{1,0:T(8,128)(2,1)}, bf16[144,1024]{1,0:T(8,128)(2,1)S(1)}, u32[]{:S(2)}, u32[]{:S(2)}) collective-permute-start(bf16[144,1024]{1,0:T(8,128)(2,1)} %get-tuple-element.36), channel_id=1, source_target_pairs={{0,32},{4,36},{8,40},{12,44},{16,48},{20,52},{24,56},{28,60},{32,6... | collective-permute-start | bytes 884744 | tf_op jit(solution)/shard_map/ppermute | solution.py:166
  283.9 0.7 copy-start.9
  287.1 11.0 %collective-permute-start.5 = (bf16[144,1024]{1,0:T(8,128)(2,1)}, bf16[144,1024]{1,0:T(8,128)(2,1)S(1)}, u32[]{:S(2)}, u32[]{:S(2)}) collective-permute-start(bf16[144,1024]{1,0:T(8,128)(2,1)} %get-tuple-element.39), channel_id=1, source_target_pairs={{0,64},{4,68},{8,72},{12,76},{16,80},{20,84},{24,88},{28,92},{32,9... | collective-permute-start | bytes 884744 | tf_op jit(solution)/shard_map/ppermute | solution.py:166
  298.1 0.7 copy-start.10
  334.5 35.6 %all-to-all-start.1 = ((bf16[32,16,2048]{2,1,0:T(8,128)(2,1)}), bf16[32,16,2048]{2,1,0:T(8,128)(2,1)S(1)}, u32[]{:S(2)}, u32[]{:S(2)}) async-start(bf16[32,16,2048]{2,1,0:T(8,128)(2,1)} %pad_maximum_fusion), calls=%async_computation.3 | async-start | bytes 4194304 | tf_op jit(solution)/shard_map/all_to_all | solution.py:458
  370.2 1.4 copy-start
Sparse Core Ops, SparseCore 0:
  11.0 34.3 all-gather.4
  49.4 46.3 all-gather.2
  107.8 47.1 reduce-scatter.5
  220.4 26.2 reduce-scatter.7
  325.4 63.4 reduce-scatter.3

commit v2 on v1

--- a/solution.py
+++ b/solution.py
@@ -64,7 +64,7 @@
 
 def states_kernel(
     x_ref, b_ref, c_ref, halo_ref, taps_ref, dtp_ref, spike_ref, off_ref, fade_ref,
-    xs_ref, bs_ref, cs_ref, row_ref, state_ref, total_ref, send_ref, buf,
+    xs_ref, bs_ref, cs_ref, row_ref, send_ref, buf, state, total,
 ):
     step = pl.program_id(0)
     inner = x_ref.shape[1]
@@ -76,8 +76,8 @@
     @pl.when(step == 0)
     def _():
         buf[0:8, :] = halo_ref[...].astype(f32)
-        state_ref[...] = jnp.zeros_like(state_ref)
-        total_ref[...] = jnp.zeros_like(total_ref)
+        state[...] = jnp.zeros_like(state)
+        total[...] = jnp.zeros_like(total)
 
     taps = taps_ref[...].astype(f32)
     for ref, out, base in ((x_ref, xs_ref, 0), (b_ref, bs_ref, inner), (c_ref, cs_ref, inner + group)):
@@ -105,7 +105,7 @@
     row_ref[heads : 2 * heads, :] = cum
     factor = jnp.exp2(cum[:, SPAN - 1 : SPAN] - rows)
     end = jnp.concatenate([cum, jnp.zeros((128 - heads, SPAN), f32)], axis=0).T[SPAN - 1 : SPAN, 0:heads]
-    total_ref[...] = total_ref[...] + jnp.concatenate(expand_heads(end, heads), axis=1)
+    total[...] = total[...] + jnp.concatenate(expand_heads(end, heads), axis=1)
     low = lanes_below((STATE, PAIR), HEAD)
     shrink = expand_heads(jnp.exp2(end), heads)
     for g in range(groups):
@@ -117,91 +117,104 @@
                 [bt * factor[2 * q : 2 * q + 1, :], bt * factor[2 * q + 1 : 2 * q + 2, :]], axis=0
             ).astype(bf16)
             res = mm(left, xs_ref[:, cols])
-            state_ref[:, cols] = state_ref[:, cols] * shrink[q] + jnp.where(low, res[:STATE], res[STATE:])
+            state[:, cols] = state[:, cols] * shrink[q] + jnp.where(low, res[:STATE], res[STATE:])
 
     @pl.when(step == pl.num_programs(0) - 1)
     def _():
-        put_message(send_ref, state_ref[...], total_ref[0:1, :])
-
-
-def put_message(ref, state, total):
-    hi = total.astype(bf16).astype(f32)
-    mid = (total - hi).astype(bf16).astype(f32)
-    low = total - hi - mid
-    ref[0:STATE, :] = state.astype(bf16)
-    ref[STATE : STATE + 16, :] = jnp.concatenate(
-        [hi, mid, low, jnp.zeros((13, total.shape[1]), f32)], axis=0
-    ).astype(bf16)
-
-
-def prefix_kernel(msg_ref, own_ref, total_ref, own_out, total_out, send_ref):
-    tail = msg_ref[STATE : STATE + 16, :].astype(f32)
-    came = msg_ref[0:STATE, :].astype(f32)
-    decay = tail[0:1] + tail[1:2] + tail[2:3]
-    own = own_ref[0] + jnp.exp2(total_ref[0:1, :]) * came
-    total = total_ref[0:1, :] + decay
-    own_out[0] = own
-    own_out[1] = own_ref[1] + jnp.exp2(total_ref[1:2, :]) * came
-    total_out[...] = jnp.concatenate([total, total_ref[1:2, :] + decay], axis=0)
-    put_message(send_ref, own, total)
-
-
-def first_kernel(msg_ref, state_ref, total_ref, own_out, total_out, send_ref):
-    tail = msg_ref[STATE : STATE + 16, :].astype(f32)
-    came = msg_ref[0:STATE, :].astype(f32)
-    decay = tail[0:1] + tail[1:2] + tail[2:3]
-    own = state_ref[...] + jnp.exp2(total_ref[0:1, :]) * came
-    total = total_ref[0:1, :] + decay
-    own_out[0] = own
-    own_out[1] = came
-    total_out[...] = jnp.concatenate([total, decay], axis=0)
-    put_message(send_ref, own, total)
-
-
-def last_kernel(msg_ref, own_ref, total_ref, out_ref):
-    out_ref[...] = own_ref[...] + jnp.exp2(total_ref[1:2, :]) * msg_ref[0:STATE, :].astype(f32)
+        half_cols = inner // 2
+        t = total[0:1, :]
+        hi = t.astype(bf16).astype(f32)
+        mid = (t - hi).astype(bf16).astype(f32)
+        tail = jnp.concatenate([hi, mid, t - hi - mid, jnp.zeros((5, inner), f32)], axis=0)
+        for e in range(send_ref.shape[0]):
+            rows_of, cols = slice(8 * (e // 2), 8 * (e // 2) + 8), slice(e % 2 * half_cols, (e % 2 + 1) * half_cols)
+            send_ref[e] = jnp.concatenate([state[rows_of, cols], tail[:, cols]], axis=0).astype(bf16)
+
+
+def place_of(device):
+    return {"ep_0": device // 8, "ep_1": device // 2 % 4, "ep_2": device % 2}
+
+
+def entering_kernel(msg_ref, out_ref, came, before, back, send_sem, recv_sem, send_sem2, recv_sem2):
+    ep = msg_ref.shape[0]
+    half_cols = msg_ref.shape[2]
+    me = (lax.axis_index("ep_0") * 4 + lax.axis_index("ep_1")) * 2 + lax.axis_index("ep_2")
+    barrier = pltpu.get_barrier_semaphore()
+
+    @pl.loop(1, ep)
+    def _(k):
+        pl.semaphore_signal(
+            barrier, inc=1, device_id=place_of((me + k) % ep), device_id_type=pl.DeviceIdType.MESH
+        )
+
+    pl.semaphore_wait(barrier, ep - 1)
+
+    def there(k):
+        to = (me + k) % ep
+        return pltpu.make_async_remote_copy(
+            src_ref=msg_ref.at[to], dst_ref=came.at[me], send_sem=send_sem.at[k], recv_sem=recv_sem.at[k],
+            device_id=place_of(to), device_id_type=pl.DeviceIdType.MESH,
+        )
+
+    def returned(k):
+        to = (me + k) % ep
+        return pltpu.make_async_remote_copy(
+            src_ref=before.at[to], dst_ref=back.at[me], send_sem=send_sem2.at[k], recv_sem=recv_sem2.at[k],
+            device_id=place_of(to), device_id_type=pl.DeviceIdType.MESH,
+        )
+
+    @pl.loop(1, ep)
+    def _(k):
+        there(k).start()
+
+    came[me] = msg_ref[me]
+
+    @pl.loop(1, ep)
+    def _(k):
+        there(k).wait()
+
+    running = jnp.zeros((8, half_cols), f32)
+    for i in range(ep):
+        before[i] = running
+        block = came[i].astype(f32)
+        running = running * jnp.exp2(block[8:9] + block[9:10] + block[10:11]) + block[0:8]
+
+    @pl.loop(1, ep)
+    def _(k):
+        returned(k).start()
+
+    back[me] = before[me]
+
+    @pl.loop(1, ep)
+    def _(k):
+        returned(k).wait()
+
+    for e in range(ep):
+        out_ref[8 * (e // 2) : 8 * (e // 2) + 8, e % 2 * half_cols : (e % 2 + 1) * half_cols] = back[e]
 
 
 def shifted(value, distance):
     return lax.ppermute(value, EP, [(i, i + distance) for i in range(lax.axis_size(EP) - distance)])
 
 
-def entering_state(state, total, message):
-    inner = state.shape[1]
-    own_shape = [
-        jax.ShapeDtypeStruct((2, STATE, inner), f32),
-        jax.ShapeDtypeStruct((2, inner), f32),
-        jax.ShapeDtypeStruct(message.shape, bf16),
-    ]
-    distance, ep = 1, lax.axis_size(EP)
-    own = state
-    while distance < ep:
-        message = shifted(message, distance)
-        last = 2 * distance >= ep
-        if last:
-            whole = pl.BlockSpec((None, STATE, inner), lambda i: (1, 0, 0))
-            return pl.pallas_call(
-                last_kernel,
-                grid=(1,),
-                in_specs=[
-                    pl.BlockSpec(message.shape, lambda i: (0, 0)),
-                    whole,
-                    pl.BlockSpec((2, inner), lambda i: (0, 0)),
-                ],
-                out_specs=pl.BlockSpec((STATE, inner), lambda i: (0, 0)),
-                out_shape=jax.ShapeDtypeStruct((STATE, inner), f32),
-                compiler_params=params("arbitrary"),
-                cost_estimate=cost(1e9, 2e6),
-                name="last",
-            )(message, own, total)
-        own, total, message = pl.pallas_call(
-            first_kernel if distance == 1 else prefix_kernel,
-            out_shape=own_shape,
-            compiler_params=params(),
-            cost_estimate=cost(1e9, 3e6),
-            name="prefix",
-        )(message, own, total)
-        distance *= 2
+def entering_state(message):
+    ep, _, half_cols = message.shape
+    sems = pltpu.SemaphoreType.DMA((ep,))
+    return pl.pallas_call(
+        entering_kernel,
+        in_specs=[pl.BlockSpec(memory_space=pltpu.VMEM)],
+        out_specs=pl.BlockSpec(memory_space=pltpu.VMEM),
+        out_shape=jax.ShapeDtypeStruct((STATE, 2 * half_cols), f32),
+        scratch_shapes=[
+            pltpu.VMEM((ep, 16, half_cols), bf16),
+            pltpu.VMEM((ep, 8, half_cols), f32),
+            pltpu.VMEM((ep, 8, half_cols), f32),
+            sems, sems, sems, sems,
+        ],
+        compiler_params=pltpu.CompilerParams(collective_id=0, has_side_effects=True),
+        cost_estimate=cost(1e10, 3e6),
+        name="entering",
+    )(message)
 
 
 def mixer_kernel(
@@ -272,6 +285,7 @@
     heads = offset.shape[0]
     width = projection.shape[1]
     every = inner + 2 * group
+    ep = lax.axis_size(EP)
     last = jnp.concatenate([a[rows - 8 :] for a in (features, insert, query)], axis=1)
     halo = shifted(last, 1)
     taps = jnp.concatenate([entry_taps, insert_taps, query_taps], axis=1)
@@ -286,7 +300,7 @@
     def across(n):
         return pl.BlockSpec((n, SPAN), lambda i: (0, i))
 
-    xs, bs, cs, row, state, total, message = pl.pallas_call(
+    xs, bs, cs, row, message = pl.pallas_call(
         states_kernel,
         grid=(steps,),
         in_specs=[
@@ -295,18 +309,20 @@
         ],
         out_specs=[
             block(inner), block(group), block(group), across(2 * heads),
-            whole(STATE, inner), whole(1, inner), whole(STATE + 16, inner),
+            whole(ep, 16, inner // 2),
         ],
         out_shape=[
             jax.ShapeDtypeStruct((rows, inner), bf16),
             jax.ShapeDtypeStruct((rows, group), bf16),
             jax.ShapeDtypeStruct((rows, group), bf16),
             jax.ShapeDtypeStruct((2 * heads, rows), f32),
-            jax.ShapeDtypeStruct((STATE, inner), f32),
-            jax.ShapeDtypeStruct((1, inner), f32),
-            jax.ShapeDtypeStruct((STATE + 16, inner), bf16),
-        ],
-        scratch_shapes=[pltpu.VMEM((SPAN + 8, every), f32)],
+            jax.ShapeDtypeStruct((ep, 16, inner // 2), bf16),
+        ],
+        scratch_shapes=[
+            pltpu.VMEM((SPAN + 8, every), f32),
+            pltpu.VMEM((STATE, inner), f32),
+            pltpu.VMEM((1, inner), f32),
+        ],
         compiler_params=params("arbitrary"),
         cost_estimate=cost(8e9, 1e7),
         name="states",
@@ -314,7 +330,7 @@
         features, insert, query, halo, taps, presoftplus.T, spike.T,
         offset.reshape(heads, 1), fading.reshape(heads, 1),
     )
-    entering = entering_state(state, total, message)
+    entering = entering_state(message)
     partial = pl.pallas_call(
         mixer_kernel,
         grid=(steps,),

time: 397 us -> 362 us (0.912)
  starting transfers between devices: 45 us -> 17.4 us
  waiting for transfers between devices: 180 us -> 163 us
  Pallas kernels: 105 us -> 118 us
    ppermute x6 -> x1, starting transfers between devices: 29.3 us -> 1.47 us  [shifted(): lax.ppermute(value, EP, [(i, i + distance) for i in range(lax.axis_size(E...]
    ppermute x6 -> x1, waiting for transfers between devices: 20.4 us -> 0.01 us  [shifted(): lax.ppermute(value, EP, [(i, i + distance) for i in range(lax.axis_size(E...]
    pallas_call x5 -> x1, Pallas kernels: 11.8 us -> 24.5 us  [entering_state(): pl.pallas_call(entering_kernel, in_specs=[pl.BlockSpec(memory_space=pltpu...]
    all_to_all x3, waiting for transfers between devices: 111 us -> 116 us  [exchanged(): return lax.all_to_all(value, EP, split_axis=0, concat_axis=0, tiled=True)]
  transfers between devices with their start and end apart: 14 -> 9, of which waited for: 10 -> 5; matrix products, arithmetic and copies ran while one was open for 2% -> 2% of each run, Pallas kernels for 26% -> 32%
where the time goes in v2:
time: 362 us; the launch traced here: 361 us
  waiting for transfers between devices  163 us (45%)
  Pallas kernels  118 us (33%)
  blocking collectives  36.9 us (10%)
  starting transfers between devices  17.4 us (5%)
  between operations  13.9 us (4%)
  local copies, waits for them, and re-layouts  5.65 us (2%)
  other arithmetic  5.22 us (1%)
    all_to_all x3, waiting for transfers between devices, exchanged(): return lax.all_to_all(value, EP, split_axis=0, concat_axis=0, tiled=True)  116 us
    all_to_all x1, blocking collectives, exchanged(): return lax.all_to_all(value, EP, split_axis=0, concat_axis=0, tiled=True)  36.9 us
    all_gather x1, waiting for transfers between devices, experts_half(): lax.all_gather(first_in[:, :LATE], 'tp', axis=0, tiled=True)  33.5 us
    pallas_call x3, Pallas kernels, expert(): pl.pallas_call(expert_kernel, grid=(rows // ROW_TILE,), in_specs=[pl.Bloc...  31.8 us
    pallas_call x1, Pallas kernels, entering_state(): pl.pallas_call(entering_kernel, in_specs=[pl.BlockSpec(memory_space=pltpu...  24.5 us
    pallas_call x1, Pallas kernels, mixer_half(): pl.pallas_call(mixer_kernel, grid=(steps,), in_specs=[block(inner), block...  24.5 us
    pallas_call x1, Pallas kernels, mixer_half(): pl.pallas_call(states_kernel, grid=(steps,), in_specs=[block(inner), bloc...  15.8 us
    all_to_all x3, starting transfers between devices, exchanged(): return lax.all_to_all(value, EP, split_axis=0, concat_axis=0, tiled=True)  15.7 us
  transfers between devices with their start and end apart: 9, of which 5 were waited for; matrix products, arithmetic and copies ran while one was open for 2% of the time, Pallas kernels for 32%

profile of v2, /device:TPU:0, one launch (start us, length us, event | category | flops | bytes accessed | tf_op | source)
XLA Modules:
  0.0 360.6 jit_solution(4758519695646029388)
XLA Ops:
  7.2 0.0 all-gather.5.cloned.1.call-start
  7.2 3.6 %route.1 = (bf16[128,2176]{1,0:T(8,128)(2,1)}, bf16[512,2048]{1,0:T(8,128)(2,1)}) custom-call(bf16[128,2048]{1,0:T(8,128)(2,1)} %x_ref.3, f32[1,2048]{1,0:T(1,128)} %bitcast.30, s32[4,128]{1,0:T(4,128)} %bitcast.32, f32[4,128]{1,0:T(4,128)} %bitcast.33), custom_call_target="tpu_custom_call" | custom-call | flops 1000000000 | bytes 3000000 | tf_op jit(solution)/shard_map/route/pallas_call | solution.py:482
  10.8 0.0 all-gather.5.cloned.1.call-update
  10.8 0.0 all-gather.3.cloned.1.call-start
  10.9 36.9 %all_to_all.20 = bf16[32,16,2048]{2,1,0:T(8,128)(2,1)S(1)} all-to-all(bf16[32,16,2048]{2,1,0:T(8,128)(2,1)} %bitcast.24), channel_id=1, replica_groups=mesh['ep_0'=4,'ep_1'=4,'ep_2'=2,'tp'=4] {'ep_0','ep_1','ep_2'}, dimensions={0} | all-to-all | bytes 4194304 | tf_op jit(solution)/shard_map/all_to_all | solution.py:474
  47.8 1.5 fusion.7
  49.3 0.0 all-gather.3.cloned.1.call-update
  49.3 0.6 and_select_fusion.apart_ref
  49.9 0.0 all-gather.5.cloned.1.call-done.table_ref
  49.9 7.5 %second.1 = bf16[1280,2048]{1,0:T(8,128)(2,1)} custom-call(bf16[512,2176]{1,0:T(8,128)(2,1)} %all-gather.5.cloned.1.call-done.table_ref, s32[1,512]{1,0:T(1,128)} %and_select_fusion.apart_ref), custom_call_target="tpu_custom_call" | custom-call | flops 3200000000 | bytes 10000000 | tf_op jit(solution)/shard_map/second/pallas_call | solution.py:499
  57.4 4.9 %all-to-all-start.2 = ((bf16[32,40,2048]{2,1,0:T(8,128)(2,1)}), bf16[32,40,2048]{2,1,0:T(8,128)(2,1)}, u32[]{:S(2)}, u32[]{:S(2)}) async-start(bf16[32,40,2048]{2,1,0:T(8,128)(2,1)} %bitcast.20), calls=%async_computation.4 | async-start | bytes 10485760 | tf_op jit(solution)/shard_map/all_to_all | solution.py:474
  62.3 0.0 reduce-scatter.6.cloned.1.call-start
  62.4 33.5 %all-gather.3.cloned.1.call-done = bf16[128,8,2048]{2,1,0:T(8,128)(2,1)} async-done(((bf16[32,8,2048]{2,1,0:T(8,128)(2,1)}), bf16[128,8,2048]{2,1,0:T(8,128)(2,1)}) %all-gather.3.cloned.1.call-update) | async-done | bytes 4194320 | tf_op jit(solution)/shard_map/all_gather | solution.py:495
  95.8 11.9 %expert.3 = bf16[1024,2048]{1,0:T(8,128)(2,1)} custom-call(bf16[1024,2048]{1,0:T(8,128)(2,1)} %bitcast.27, bf16[1,2048,512]{2,1,0:T(8,128)(2,1)} %gate_ref.5, bf16[1,2048,512]{2,1,0:T(8,128)(2,1)} %up_ref.5, bf16[1,512,2048]{2,1,0:T(8,128)(2,1)} %down_ref.5), custom_call_target="tpu_custom_call" | custom-call | flops 6442450944 | bytes 14680064 | tf_op jit(solution)/shard_map/expert/pallas_call | solution.py:429
  107.7 0.0 reduce-scatter.6.cloned.1.call-update
  107.7 20.5 %all-to-all-done.2 = bf16[32,40,2048]{2,1,0:T(8,128)(2,1)} async-done(((bf16[32,40,2048]{2,1,0:T(8,128)(2,1)}), bf16[32,40,2048]{2,1,0:T(8,128)(2,1)}, u32[]{:S(2)}, u32[]{:S(2)}) %all-to-all-start.2) | async-done | bytes 5242912 | tf_op jit(solution)/shard_map/all_to_all | solution.py:474
  128.2 13.9 %expert.5 = bf16[1280,2048]{1,0:T(8,128)(2,1)} custom-call(bf16[1280,2048]{1,0:T(8,128)(2,1)} %bitcast.15.x_ref, bf16[1,2048,512]{2,1,0:T(8,128)(2,1)} %gate_ref.5, bf16[1,2048,512]{2,1,0:T(8,128)(2,1)} %up_ref.5, bf16[1,512,2048]{2,1,0:T(8,128)(2,1)} %down_ref.5), custom_call_target="tpu_custom_call" | custom-call | flops 8053063680 | bytes 16777216 | tf_op jit(solution)/shard_map/expert/pallas_call | solution.py:429
  142.0 4.9 %all-to-all-start.3 = ((bf16[32,40,2048]{2,1,0:T(8,128)(2,1)}), bf16[32,40,2048]{2,1,0:T(8,128)(2,1)}, u32[]{:S(2)}, u32[]{:S(2)}) async-start(bf16[32,40,2048]{2,1,0:T(8,128)(2,1)} %bitcast.21), calls=%async_computation.5 | async-start | bytes 10485760 | tf_op jit(solution)/shard_map/all_to_all | solution.py:474
  146.9 0.0 reduce-scatter.8.cloned.1.call-start
  147.0 0.8 add_select_fusion.apart_ref
  147.8 65.0 %all-to-all-done.3 = bf16[32,40,2048]{2,1,0:T(8,128)(2,1)} async-done(((bf16[32,40,2048]{2,1,0:T(8,128)(2,1)}), bf16[32,40,2048]{2,1,0:T(8,128)(2,1)}, u32[]{:S(2)}, u32[]{:S(2)}) %all-to-all-start.3) | async-done | bytes 5242912 | tf_op jit(solution)/shard_map/all_to_all | solution.py:474
  212.8 0.0 slice-start
  212.8 0.0 slice-start.1
  212.8 0.0 slice-start.2
  212.8 0.0 copy-start.1
  212.8 0.0 copy-start.2
  212.8 0.0 copy-start.3
  212.8 0.0 copy-start.4
  212.9 0.0 copy-start.5
  212.9 0.0 copy-start.6
  212.9 7.4 %gather.1 = bf16[512,2048]{1,0:T(8,128)(2,1)} custom-call(bf16[512,2176]{1,0:T(8,128)(2,1)} %all-gather.5.cloned.1.call-done.table_ref, s32[512,1]{1,0:T(8,128)} %add_select_fusion.apart_ref, bf16[1280,2048]{1,0:T(8,128)(2,1)} %bitcast.17.back_ref), custom_call_target="tpu_custom_call" | custom-call | flops 3200000000 | bytes 10000000 | tf_op jit(solution)/shard_map/gather/pallas_call | solution.py:525
  220.3 0.0 reduce-scatter.8.cloned.1.call-update
  220.3 0.0 reduce-scatter.4.cloned.1.call-start
  220.3 0.0 slice-done
  220.4 0.0 slice-done.1
  220.4 0.0 slice-done.2
  220.4 1.5 collective-permute-start
  221.9 0.0 copy-done.1
  221.9 0.0 copy-done.2
  221.9 0.0 copy-done.3
  221.9 0.6 pad_maximum_fusion.2.taps_ref
  222.5 0.0 copy-done.4
  222.5 0.7 copy.25.off_ref
  223.2 0.0 copy-done.5
  223.2 0.7 copy.26.fade_ref
  223.9 0.0 copy-done.6
  223.9 0.1 broadcast_in_dim.3
  223.9 0.7 reshape_reshape.3.skip_ref
  224.6 0.0 collective-permute-done.halo_ref
  224.6 0.0 copy-start.7
  224.6 0.6 copy-done.7
  225.2 15.8 %states.1 = (bf16[1536,1024]{1,0:T(8,128)(2,1)}, bf16[1536,256]{1,0:T(8,128)(2,1)}, bf16[1536,256]{1,0:T(8,128)(2,1)}, f32[32,1536]{1,0:T(8,128)}, bf16[32,16,512]{2,1,0:T(8,128)(2,1)}) custom-call(bf16[1536,1024]{1,0:T(8,128)(2,1)} %x_ref.2, bf16[1536,256]{1,0:T(8,128)(2,1)} %b_ref.1, bf16[1536,256]{1,0:T(8,128)(2,1)} %c_ref.1, bf16[8,1536]{1,0:T(8,128)(2,1)} %copy-done.7, ...), custom_call_target="tpu_custom_call" | custom-call | flops 8000000000 | bytes 10000000 | tf_op jit(solution)/shard_map/states/pallas_call | solution.py:303
  241.0 24.5 %entering.1.enter_ref = f32[128,1024]{1,0:T(8,128)} custom-call(bf16[32,16,512]{2,1,0:T(8,128)(2,1)} %get-tuple-element.13.msg_ref), custom_call_target="tpu_custom_call" | custom-call | flops 10000000000 | bytes 3000000 | tf_op jit(solution)/shard_map/entering/pallas_call | solution.py:203
  265.5 24.5 %mixer.1 = bf16[1536,2048]{1,0:T(8,128)(2,1)} custom-call(bf16[1536,1024]{1,0:T(8,128)(2,1)} %get-tuple-element.9.xs_ref, bf16[1536,256]{1,0:T(8,128)(2,1)} %get-tuple-element.10.bs_ref, bf16[1536,256]{1,0:T(8,128)(2,1)} %get-tuple-element.11.cs_ref, bf16[1536,1024]{1,0:T(8,128)(2,1)} %z_ref.1, f32[32,1536]{1,0:T(8,128)} %get-tuple-element.12.row_ref, ...), custom_call_target="tpu_custom_call" | custom-call | flops 20000000000 | bytes 20000000 | tf_op jit(solution)/shard_map/mixer/pallas_call | solution.py:334
  290.0 0.0 reduce-scatter.4.cloned.1.call-update
  290.0 6.1 %expert.4 = bf16[256,2048]{1,0:T(8,128)(2,1)} custom-call(bf16[256,2048]{1,0:T(8,128)(2,1)} %get-tuple-element.17.x_ref, bf16[1,2048,512]{2,1,0:T(8,128)(2,1)} %gate_ref.5, bf16[1,2048,512]{2,1,0:T(8,128)(2,1)} %up_ref.5, bf16[1,512,2048]{2,1,0:T(8,128)(2,1)} %down_ref.5), custom_call_target="tpu_custom_call" | custom-call | flops 1610612736 | bytes 8388608 | tf_op jit(solution)/shard_map/expert/pallas_call | solution.py:429
  296.1 0.0 reduce-scatter.6.cloned.1.call-done
  296.1 3.2 pad_maximum_fusion
  299.3 6.0 %all-to-all-start.1 = ((bf16[32,16,2048]{2,1,0:T(8,128)(2,1)}), bf16[32,16,2048]{2,1,0:T(8,128)(2,1)S(1)}, u32[]{:S(2)}, u32[]{:S(2)}) async-start(bf16[32,16,2048]{2,1,0:T(8,128)(2,1)} %pad_maximum_fusion), calls=%async_computation.3 | async-start | bytes 4194304 | tf_op jit(solution)/shard_map/all_to_all | solution.py:474
  305.3 0.0 reduce-scatter.8.cloned.1.call-done.sum_ref
  305.3 30.0 %all-to-all-done.1 = bf16[32,16,2048]{2,1,0:T(8,128)(2,1)S(1)} async-done(((bf16[32,16,2048]{2,1,0:T(8,128)(2,1)}), bf16[32,16,2048]{2,1,0:T(8,128)(2,1)S(1)}, u32[]{:S(2)}, u32[]{:S(2)}) %all-to-all-start.1) | async-done | bytes 2097184 | tf_op jit(solution)/shard_map/all_to_all | solution.py:474
  335.4 1.4 copy-done
  336.7 3.1 final.1
  339.9 14.2 %reduce-scatter.4.cloned.1.call-done = bf16[384,2048]{1,0:T(8,128)(2,1)} async-done(((bf16[1536,2048]{1,0:T(8,128)(2,1)}), bf16[384,2048]{1,0:T(8,128)(2,1)}) %reduce-scatter.4.cloned.1.call-update) | async-done | bytes 1572880 | tf_op jit(solution)/shard_map/reduce_scatter | solution.py:355
  (2 shorter events, 0.0 us)
Async XLA Ops:
  7.2 42.8 %all-gather.5.cloned.1.call-start = ((), (), s32[]{:S(2)}) async-start(), calls=%async_computation.10 | async-start | bytes 2785280 | tf_op jit(solution)/shard_map/all_gather | solution.py:493
  10.8 85.0 %all-gather.3.cloned.1.call-start = ((), (), s32[]{:S(2)}) async-start(), calls=%async_computation.8 | async-start | bytes 5242880 | tf_op jit(solution)/shard_map/all_gather | solution.py:495
  57.4 70.8 %all-to-all-start.2 = ((bf16[32,40,2048]{2,1,0:T(8,128)(2,1)}), bf16[32,40,2048]{2,1,0:T(8,128)(2,1)}, u32[]{:S(2)}, u32[]{:S(2)}) async-start(bf16[32,40,2048]{2,1,0:T(8,128)(2,1)} %bitcast.20), calls=%async_computation.4 | async-start | bytes 10485760 | tf_op jit(solution)/shard_map/all_to_all | solution.py:474
  62.3 233.8 %reduce-scatter.6.cloned.1.call-start = ((), (), s32[]{:S(2)}) async-start(), calls=%async_computation.9 | async-start | bytes 5242880 | tf_op jit(solution)/shard_map/reduce_scatter | solution.py:516
  142.0 70.8 %all-to-all-start.3 = ((bf16[32,40,2048]{2,1,0:T(8,128)(2,1)}), bf16[32,40,2048]{2,1,0:T(8,128)(2,1)}, u32[]{:S(2)}, u32[]{:S(2)}) async-start(bf16[32,40,2048]{2,1,0:T(8,128)(2,1)} %bitcast.21), calls=%async_computation.5 | async-start | bytes 10485760 | tf_op jit(solution)/shard_map/all_to_all | solution.py:474
  146.9 158.4 %reduce-scatter.8.cloned.1.call-start = ((), (), s32[]{:S(2)}) async-start(), calls=%async_computation.11 | async-start | bytes 2621440 | tf_op jit(solution)/shard_map/reduce_scatter | solution.py:540
  212.8 7.5 %slice-start = ((bf16[1536,1024]{1,0:T(8,128)(2,1)}), bf16[8,1024]{1,0:T(8,128)(2,1)S(1)}, s32[]{:S(2)}) async-start(bf16[1536,1024]{1,0:T(8,128)(2,1)} %x_ref.2), calls=%async_computation.12 | async-start | bytes 32768 | tf_op jit(solution)/shard_map/slice | solution.py:289
  212.8 7.5 %slice-start.1 = ((bf16[1536,256]{1,0:T(8,128)(2,1)}), bf16[8,256]{1,0:T(8,128)(2,1)S(1)}, s32[]{:S(2)}) async-start(bf16[1536,256]{1,0:T(8,128)(2,1)} %b_ref.1), calls=%async_computation.13 | async-start | bytes 8192 | tf_op jit(solution)/shard_map/slice | solution.py:289
  212.8 7.6 %slice-start.2 = ((bf16[1536,256]{1,0:T(8,128)(2,1)}), bf16[8,256]{1,0:T(8,128)(2,1)S(1)}, s32[]{:S(2)}) async-start(bf16[1536,256]{1,0:T(8,128)(2,1)} %c_ref.1), calls=%async_computation.14 | async-start | bytes 8192 | tf_op jit(solution)/shard_map/slice | solution.py:289
  212.8 9.1 %copy-start.1 = (bf16[4,1024]{1,0:T(4,128)(2,1)S(1)}, bf16[4,1024]{1,0:T(4,128)(2,1)}, u32[]{:S(2)}) copy-start(bf16[4,1024]{1,0:T(4,128)(2,1)} %param.26) | copy-start | bytes 24580
  212.8 9.1 %copy-start.2 = (bf16[4,256]{1,0:T(4,128)(2,1)S(1)}, bf16[4,256]{1,0:T(4,128)(2,1)}, u32[]{:S(2)}) copy-start(bf16[4,256]{1,0:T(4,128)(2,1)} %param.28) | copy-start | bytes 6148
  212.8 9.1 %copy-start.3 = (bf16[4,256]{1,0:T(4,128)(2,1)S(1)}, bf16[4,256]{1,0:T(4,128)(2,1)}, u32[]{:S(2)}) copy-start(bf16[4,256]{1,0:T(4,128)(2,1)} %param.27) | copy-start | bytes 6148
  212.8 9.7 %copy-start.4 = (f32[16]{0:T(128)S(1)}, f32[16]{0:T(128)}, u32[]{:S(2)}) copy-start(f32[16]{0:T(128)} %param.29) | copy-start | bytes 196
  212.9 10.3 %copy-start.5 = (f32[16]{0:T(128)S(1)}, f32[16]{0:T(128)}, u32[]{:S(2)}) copy-start(f32[16]{0:T(128)} %param.30) | copy-start | bytes 196
  212.9 11.0 %copy-start.6 = (f32[16]{0:T(128)S(1)}, f32[16]{0:T(128)}, u32[]{:S(2)}) copy-start(f32[16]{0:T(128)} %param.31) | copy-start | bytes 196
  220.3 133.8 %reduce-scatter.4.cloned.1.call-start = ((), (), s32[]{:S(2)}) async-start(), calls=%async_computation.7 | async-start | bytes 7864320 | tf_op jit(solution)/shard_map/reduce_scatter | solution.py:355
  220.4 4.2 %collective-permute-start = (bf16[8,1536]{1,0:T(8,128)(2,1)S(1)}, bf16[8,1536]{1,0:T(8,128)(2,1)S(1)}, u32[]{:S(2)}, u32[]{:S(2)}) collective-permute-start(bf16[8,1536]{1,0:T(8,128)(2,1)S(1)} %pad_maximum_fusion.1), channel_id=1, source_target_pairs={{0,4},{4,8},{8,12},{12,16},{16,20},{20,24},{24,28},{28,32},{32,36}... | collective-permute-start | bytes 73736 | tf_op jit(solution)/shard_map/ppermute | solution.py:197
  224.6 0.6 copy-start.7
  299.3 36.0 %all-to-all-start.1 = ((bf16[32,16,2048]{2,1,0:T(8,128)(2,1)}), bf16[32,16,2048]{2,1,0:T(8,128)(2,1)S(1)}, u32[]{:S(2)}, u32[]{:S(2)}) async-start(bf16[32,16,2048]{2,1,0:T(8,128)(2,1)} %pad_maximum_fusion), calls=%async_computation.3 | async-start | bytes 4194304 | tf_op jit(solution)/shard_map/all_to_all | solution.py:474
  335.4 1.4 copy-start
Sparse Core Ops, SparseCore 0:
  11.0 34.3 all-gather.4
  49.4 46.3 all-gather.2
  107.8 47.1 reduce-scatter.5
  220.4 26.2 reduce-scatter.7
  290.1 63.8 reduce-scatter.3

commit v3 on v2

--- a/solution.py
+++ b/solution.py
@@ -175,7 +175,7 @@
 
     running = jnp.zeros((8, half_cols), f32)
     for i in range(ep):
-        before[i] = running
+        before[i] = running.astype(bf16)
         block = came[i].astype(f32)
         running = running * jnp.exp2(block[8:9] + block[9:10] + block[10:11]) + block[0:8]
 
@@ -190,7 +190,7 @@
         returned(k).wait()
 
     for e in range(ep):
-        out_ref[8 * (e // 2) : 8 * (e // 2) + 8, e % 2 * half_cols : (e % 2 + 1) * half_cols] = back[e]
+        out_ref[8 * (e // 2) : 8 * (e // 2) + 8, e % 2 * half_cols : (e % 2 + 1) * half_cols] = back[e].astype(f32)
 
 
 def shifted(value, distance):
@@ -207,8 +207,8 @@
         out_shape=jax.ShapeDtypeStruct((STATE, 2 * half_cols), f32),
         scratch_shapes=[
             pltpu.VMEM((ep, 16, half_cols), bf16),
-            pltpu.VMEM((ep, 8, half_cols), f32),
-            pltpu.VMEM((ep, 8, half_cols), f32),
+            pltpu.VMEM((ep, 8, half_cols), bf16),
+            pltpu.VMEM((ep, 8, half_cols), bf16),
             sems, sems, sems, sems,
         ],
         compiler_params=pltpu.CompilerParams(collective_id=0, has_side_effects=True),
@@ -443,31 +443,195 @@
     )(rows_in, gate, up, down)
 
 
-def gather_kernel(table_ref, apart_ref, back_ref, out_ref, pick, *, experts):
-    rows = back_ref.shape[0]
-
-    @pl.when(pl.program_id(0) == 0)
-    def _():
-        chosen = expert_of(rows, 0, SECOND, experts)
-        table = table_ref[...]
+def joint_kernel(
+    rows_hbm, first_ref, tags_ref, gate_hbm, up_hbm, down_hbm, out_ref,
+    rows, gate, up, down, res, back, first_back, pick, pick_first, part, shares,
+    load_sem, weight_sem, send_sem, recv_sem, first_send, first_recv, part_send, part_recv,
+):
+    ep, per, width = res.shape
+    experts = ep
+    tokens = out_ref.shape[0]
+    blocks = tags_ref.shape[0] // tokens
+    col_tile = part.shape[3]
+    z, y, core = lax.axis_index("ep_0"), lax.axis_index("ep_1"), lax.axis_index("ep_2")
+    tp = lax.axis_index("tp")
+    me = (z * 4 + y) * 2 + core
+    mesh_ids = pl.DeviceIdType.MESH
+
+    def place(k):
+        return (z + k // 2) % 4, (y + k // 8 + k // 2) % 4, (core + k) % 2
+
+    def index(k):
+        a, b, c = place(k)
+        return (a * 4 + b) * 2 + c
+
+    def device(k):
+        a, b, c = place(k)
+        return {"ep_0": a, "ep_1": b, "ep_2": c}
+
+    def load(k):
+        return pltpu.make_async_copy(rows_hbm.at[index(k)], rows.at[k], load_sem.at[k])
+
+    def weights():
+        return [
+            pltpu.make_async_copy(src, dst, weight_sem.at[n])
+            for n, (src, dst) in enumerate(((gate_hbm, gate), (up_hbm, up), (down_hbm, down)))
+        ]
+
+    def give_back(k):
+        return pltpu.make_async_remote_copy(
+            src_ref=res.at[k], dst_ref=back.at[me], send_sem=send_sem.at[k], recv_sem=recv_sem.at[k],
+            device_id=device(k), device_id_type=mesh_ids,
+        )
+
+    def give_first(k):
+        return pltpu.make_async_remote_copy(
+            src_ref=first_ref.at[index(k)], dst_ref=first_back.at[me],
+            send_sem=first_send.at[k], recv_sem=first_recv.at[k],
+            device_id=device(k), device_id_type=mesh_ids,
+        )
+
+    def give_part(t, r):
+        return pltpu.make_async_remote_copy(
+            src_ref=part.at[t, r], dst_ref=shares.at[t, r],
+            send_sem=part_send.at[t, r], recv_sem=part_recv.at[t, r],
+            device_id={"tp": (tp + r) % blocks}, device_id_type=mesh_ids,
+        )
+
+    for w in weights():
+        w.start()
+
+    @pl.loop(0, ep)
+    def _(k):
+        load(k).start()
+
+    barrier = pltpu.get_barrier_semaphore()
+
+    @pl.loop(1, ep)
+    def _(k):
+        pl.semaphore_signal(barrier, inc=1, device_id=device(k), device_id_type=mesh_ids)
+
+    for r in range(1, blocks):
+        pl.semaphore_signal(
+            barrier, inc=1, device_id={"tp": (tp + r) % blocks}, device_id_type=mesh_ids
+        )
+    pl.semaphore_wait(barrier, ep - 1 + blocks - 1)
+
+    for w in weights():
+        w.wait()
+
+    group = 8
+
+    @pl.loop(0, ep // group)
+    def _(c):
+        @pl.loop(0, group)
+        def _(j):
+            load(c * group + j).wait()
+
+        x = rows[pl.ds(c * group, group)].reshape(group * per, width)
+        g = jnp.minimum(mm(x, gate[...]), clamp_top)
+        u = jnp.clip(mm(x, up[...]), -clamp_top, clamp_top) + 1.0
+        act = (g * (0.5 + 0.5 * jnp.tanh((0.5 * sigmoid_sharp) * g)) * u).astype(bf16)
+        res[pl.ds(c * group, group)] = mm(act, down[...]).astype(bf16).reshape(group, per, width)
+
+        @pl.loop(0, group)
+        def _(j):
+            @pl.when(c * group + j > 0)
+            def _():
+                give_back(c * group + j).start()
+
+    @pl.loop(1, ep)
+    def _(k):
+        give_first(k).start()
+
+    back[me] = res[0]
+    first_back[me] = first_ref[me]
+
+    count = experts * per
+    chosen = expert_of(count, 0, per, experts)
+    block, wanted = second_slot(lax.broadcasted_iota(jnp.int32, (1, count), 1) % per)
+    for r in range(blocks):
+        q = (tp + r) % blocks
+        table = tags_ref[pl.ds(pl.multiple_of(q * tokens, tokens), tokens), :]
         slot = mm_last(table[:, 0:experts], chosen)
         weight = mm_last(table[:, experts : 2 * experts], chosen)
-        block, wanted = second_slot(lax.broadcasted_iota(jnp.int32, (1, rows), 1) % SECOND)
-        hit = (slot == wanted.astype(f32)) & (apart_ref[...] == block)
-        pick[...] = jnp.where(hit, weight, 0.0).astype(bf16)
-
-    out_ref[...] = mm(pick[...], back_ref[...]).astype(bf16)
-
-
-def final_kernel(table_ref, back_ref, sum_ref, out_ref, *, experts):
-    rows = back_ref.shape[0]
-    table = table_ref[...]
-    chosen = expert_of(rows, 0, FIRST, experts)
-    slot = mm_last(table[:, 0:experts], chosen)
-    weight = mm_last(table[:, experts : 2 * experts], chosen)
-    at = lax.broadcasted_iota(jnp.int32, (1, rows), 1) % FIRST
-    own = mm(jnp.where(slot == at.astype(f32), weight, 0.0).astype(bf16), back_ref[...])
-    out_ref[...] = (own + sum_ref[...].astype(f32)).astype(bf16)
+        hit = (slot == wanted.astype(f32)) & (block == r)
+        pick[r * tokens : (r + 1) * tokens, :] = jnp.where(hit, weight, 0.0).astype(bf16)
+    own = tags_ref[pl.ds(pl.multiple_of(tp * tokens, tokens), tokens), :]
+    chosen = expert_of(experts * FIRST, 0, FIRST, experts)
+    slot = mm_last(own[:, 0:experts], chosen)
+    weight = mm_last(own[:, experts : 2 * experts], chosen)
+    at = lax.broadcasted_iota(jnp.int32, (1, experts * FIRST), 1) % FIRST
+    pick_first[...] = jnp.where(slot == at.astype(f32), weight, 0.0).astype(bf16)
+
+    @pl.loop(1, ep)
+    def _(k):
+        give_back(k).wait_recv()
+
+    for t in range(width // col_tile):
+        cols = slice(t * col_tile, (t + 1) * col_tile)
+        got = mm(pick[...], back[:, :, cols].reshape(count, col_tile)).astype(bf16)
+        part[t] = got.reshape(blocks, tokens, col_tile)
+        for r in range(1, blocks):
+            give_part(t, r).start()
+
+    @pl.loop(1, ep)
+    def _(k):
+        give_first(k).wait_recv()
+
+    for t in range(width // col_tile):
+        cols = slice(t * col_tile, (t + 1) * col_tile)
+        total = mm(pick_first[...], first_back[:, :, cols].reshape(experts * FIRST, col_tile))
+        total = total + part[t, 0].astype(f32)
+        for r in range(1, blocks):
+            give_part(t, r).wait_recv()
+            total = total + shares[t, r].astype(f32)
+        out_ref[:, cols] = total.astype(bf16)
+
+    @pl.loop(1, ep)
+    def _(k):
+        give_back(k).wait_send()
+        give_first(k).wait_send()
+
+    for t in range(width // col_tile):
+        for r in range(1, blocks):
+            give_part(t, r).wait_send()
+
+
+def joint(second_in, first_res, tags, gate, up, down, tokens):
+    ep, per, width = second_in.shape
+    hidden = gate.shape[1]
+    blocks = tags.shape[0] // tokens
+    tiles = width // 512
+    any_ref = pl.BlockSpec(memory_space=pl.ANY)
+    vmem = pl.BlockSpec(memory_space=pltpu.VMEM)
+    dma = pltpu.SemaphoreType.DMA
+    return pl.pallas_call(
+        joint_kernel,
+        in_specs=[any_ref, vmem, vmem, any_ref, any_ref, any_ref],
+        out_specs=vmem,
+        out_shape=jax.ShapeDtypeStruct((tokens, width), bf16),
+        scratch_shapes=[
+            pltpu.VMEM((ep, per, width), bf16),
+            pltpu.VMEM((width, hidden), bf16),
+            pltpu.VMEM((width, hidden), bf16),
+            pltpu.VMEM((hidden, width), bf16),
+            pltpu.VMEM((ep, per, width), bf16),
+            pltpu.VMEM((ep, per, width), bf16),
+            pltpu.VMEM((ep, FIRST, width), bf16),
+            pltpu.VMEM((blocks * tokens, ep * per), bf16),
+            pltpu.VMEM((tokens, ep * FIRST), bf16),
+            pltpu.VMEM((tiles, blocks, tokens, 512), bf16),
+            pltpu.VMEM((tiles, blocks, tokens, 512), bf16),
+            dma((ep,)), dma((3,)), dma((ep,)), dma((ep,)), dma((ep,)), dma((ep,)),
+            dma((tiles, blocks)), dma((tiles, blocks)),
+        ],
+        compiler_params=pltpu.CompilerParams(
+            collective_id=1, has_side_effects=True, vmem_limit_bytes=60 * 1024 * 1024
+        ),
+        cost_estimate=cost(4e10, 3e7),
+        name="joint",
+    )(second_in, first_res, tags, gate, up, down)
 
 
 def exchanged(value):
@@ -516,42 +680,8 @@
     late_sum = lax.psum_scatter(
         late_part.reshape(blocks * experts, LATE, width), "tp", scatter_dimension=0, tiled=True
     )
-    second_part = expert(second_in.reshape(count, width), gate, up, down)
-    second_back = exchanged(second_part.reshape(experts, SECOND, width))
-    first_back = exchanged(
-        jnp.concatenate([late_sum, own_part.reshape(experts, FIRST - LATE, width)], axis=1)
-    )
-    col_tile = 512
-    second_mix = pl.pallas_call(
-        functools.partial(gather_kernel, experts=experts),
-        grid=(width // col_tile,),
-        in_specs=[
-            pl.BlockSpec((blocks * tokens, 128), lambda i: (0, width // 128)),
-            pl.BlockSpec((blocks * tokens, 1), lambda i: (0, 0)),
-            pl.BlockSpec((count, col_tile), lambda i: (0, i)),
-        ],
-        out_specs=pl.BlockSpec((blocks * tokens, col_tile), lambda i: (0, i)),
-        out_shape=jax.ShapeDtypeStruct((blocks * tokens, width), bf16),
-        scratch_shapes=[pltpu.VMEM((blocks * tokens, count), bf16)],
-        compiler_params=params("arbitrary"),
-        cost_estimate=cost(3.2e9, 1e7),
-        name="gather",
-    )(table, apart.reshape(-1, 1), second_back.reshape(count, width))
-    second_sum = lax.psum_scatter(second_mix, "tp", scatter_dimension=0, tiled=True)
-    return pl.pallas_call(
-        functools.partial(final_kernel, experts=experts),
-        grid=(1,),
-        in_specs=[
-            pl.BlockSpec((tokens, 128), lambda i: (0, width // 128)),
-            pl.BlockSpec((experts * FIRST, width), lambda i: (0, 0)),
-            pl.BlockSpec((tokens, width), lambda i: (0, 0)),
-        ],
-        out_specs=pl.BlockSpec((tokens, width), lambda i: (0, 0)),
-        out_shape=jax.ShapeDtypeStruct((tokens, width), bf16),
-        compiler_params=params("arbitrary"),
-        cost_estimate=cost(2e8, 2e6),
-        name="final",
-    )(own, first_back.reshape(experts * FIRST, width), second_sum)
+    first_res = jnp.concatenate([late_sum, own_part.reshape(experts, FIRST - LATE, width)], axis=1)
+    return joint(second_in, first_res, table[:, width:], gate[0], up[0], down[0], tokens)
 
 
 def body(*args):

time: 362 us -> 384 us (1.061); the launches traced: 361 us -> 377 us
  Pallas kernels: 118 us -> 205 us
  waiting for transfers between devices: 163 us -> 101 us
  starting transfers between devices: 17.4 us -> 7.26 us
    pallas_call x2 -> x1, Pallas kernels: 10.5 us -> 111 us  [joint(): pl.pallas_call(joint_kernel, in_specs=[any_ref, vmem, vmem, any_ref, any_...]
    all_to_all x3 -> x1, waiting for transfers between devices: 116 us -> 54.9 us  [exchanged(): return lax.all_to_all(value, EP, split_axis=0, concat_axis=0, tiled=True)]
    reduce_scatter x1, waiting for transfers between devices: 14.2 us -> 0.02 us  [mixer_half(): return lax.psum_scatter(partial, 'tp', scatter_dimension=0, tiled=True)]
    pallas_call x3 -> x2, Pallas kernels: 31.8 us -> 17.9 us  [expert(): pl.pallas_call(expert_kernel, grid=(rows // ROW_TILE,), in_specs=[pl.Bloc...]
    all_gather x1, waiting for transfers between devices: 33.5 us -> 45.3 us  [experts_half(): lax.all_gather(first_in[:, :LATE], 'tp', axis=0, tiled=True)]
    all_to_all x3 -> x1, starting transfers between devices: 15.7 us -> 5.52 us  [exchanged(): return lax.all_to_all(value, EP, split_axis=0, concat_axis=0, tiled=True)]
  transfers between devices with their start and end apart: 9 -> 6, of which waited for: 5 -> 2; matrix products, arithmetic and copies ran while one was open for 2% -> 2% of each run, Pallas kernels for 32% -> 54%
where the time goes in v3:
time: 384 us; the launch traced here: 377 us
  Pallas kernels  205 us (53%)
  waiting for transfers between devices  101 us (26%)
  blocking collectives  36.9 us (10%)
  between operations  13.9 us (4%)
  local copies, waits for them, and re-layouts  8.21 us (2%)
  starting transfers between devices  7.26 us (2%)
  other arithmetic  4.33 us (1%)
    pallas_call x1, Pallas kernels, joint(): pl.pallas_call(joint_kernel, in_specs=[any_ref, vmem, vmem, any_ref, any_...  111 us
    all_to_all x1, waiting for transfers between devices, exchanged(): return lax.all_to_all(value, EP, split_axis=0, concat_axis=0, tiled=True)  54.9 us
    all_gather x1, waiting for transfers between devices, experts_half(): lax.all_gather(first_in[:, :LATE], 'tp', axis=0, tiled=True)  45.3 us
    all_to_all x1, blocking collectives, exchanged(): return lax.all_to_all(value, EP, split_axis=0, concat_axis=0, tiled=True)  36.9 us
    pallas_call x1, Pallas kernels, entering_state(): pl.pallas_call(entering_kernel, in_specs=[pl.BlockSpec(memory_space=pltpu...  25 us
    pallas_call x1, Pallas kernels, mixer_half(): pl.pallas_call(mixer_kernel, grid=(steps,), in_specs=[block(inner), block...  24.5 us
    pallas_call x2, Pallas kernels, expert(): pl.pallas_call(expert_kernel, grid=(rows // ROW_TILE,), in_specs=[pl.Bloc...  17.9 us
    pallas_call x1, Pallas kernels, mixer_half(): pl.pallas_call(states_kernel, grid=(steps,), in_specs=[block(inner), bloc...  15.7 us
  transfers between devices with their start and end apart: 6, of which 2 were waited for; matrix products, arithmetic and copies ran while one was open for 2% of the time, Pallas kernels for 54%

profile of v3, /device:TPU:0, one launch (start us, length us, event | category | flops | bytes accessed | tf_op | source)
XLA Modules:
  0.0 376.7 jit_solution(16144135373831621166)
XLA Ops:
  7.2 0.0 all-gather.5.cloned.1.call-start
  7.2 3.6 route.1
  10.8 36.9 %all_to_all.10 = bf16[32,16,2048]{2,1,0:T(8,128)(2,1)S(1)} all-to-all(bf16[32,16,2048]{2,1,0:T(8,128)(2,1)} %bitcast.21), channel_id=1, replica_groups=mesh['ep_0'=4,'ep_1'=4,'ep_2'=2,'tp'=4] {'ep_0','ep_1','ep_2'}, dimensions={0} | all-to-all | bytes 4194304 | tf_op jit(solution)/shard_map/all_to_all | solution.py:638
  47.7 1.4 fusion.2
  49.1 0.0 all-gather.5.cloned.1.call-update
  49.2 0.0 all-gather.3.cloned.1.call-start
  49.2 0.7 all-gather.3.cloned.1.call-update
  49.9 0.0 reduce-scatter.5.cloned.1.call-start
  50.0 45.3 %all-gather.5.cloned.1.call-done = bf16[128,8,2048]{2,1,0:T(8,128)(2,1)} async-done(((bf16[32,8,2048]{2,1,0:T(8,128)(2,1)}), bf16[128,8,2048]{2,1,0:T(8,128)(2,1)}) %all-gather.5.cloned.1.call-update) | async-done | bytes 4194320 | tf_op jit(solution)/shard_map/all_gather | solution.py:659
  95.2 11.8 %expert.2 = bf16[1024,2048]{1,0:T(8,128)(2,1)} custom-call(bf16[1024,2048]{1,0:T(8,128)(2,1)} %bitcast.27, bf16[1,2048,512]{2,1,0:T(8,128)(2,1)} %gate_ref.3, bf16[1,2048,512]{2,1,0:T(8,128)(2,1)} %up_ref.3, bf16[1,512,2048]{2,1,0:T(8,128)(2,1)} %down_ref.3), custom_call_target="tpu_custom_call" | custom-call | flops 6442450944 | bytes 14680064 | tf_op jit(solution)/shard_map/expert/pallas_call | solution.py:429
  107.0 0.0 slice-start
  107.0 0.0 slice-start.1
  107.0 0.0 slice-start.2
  107.0 0.0 copy-start
  107.1 0.0 copy-start.1
  107.1 0.0 copy-start.2
  107.1 0.0 copy-start.3
  107.1 0.0 copy-start.4
  107.1 0.0 copy-start.5
  107.1 0.0 reduce-scatter.5.cloned.1.call-update
  107.1 0.0 reduce-scatter.3.cloned.1.call-start
  107.2 0.6 slice-done
  107.8 0.0 slice-done.1
  107.8 0.0 slice-done.2
  107.8 1.6 collective-permute-start
  109.3 0.0 copy-done
  109.4 0.0 copy-done.1
  109.4 0.0 copy-done.2
  109.4 0.6 pad_maximum_fusion.2.taps_ref
  110.0 0.0 copy-done.3
  110.0 0.7 copy.25.off_ref
  110.7 0.0 copy-done.4
  110.7 0.7 copy.26.fade_ref
  111.3 0.0 copy-done.5
  111.3 0.1 broadcast_in_dim.3
  111.4 0.7 reshape_reshape.3.skip_ref
  112.1 0.0 collective-permute-done.halo_ref
  112.1 0.0 copy-start.6
  112.1 0.6 copy-done.6
  112.7 15.7 %states.1 = (bf16[1536,1024]{1,0:T(8,128)(2,1)}, bf16[1536,256]{1,0:T(8,128)(2,1)}, bf16[1536,256]{1,0:T(8,128)(2,1)}, f32[32,1536]{1,0:T(8,128)}, bf16[32,16,512]{2,1,0:T(8,128)(2,1)}) custom-call(bf16[1536,1024]{1,0:T(8,128)(2,1)} %x_ref.2, bf16[1536,256]{1,0:T(8,128)(2,1)} %b_ref.1, bf16[1536,256]{1,0:T(8,128)(2,1)} %c_ref.1, bf16[8,1536]{1,0:T(8,128)(2,1)} %copy-done.6, ...), custom_call_target="tpu_custom_call" | custom-call | flops 8000000000 | bytes 10000000 | tf_op jit(solution)/shard_map/states/pallas_call | solution.py:303
  128.4 25.0 %entering.1.enter_ref = f32[128,1024]{1,0:T(8,128)} custom-call(bf16[32,16,512]{2,1,0:T(8,128)(2,1)} %get-tuple-element.13.msg_ref), custom_call_target="tpu_custom_call" | custom-call | flops 10000000000 | bytes 3000000 | tf_op jit(solution)/shard_map/entering/pallas_call | solution.py:203
  153.4 24.5 %mixer.1 = bf16[1536,2048]{1,0:T(8,128)(2,1)} custom-call(bf16[1536,1024]{1,0:T(8,128)(2,1)} %get-tuple-element.9.xs_ref, bf16[1536,256]{1,0:T(8,128)(2,1)} %get-tuple-element.10.bs_ref, bf16[1536,256]{1,0:T(8,128)(2,1)} %get-tuple-element.11.cs_ref, bf16[1536,1024]{1,0:T(8,128)(2,1)} %z_ref.1, f32[32,1536]{1,0:T(8,128)} %get-tuple-element.12.row_ref, ...), custom_call_target="tpu_custom_call" | custom-call | flops 20000000000 | bytes 20000000 | tf_op jit(solution)/shard_map/mixer/pallas_call | solution.py:334
  177.9 0.0 reduce-scatter.3.cloned.1.call-update
  177.9 0.6 and_select_fusion.apart_ref
  178.5 0.0 all-gather.3.cloned.1.call-done.table_ref
  178.5 7.4 %second.1 = bf16[1280,2048]{1,0:T(8,128)(2,1)} custom-call(bf16[512,2176]{1,0:T(8,128)(2,1)} %all-gather.3.cloned.1.call-done.table_ref, s32[1,512]{1,0:T(1,128)} %and_select_fusion.apart_ref), custom_call_target="tpu_custom_call" | custom-call | flops 3200000000 | bytes 10000000 | tf_op jit(solution)/shard_map/second/pallas_call | solution.py:663
  185.9 5.5 %all-to-all-start = ((bf16[32,40,2048]{2,1,0:T(8,128)(2,1)}), bf16[32,40,2048]{2,1,0:T(8,128)(2,1)}, u32[]{:S(2)}, u32[]{:S(2)}) async-start(bf16[32,40,2048]{2,1,0:T(8,128)(2,1)} %bitcast.18), calls=%async_computation.1 | async-start | bytes 10485760 | tf_op jit(solution)/shard_map/all_to_all | solution.py:638
  191.5 6.1 %expert.3 = bf16[256,2048]{1,0:T(8,128)(2,1)} custom-call(bf16[256,2048]{1,0:T(8,128)(2,1)} %get-tuple-element.17.x_ref, bf16[1,2048,512]{2,1,0:T(8,128)(2,1)} %gate_ref.3, bf16[1,2048,512]{2,1,0:T(8,128)(2,1)} %up_ref.3, bf16[1,512,2048]{2,1,0:T(8,128)(2,1)} %down_ref.3), custom_call_target="tpu_custom_call" | custom-call | flops 1610612736 | bytes 8388608 | tf_op jit(solution)/shard_map/expert/pallas_call | solution.py:429
  197.6 1.6 slice.26.tags_ref
  199.1 0.0 reduce-scatter.5.cloned.1.call-done
  199.1 3.1 pad_maximum_fusion.first_ref
  202.3 54.9 %all-to-all-done.rows_hbm = bf16[32,40,2048]{2,1,0:T(8,128)(2,1)} async-done(((bf16[32,40,2048]{2,1,0:T(8,128)(2,1)}), bf16[32,40,2048]{2,1,0:T(8,128)(2,1)}, u32[]{:S(2)}, u32[]{:S(2)}) %all-to-all-start) | async-done | bytes 5242912 | tf_op jit(solution)/shard_map/all_to_all | solution.py:638
  257.2 111.1 %joint.1 = bf16[128,2048]{1,0:T(8,128)(2,1)} custom-call(bf16[32,40,2048]{2,1,0:T(8,128)(2,1)} %all-to-all-done.rows_hbm, bf16[32,16,2048]{2,1,0:T(8,128)(2,1)} %pad_maximum_fusion.first_ref, bf16[512,128]{1,0:T(8,128)(2,1)} %slice.26.tags_ref, bf16[2048,512]{1,0:T(8,128)(2,1)} %bitcast.22, bf16[2048,512]{1,0:T(8,128)(2,1)} %bitcast.23, ...), custom_call_target="tpu_custom_call" | custom-call | flops 40000000000 | bytes 30000000 | tf_op jit(solution)/shard_map/joint/pallas_call | solution.py:609
  368.3 0.0 reduce-scatter.3.cloned.1.call-done
  368.3 1.9 copy.28
  (1 shorter events, 0.0 us)
Async XLA Ops:
  7.2 88.1 %all-gather.5.cloned.1.call-start = ((), (), s32[]{:S(2)}) async-start(), calls=%async_computation.6 | async-start | bytes 5242880 | tf_op jit(solution)/shard_map/all_gather | solution.py:659
  49.2 129.3 %all-gather.3.cloned.1.call-start = ((), (), s32[]{:S(2)}) async-start(), calls=%async_computation.5 | async-start | bytes 2785280 | tf_op jit(solution)/shard_map/all_gather | solution.py:657
  49.9 149.2 %reduce-scatter.5.cloned.1.call-start = ((), (), s32[]{:S(2)}) async-start(), calls=%async_computation.7 | async-start | bytes 5242880 | tf_op jit(solution)/shard_map/reduce_scatter | solution.py:680
  107.0 0.7 slice-start
  107.0 0.7 slice-start.1
  107.0 0.7 slice-start.2
  107.0 2.3 copy-start
  107.1 2.3 copy-start.1
  107.1 2.3 copy-start.2
  107.1 2.9 copy-start.3
  107.1 3.6 copy-start.4
  107.1 4.2 %copy-start.5 = (f32[16]{0:T(128)S(1)}, f32[16]{0:T(128)}, u32[]{:S(2)}) copy-start(f32[16]{0:T(128)} %param.31) | copy-start | bytes 196
  107.1 261.2 %reduce-scatter.3.cloned.1.call-start = ((), (), s32[]{:S(2)}) async-start(), calls=%async_computation.4 | async-start | bytes 7864320 | tf_op jit(solution)/shard_map/reduce_scatter | solution.py:355
  107.8 4.3 %collective-permute-start = (bf16[8,1536]{1,0:T(8,128)(2,1)S(1)}, bf16[8,1536]{1,0:T(8,128)(2,1)S(1)}, u32[]{:S(2)}, u32[]{:S(2)}) collective-permute-start(bf16[8,1536]{1,0:T(8,128)(2,1)S(1)} %pad_maximum_fusion.1), channel_id=1, source_target_pairs={{0,4},{4,8},{8,12},{12,16},{16,20},{20,24},{24,28},{28,32},{32,36}... | collective-permute-start | bytes 73736 | tf_op jit(solution)/shard_map/ppermute | solution.py:197
  112.1 0.6 copy-start.6
  185.9 71.2 %all-to-all-start = ((bf16[32,40,2048]{2,1,0:T(8,128)(2,1)}), bf16[32,40,2048]{2,1,0:T(8,128)(2,1)}, u32[]{:S(2)}, u32[]{:S(2)}) async-start(bf16[32,40,2048]{2,1,0:T(8,128)(2,1)} %bitcast.18), calls=%async_computation.1 | async-start | bytes 10485760 | tf_op jit(solution)/shard_map/all_to_all | solution.py:638
Sparse Core Ops, SparseCore 0:
  49.3 45.8 all-gather.4
  96.9 32.1 all-gather.2
  131.5 46.9 reduce-scatter.4
  181.3 63.6 reduce-scatter.2

commit v4 on v3

--- a/solution.py
+++ b/solution.py
@@ -444,9 +444,11 @@
 
 
 def joint_kernel(
-    rows_hbm, first_ref, tags_ref, gate_hbm, up_hbm, down_hbm, out_ref,
-    rows, gate, up, down, res, back, first_back, pick, pick_first, part, shares,
-    load_sem, weight_sem, send_sem, recv_sem, first_send, first_recv, part_send, part_recv,
+    rows_hbm, late_hbm, own_ref, tags_ref, gate_hbm, up_hbm, down_hbm, out_ref,
+    rows, gate, up, down, res, back, late_all, late_sum, late_back, own_back,
+    pick, pick_first, part, shares,
+    load_sem, weight_sem, late_load, send_sem, recv_sem, share_send, share_recv,
+    late_send, late_recv, own_send, own_recv, part_send, part_recv,
 ):
     ep, per, width = res.shape
     experts = ep
@@ -484,11 +486,25 @@
             device_id=device(k), device_id_type=mesh_ids,
         )
 
-    def give_first(k):
+    def give_late(k):
         return pltpu.make_async_remote_copy(
-            src_ref=first_ref.at[index(k)], dst_ref=first_back.at[me],
-            send_sem=first_send.at[k], recv_sem=first_recv.at[k],
+            src_ref=late_sum.at[index(k)], dst_ref=late_back.at[me],
+            send_sem=late_send.at[k], recv_sem=late_recv.at[k],
             device_id=device(k), device_id_type=mesh_ids,
+        )
+
+    def give_own(k):
+        return pltpu.make_async_remote_copy(
+            src_ref=own_ref.at[index(k)], dst_ref=own_back.at[me],
+            send_sem=own_send.at[k], recv_sem=own_recv.at[k],
+            device_id=device(k), device_id_type=mesh_ids,
+        )
+
+    def give_share(r):
+        return pltpu.make_async_remote_copy(
+            src_ref=late_hbm.at[(tp + r) % blocks], dst_ref=late_all.at[r],
+            send_sem=share_send.at[r], recv_sem=share_recv.at[r],
+            device_id={"tp": (tp + r) % blocks}, device_id_type=mesh_ids,
         )
 
     def give_part(t, r):
@@ -517,6 +533,11 @@
         )
     pl.semaphore_wait(barrier, ep - 1 + blocks - 1)
 
+    for r in range(1, blocks):
+        give_share(r).start()
+    own_share = pltpu.make_async_copy(late_hbm.at[tp], late_all.at[0], late_load)
+    own_share.start()
+
     for w in weights():
         w.wait()
 
@@ -542,10 +563,10 @@
 
     @pl.loop(1, ep)
     def _(k):
-        give_first(k).start()
+        give_own(k).start()
 
     back[me] = res[0]
-    first_back[me] = first_ref[me]
+    own_back[me] = own_ref[me]
 
     count = experts * per
     chosen = expert_of(count, 0, per, experts)
@@ -558,11 +579,30 @@
         hit = (slot == wanted.astype(f32)) & (block == r)
         pick[r * tokens : (r + 1) * tokens, :] = jnp.where(hit, weight, 0.0).astype(bf16)
     own = tags_ref[pl.ds(pl.multiple_of(tp * tokens, tokens), tokens), :]
-    chosen = expert_of(experts * FIRST, 0, FIRST, experts)
+    chosen = expert_of(experts * LATE, 0, LATE, experts)
     slot = mm_last(own[:, 0:experts], chosen)
     weight = mm_last(own[:, experts : 2 * experts], chosen)
-    at = lax.broadcasted_iota(jnp.int32, (1, experts * FIRST), 1) % FIRST
-    pick_first[...] = jnp.where(slot == at.astype(f32), weight, 0.0).astype(bf16)
+    at = lax.broadcasted_iota(jnp.int32, (1, experts * LATE), 1) % LATE
+    for n in range(FIRST // LATE):
+        hit = slot == (at + n * LATE).astype(f32)
+        pick_first[n] = jnp.where(hit, weight, 0.0).astype(bf16)
+
+    own_share.wait()
+    for r in range(1, blocks):
+        give_share(r).wait_recv()
+
+    @pl.loop(0, ep)
+    def _(k):
+        total = late_all[0, k].astype(f32)
+        for r in range(1, blocks):
+            total = total + late_all[r, k].astype(f32)
+        late_sum[k] = total.astype(bf16)
+
+    @pl.loop(1, ep)
+    def _(k):
+        give_late(k).start()
+
+    late_back[me] = late_sum[me]
 
     @pl.loop(1, ep)
     def _(k):
@@ -577,12 +617,14 @@
 
     @pl.loop(1, ep)
     def _(k):
-        give_first(k).wait_recv()
+        give_own(k).wait_recv()
+        give_late(k).wait_recv()
 
     for t in range(width // col_tile):
         cols = slice(t * col_tile, (t + 1) * col_tile)
-        total = mm(pick_first[...], first_back[:, :, cols].reshape(experts * FIRST, col_tile))
-        total = total + part[t, 0].astype(f32)
+        total = part[t, 0].astype(f32)
+        for n, ref in enumerate((late_back, own_back)):
+            total = total + mm(pick_first[n], ref[:, :, cols].reshape(experts * LATE, col_tile))
         for r in range(1, blocks):
             give_part(t, r).wait_recv()
             total = total + shares[t, r].astype(f32)
@@ -591,14 +633,16 @@
     @pl.loop(1, ep)
     def _(k):
         give_back(k).wait_send()
-        give_first(k).wait_send()
-
-    for t in range(width // col_tile):
-        for r in range(1, blocks):
+        give_own(k).wait_send()
+        give_late(k).wait_send()
+
+    for r in range(1, blocks):
+        give_share(r).wait_send()
+        for t in range(width // col_tile):
             give_part(t, r).wait_send()
 
 
-def joint(second_in, first_res, tags, gate, up, down, tokens):
+def joint(second_in, late_part, own_part, tags, gate, up, down, tokens):
     ep, per, width = second_in.shape
     hidden = gate.shape[1]
     blocks = tags.shape[0] // tokens
@@ -608,7 +652,7 @@
     dma = pltpu.SemaphoreType.DMA
     return pl.pallas_call(
         joint_kernel,
-        in_specs=[any_ref, vmem, vmem, any_ref, any_ref, any_ref],
+        in_specs=[any_ref, any_ref, vmem, vmem, any_ref, any_ref, any_ref],
         out_specs=vmem,
         out_shape=jax.ShapeDtypeStruct((tokens, width), bf16),
         scratch_shapes=[
@@ -618,12 +662,16 @@
             pltpu.VMEM((hidden, width), bf16),
             pltpu.VMEM((ep, per, width), bf16),
             pltpu.VMEM((ep, per, width), bf16),
-            pltpu.VMEM((ep, FIRST, width), bf16),
+            pltpu.VMEM((blocks, ep, LATE, width), bf16),
+            pltpu.VMEM((ep, LATE, width), bf16),
+            pltpu.VMEM((ep, LATE, width), bf16),
+            pltpu.VMEM((ep, LATE, width), bf16),
             pltpu.VMEM((blocks * tokens, ep * per), bf16),
-            pltpu.VMEM((tokens, ep * FIRST), bf16),
+            pltpu.VMEM((FIRST // LATE, tokens, ep * LATE), bf16),
             pltpu.VMEM((tiles, blocks, tokens, 512), bf16),
             pltpu.VMEM((tiles, blocks, tokens, 512), bf16),
-            dma((ep,)), dma((3,)), dma((ep,)), dma((ep,)), dma((ep,)), dma((ep,)),
+            dma((ep,)), dma((3,)), dma, dma((ep,)), dma((ep,)), dma((blocks,)), dma((blocks,)),
+            dma((ep,)), dma((ep,)), dma((ep,)), dma((ep,)),
             dma((tiles, blocks)), dma((tiles, blocks)),
         ],
         compiler_params=pltpu.CompilerParams(
@@ -631,7 +679,7 @@
         ),
         cost_estimate=cost(4e10, 3e7),
         name="joint",
-    )(second_in, first_res, tags, gate, up, down)
+    )(second_in, late_part, own_part, tags, gate, up, down)
 
 
 def exchanged(value):
@@ -677,11 +725,10 @@
 
     late_part = expert(late_rows, gate, up, down)
     own_part = expert(first_in[:, LATE:].reshape(-1, width), gate, up, down)
-    late_sum = lax.psum_scatter(
-        late_part.reshape(blocks * experts, LATE, width), "tp", scatter_dimension=0, tiled=True
+    return joint(
+        second_in, late_part.reshape(blocks, experts, LATE, width),
+        own_part.reshape(experts, FIRST - LATE, width), table[:, width:], gate[0], up[0], down[0], tokens,
     )
-    first_res = jnp.concatenate([late_sum, own_part.reshape(experts, FIRST - LATE, width)], axis=1)
-    return joint(second_in, first_res, table[:, width:], gate[0], up[0], down[0], tokens)
 
 
 def body(*args):

time: 384 us -> 324 us (0.84)
  the two profiles are of different devices: /device:TPU:0 before, /device:TPU:9 now
where the time goes in v4:
time: 324 us; the launch traced here: 323 us
  Pallas kernels  212 us (65%)
  waiting for transfers between devices  43.6 us (13%)
  blocking collectives  36.2 us (11%)
  between operations  13.9 us (4%)
  starting transfers between devices  8.93 us (3%)
  local copies, waits for them, and re-layouts  7.63 us (2%)
    pallas_call x1, Pallas kernels, joint(): pl.pallas_call(joint_kernel, in_specs=[any_ref, any_ref, vmem, vmem, any_...  121 us
    all_to_all x1, waiting for transfers between devices, exchanged(): return lax.all_to_all(value, EP, split_axis=0, concat_axis=0, tiled=True)  43.5 us
    all_to_all x1, blocking collectives, exchanged(): return lax.all_to_all(value, EP, split_axis=0, concat_axis=0, tiled=True)  36.2 us
    pallas_call x1, Pallas kernels, mixer_half(): pl.pallas_call(mixer_kernel, grid=(steps,), in_specs=[block(inner), block...  24.5 us
    pallas_call x1, Pallas kernels, entering_state(): pl.pallas_call(entering_kernel, in_specs=[pl.BlockSpec(memory_space=pltpu...  21.6 us
    pallas_call x2, Pallas kernels, expert(): pl.pallas_call(expert_kernel, grid=(rows // ROW_TILE,), in_specs=[pl.Bloc...  18 us
    pallas_call x1, Pallas kernels, mixer_half(): pl.pallas_call(states_kernel, grid=(steps,), in_specs=[block(inner), bloc...  15.8 us
    pallas_call x1, Pallas kernels, experts_half(): pl.pallas_call(functools.partial(second_kernel, experts=experts), grid=(c...  7.44 us
  transfers between devices with their start and end apart: 5, of which 1 were waited for; matrix products, arithmetic and copies ran while one was open for 2% of the time, Pallas kernels for 64%

profile of v4, /device:TPU:9, one launch (start us, length us, event | category | flops | bytes accessed | tf_op | source)
XLA Modules:
  0.0 323.4 jit_solution(6824287081917885133)
XLA Ops:
  7.2 0.0 all-gather.3.cloned.1.call-start
  7.2 3.6 %route.1 = (bf16[128,2176]{1,0:T(8,128)(2,1)}, bf16[512,2048]{1,0:T(8,128)(2,1)}) custom-call(bf16[128,2048]{1,0:T(8,128)(2,1)} %x_ref.3, f32[1,2048]{1,0:T(1,128)} %bitcast.29, s32[4,128]{1,0:T(4,128)} %bitcast.31, f32[4,128]{1,0:T(4,128)} %bitcast.32), custom_call_target="tpu_custom_call" | custom-call | flops 1000000000 | bytes 3000000 | tf_op jit(solution)/shard_map/route/pallas_call | solution.py:694
  10.8 0.0 all-gather.3.cloned.1.call-update
  10.8 0.0 all-gather.5.cloned.1.call-start
  10.9 36.2 %all_to_all.10 = bf16[32,16,2048]{2,1,0:T(8,128)(2,1)S(1)} all-to-all(bf16[32,16,2048]{2,1,0:T(8,128)(2,1)} %bitcast.19), channel_id=1, replica_groups=mesh['ep_0'=4,'ep_1'=4,'ep_2'=2,'tp'=4] {'ep_0','ep_1','ep_2'}, dimensions={0} | all-to-all | bytes 4194304 | tf_op jit(solution)/shard_map/all_to_all | solution.py:686
  47.1 0.0 slice-start
  47.1 0.0 slice-start.1
  47.1 0.0 slice-start.2
  47.1 0.0 copy-start
  47.1 0.0 copy-start.1
  47.1 0.0 copy-start.2
  47.1 0.0 copy-start.3
  47.2 0.0 copy-start.4
  47.2 0.0 copy-start.5
  47.2 1.4 slice_bitcast_fusion
  48.6 0.0 all-gather.5.cloned.1.call-update
  48.6 0.0 reduce-scatter.2.cloned.1.call-start
  48.7 0.0 slice-done
  48.7 0.0 slice-done.1
  48.7 0.0 slice-done.2
  48.7 2.5 collective-permute-start
  51.2 0.0 copy-done
  51.2 0.0 copy-done.1
  51.2 0.0 copy-done.2
  51.2 0.6 pad_maximum_fusion.1.taps_ref
  51.9 0.0 copy-done.3
  51.9 0.7 copy.25.off_ref
  52.5 0.0 copy-done.4
  52.5 0.7 copy.26.fade_ref
  53.2 0.0 copy-done.5
  53.2 0.1 broadcast_in_dim.3
  53.3 0.7 reshape_reshape.3.skip_ref
  54.0 0.0 collective-permute-done.halo_ref
  54.0 0.0 copy-start.6
  54.0 0.6 copy-done.6
  54.6 15.8 %states.1 = (bf16[1536,1024]{1,0:T(8,128)(2,1)}, bf16[1536,256]{1,0:T(8,128)(2,1)}, bf16[1536,256]{1,0:T(8,128)(2,1)}, f32[32,1536]{1,0:T(8,128)}, bf16[32,16,512]{2,1,0:T(8,128)(2,1)}) custom-call(bf16[1536,1024]{1,0:T(8,128)(2,1)} %x_ref.2, bf16[1536,256]{1,0:T(8,128)(2,1)} %b_ref.1, bf16[1536,256]{1,0:T(8,128)(2,1)} %c_ref.1, bf16[8,1536]{1,0:T(8,128)(2,1)} %copy-done.6, ...), custom_call_target="tpu_custom_call" | custom-call | flops 8000000000 | bytes 10000000 | tf_op jit(solution)/shard_map/states/pallas_call | solution.py:303
  70.4 21.6 %entering.1.enter_ref = f32[128,1024]{1,0:T(8,128)} custom-call(bf16[32,16,512]{2,1,0:T(8,128)(2,1)} %get-tuple-element.13.msg_ref), custom_call_target="tpu_custom_call" | custom-call | flops 10000000000 | bytes 3000000 | tf_op jit(solution)/shard_map/entering/pallas_call | solution.py:203
  92.0 24.5 %mixer.1 = bf16[1536,2048]{1,0:T(8,128)(2,1)} custom-call(bf16[1536,1024]{1,0:T(8,128)(2,1)} %get-tuple-element.9.xs_ref, bf16[1536,256]{1,0:T(8,128)(2,1)} %get-tuple-element.10.bs_ref, bf16[1536,256]{1,0:T(8,128)(2,1)} %get-tuple-element.11.cs_ref, bf16[1536,1024]{1,0:T(8,128)(2,1)} %z_ref.1, f32[32,1536]{1,0:T(8,128)} %get-tuple-element.12.row_ref, ...), custom_call_target="tpu_custom_call" | custom-call | flops 20000000000 | bytes 20000000 | tf_op jit(solution)/shard_map/mixer/pallas_call | solution.py:334
  116.4 0.0 reduce-scatter.2.cloned.1.call-update
  116.5 0.6 and_select_fusion.apart_ref
  117.1 0.0 all-gather.3.cloned.1.call-done.table_ref
  117.1 7.4 %second.1 = bf16[1280,2048]{1,0:T(8,128)(2,1)} custom-call(bf16[512,2176]{1,0:T(8,128)(2,1)} %all-gather.3.cloned.1.call-done.table_ref, s32[1,512]{1,0:T(1,128)} %and_select_fusion.apart_ref), custom_call_target="tpu_custom_call" | custom-call | flops 3200000000 | bytes 10000000 | tf_op jit(solution)/shard_map/second/pallas_call | solution.py:711
  124.5 6.3 %all-to-all-start = ((bf16[32,40,2048]{2,1,0:T(8,128)(2,1)}), bf16[32,40,2048]{2,1,0:T(8,128)(2,1)}, u32[]{:S(2)}, u32[]{:S(2)}) async-start(bf16[32,40,2048]{2,1,0:T(8,128)(2,1)} %bitcast.18), calls=%async_computation.1 | async-start | bytes 10485760 | tf_op jit(solution)/shard_map/all_to_all | solution.py:686
  130.8 6.1 %expert.3 = bf16[256,2048]{1,0:T(8,128)(2,1)} custom-call(bf16[256,2048]{1,0:T(8,128)(2,1)} %get-tuple-element.16.x_ref, bf16[1,2048,512]{2,1,0:T(8,128)(2,1)} %gate_ref.3, bf16[1,2048,512]{2,1,0:T(8,128)(2,1)} %up_ref.3, bf16[1,512,2048]{2,1,0:T(8,128)(2,1)} %down_ref.3), custom_call_target="tpu_custom_call" | custom-call | flops 1610612736 | bytes 8388608 | tf_op jit(solution)/shard_map/expert/pallas_call | solution.py:429
  137.0 1.6 slice.26.tags_ref
  138.5 0.0 all-gather.5.cloned.1.call-done
  138.5 11.9 %expert.2 = bf16[1024,2048]{1,0:T(8,128)(2,1)} custom-call(bf16[1024,2048]{1,0:T(8,128)(2,1)} %bitcast.26, bf16[1,2048,512]{2,1,0:T(8,128)(2,1)} %gate_ref.3, bf16[1,2048,512]{2,1,0:T(8,128)(2,1)} %up_ref.3, bf16[1,512,2048]{2,1,0:T(8,128)(2,1)} %down_ref.3), custom_call_target="tpu_custom_call" | custom-call | flops 6442450944 | bytes 14680064 | tf_op jit(solution)/shard_map/expert/pallas_call | solution.py:429
  150.5 43.5 %all-to-all-done.rows_hbm = bf16[32,40,2048]{2,1,0:T(8,128)(2,1)} async-done(((bf16[32,40,2048]{2,1,0:T(8,128)(2,1)}), bf16[32,40,2048]{2,1,0:T(8,128)(2,1)}, u32[]{:S(2)}, u32[]{:S(2)}) %all-to-all-start) | async-done | bytes 5242912 | tf_op jit(solution)/shard_map/all_to_all | solution.py:686
  194.0 121.0 %joint.1 = bf16[128,2048]{1,0:T(8,128)(2,1)} custom-call(bf16[32,40,2048]{2,1,0:T(8,128)(2,1)} %all-to-all-done.rows_hbm, bf16[4,32,8,2048]{3,2,1,0:T(8,128)(2,1)} %bitcast.33, bf16[32,8,2048]{2,1,0:T(8,128)(2,1)} %bitcast.23, bf16[512,128]{1,0:T(8,128)(2,1)} %slice.26.tags_ref, bf16[2048,512]{1,0:T(8,128)(2,1)} %bitcast.20, bf16[2048,512]{1,0:T(8,128)(2,1)} %bitcast.21, ...), custom_call_target="tpu_custom_call" | custom-call | flops 40000000000 | bytes 30000000 | tf_op jit(solution)/shard_map/joint/pallas_call | solution.py:653
  315.0 0.0 reduce-scatter.2.cloned.1.call-done
  315.0 1.9 copy.28
  (1 shorter events, 0.0 us)
Async XLA Ops:
  7.2 109.9 %all-gather.3.cloned.1.call-start = ((), (), s32[]{:S(2)}) async-start(), calls=%async_computation.4 | async-start | bytes 2785280 | tf_op jit(solution)/shard_map/all_gather | solution.py:705
  10.8 127.7 %all-gather.5.cloned.1.call-start = ((), (), s32[]{:S(2)}) async-start(), calls=%async_computation.5 | async-start | bytes 5242880 | tf_op jit(solution)/shard_map/all_gather | solution.py:707
  47.1 1.6 slice-start
  47.1 1.6 slice-start.1
  47.1 1.6 slice-start.2
  47.1 4.1 %copy-start = (bf16[4,1024]{1,0:T(4,128)(2,1)S(1)}, bf16[4,1024]{1,0:T(4,128)(2,1)}, u32[]{:S(2)}) copy-start(bf16[4,1024]{1,0:T(4,128)(2,1)} %param.26) | copy-start | bytes 24580
  47.1 4.1 %copy-start.1 = (bf16[4,256]{1,0:T(4,128)(2,1)S(1)}, bf16[4,256]{1,0:T(4,128)(2,1)}, u32[]{:S(2)}) copy-start(bf16[4,256]{1,0:T(4,128)(2,1)} %param.28) | copy-start | bytes 6148
  47.1 4.1 %copy-start.2 = (bf16[4,256]{1,0:T(4,128)(2,1)S(1)}, bf16[4,256]{1,0:T(4,128)(2,1)}, u32[]{:S(2)}) copy-start(bf16[4,256]{1,0:T(4,128)(2,1)} %param.27) | copy-start | bytes 6148
  47.1 4.7 %copy-start.3 = (f32[16]{0:T(128)S(1)}, f32[16]{0:T(128)}, u32[]{:S(2)}) copy-start(f32[16]{0:T(128)} %param.29) | copy-start | bytes 196
  47.2 5.4 %copy-start.4 = (f32[16]{0:T(128)S(1)}, f32[16]{0:T(128)}, u32[]{:S(2)}) copy-start(f32[16]{0:T(128)} %param.30) | copy-start | bytes 196
  47.2 6.0 %copy-start.5 = (f32[16]{0:T(128)S(1)}, f32[16]{0:T(128)}, u32[]{:S(2)}) copy-start(f32[16]{0:T(128)} %param.31) | copy-start | bytes 196
  48.6 266.4 %reduce-scatter.2.cloned.1.call-start = ((), (), s32[]{:S(2)}) async-start(), calls=%async_computation.3 | async-start | bytes 7864320 | tf_op jit(solution)/shard_map/reduce_scatter | solution.py:355
  48.7 5.2 %collective-permute-start = (bf16[8,1536]{1,0:T(8,128)(2,1)S(1)}, bf16[8,1536]{1,0:T(8,128)(2,1)S(1)}, u32[]{:S(2)}, u32[]{:S(2)}) collective-permute-start(bf16[8,1536]{1,0:T(8,128)(2,1)S(1)} %pad_maximum_fusion), channel_id=1, source_target_pairs={{0,4},{4,8},{8,12},{12,16},{16,20},{20,24},{24,28},{28,32},{32,36}... | collective-permute-start | bytes 73736 | tf_op jit(solution)/shard_map/ppermute | solution.py:197
  54.0 0.6 copy-start.6
  124.5 69.4 %all-to-all-start = ((bf16[32,40,2048]{2,1,0:T(8,128)(2,1)}), bf16[32,40,2048]{2,1,0:T(8,128)(2,1)}, u32[]{:S(2)}, u32[]{:S(2)}) async-start(bf16[32,40,2048]{2,1,0:T(8,128)(2,1)} %bitcast.18), calls=%async_computation.1 | async-start | bytes 10485760 | tf_op jit(solution)/shard_map/all_to_all | solution.py:686
Sparse Core Ops, SparseCore 0:
  10.9 33.9 all-gather.2
  48.8 46.1 all-gather.4
  116.6 63.5 reduce-scatter.1

commit v5 on v4

--- a/solution.py
+++ b/solution.py
@@ -92,9 +92,16 @@
             out[:, j : j + 128] = silu(acc).astype(bf16)
     buf[0:8, :] = buf[SPAN : SPAN + 8, :]
 
-    pre = dtp_ref[...].astype(f32) + off_ref[...]
+    diagonal = lax.broadcasted_iota(jnp.int32, (heads, heads), 0) == lax.broadcasted_iota(
+        jnp.int32, (heads, heads), 1
+    )
+
+    def column(ref):
+        return jnp.sum(jnp.where(diagonal, jnp.broadcast_to(ref[...], (heads, heads)), 0.0), axis=1, keepdims=True)
+
+    pre = dtp_ref[...].astype(f32) + column(off_ref)
     dt = jnp.maximum(pre, 0.0) + jnp.log1p(jnp.exp(-jnp.abs(pre)))
-    log_decay = (spike_ref[...] - jnp.exp(fade_ref[...]) * dt) * LOG2E
+    log_decay = (spike_ref[...] - jnp.exp(column(fade_ref)) * dt) * LOG2E
     upto = (
         lax.broadcasted_iota(jnp.int32, (SPAN, SPAN), 0)
         <= lax.broadcasted_iota(jnp.int32, (SPAN, SPAN), 1)
@@ -237,6 +244,7 @@
         jnp.int32, (SPAN, SPAN), 1
     )
     low = lanes_below((STATE, PAIR), HEAD)
+    skips = expand_heads(skip_ref[...], heads)
     rows = row_ref[0:heads, :]
     cum = jnp.concatenate(
         [row_ref[heads : 2 * heads, :], jnp.zeros((128 - heads, SPAN), f32)], axis=0
@@ -266,7 +274,7 @@
             res = mm(jnp.concatenate(lefts, axis=0), jnp.concatenate([xp, sp.astype(bf16)], axis=0))
             add = mm(jnp.concatenate(downs, axis=0), xp)
             state[:, cols] = sp * shrink[q] + jnp.where(low, add[:STATE], add[STATE:])
-            y = jnp.where(low, res[:SPAN], res[SPAN:]) + xp.astype(f32) * skip_ref[:, cols]
+            y = jnp.where(low, res[:SPAN], res[SPAN:]) + xp.astype(f32) * skips[q]
             y = y * silu(z_ref[:, cols].astype(f32))
             gated[:, cols] = y
             squares = squares + y * y
@@ -305,7 +313,7 @@
         grid=(steps,),
         in_specs=[
             block(inner), block(group), block(group), whole(8, every), whole(4, every),
-            across(heads), across(heads), whole(heads, 1), whole(heads, 1),
+            across(heads), across(heads), whole(1, heads), whole(1, heads),
         ],
         out_specs=[
             block(inner), block(group), block(group), across(2 * heads),
@@ -328,7 +336,7 @@
         name="states",
     )(
         features, insert, query, halo, taps, presoftplus.T, spike.T,
-        offset.reshape(heads, 1), fading.reshape(heads, 1),
+        offset.reshape(1, heads), fading.reshape(1, heads),
     )
     entering = entering_state(message)
     partial = pl.pallas_call(
@@ -336,7 +344,7 @@
         grid=(steps,),
         in_specs=[
             block(inner), block(group), block(group), block(inner), across(2 * heads),
-            whole(STATE, inner), whole(1, inner), whole(1, inner), whole(inner, width),
+            whole(STATE, inner), whole(1, heads), whole(1, inner), whole(inner, width),
         ],
         out_specs=block(width),
         out_shape=jax.ShapeDtypeStruct((rows, width), bf16),
@@ -350,7 +358,7 @@
         name="mixer",
     )(
         xs, bs, cs, gating, row, entering,
-        jnp.repeat(skip, HEAD).reshape(1, inner), gain.reshape(1, inner), projection,
+        skip.reshape(1, heads), gain.reshape(1, inner), projection,
     )
     return lax.psum_scatter(partial, "tp", scatter_dimension=0, tiled=True)
 
@@ -445,8 +453,8 @@
 
 def joint_kernel(
     rows_hbm, late_hbm, own_ref, tags_ref, gate_hbm, up_hbm, down_hbm, out_ref,
-    rows, gate, up, down, res, back, late_all, late_sum, late_back, own_back,
-    pick, pick_first, part, shares,
+    rows, gate, up, down, res, back, late_own, mid_own, mid, mid_sum, from_left, from_right,
+    late_sum, late_back, own_back, pick, pick_first, part, part_mid, part_sum, part_left, part_right,
     load_sem, weight_sem, late_load, send_sem, recv_sem, share_send, share_recv,
     late_send, late_recv, own_send, own_recv, part_send, part_recv,
 ):
@@ -500,19 +508,51 @@
             device_id=device(k), device_id_type=mesh_ids,
         )
 
-    def give_share(r):
+    half = ep // 2
+    parts = (pl.ds(0, half), pl.ds(half, half))
+    sides = (1, blocks - 1)
+    opposite = (tp + 2) % blocks
+
+    def along(side, src, dst, send, recv):
         return pltpu.make_async_remote_copy(
-            src_ref=late_hbm.at[(tp + r) % blocks], dst_ref=late_all.at[r],
-            send_sem=share_send.at[r], recv_sem=share_recv.at[r],
-            device_id={"tp": (tp + r) % blocks}, device_id_type=mesh_ids,
+            src_ref=src, dst_ref=dst, send_sem=send, recv_sem=recv,
+            device_id={"tp": (tp + sides[side]) % blocks}, device_id_type=mesh_ids,
         )
 
-    def give_part(t, r):
-        return pltpu.make_async_remote_copy(
-            src_ref=part.at[t, r], dst_ref=shares.at[t, r],
-            send_sem=part_send.at[t, r], recv_sem=part_recv.at[t, r],
-            device_id={"tp": (tp + r) % blocks}, device_id_type=mesh_ids,
-        )
+    def share(stage, side):
+        owner = (tp + sides[side]) % blocks
+        landing = (from_left, from_right)[side]
+        if stage == 0:
+            src, dst = late_hbm.at[opposite, parts[side]], mid.at[side]
+        elif stage == 1:
+            src, dst = late_hbm.at[owner, parts[1 - side]], landing.at[parts[1 - side]]
+        else:
+            src, dst = mid_sum.at[side], landing.at[parts[side]]
+        return along(side, src, dst, share_send.at[stage, side], share_recv.at[stage, side])
+
+    def own_loads():
+        return [pltpu.make_async_copy(late_hbm.at[tp], late_own, late_load.at[2])] + [
+            pltpu.make_async_copy(
+                late_hbm.at[(tp + sides[n]) % blocks, parts[n]], mid_own.at[n], late_load.at[n]
+            )
+            for n in range(2)
+        ]
+
+    tiles = part.shape[0]
+
+    def side_of(t):
+        return 0 if t < tiles // 2 else 1
+
+    def give_part(stage, t):
+        side = side_of(t) if stage != 1 else 1 - side_of(t)
+        landing = (part_left, part_right)[side]
+        if stage == 0:
+            src, dst = part.at[t, 2], part_mid.at[t]
+        elif stage == 1:
+            src, dst = part.at[t, sides[side]], landing.at[t]
+        else:
+            src, dst = part_sum.at[t], landing.at[t]
+        return along(side, src, dst, part_send.at[stage, t], part_recv.at[stage, t])
 
     for w in weights():
         w.start()
@@ -527,16 +567,17 @@
     def _(k):
         pl.semaphore_signal(barrier, inc=1, device_id=device(k), device_id_type=mesh_ids)
 
-    for r in range(1, blocks):
+    for r in sides:
         pl.semaphore_signal(
             barrier, inc=1, device_id={"tp": (tp + r) % blocks}, device_id_type=mesh_ids
         )
-    pl.semaphore_wait(barrier, ep - 1 + blocks - 1)
-
-    for r in range(1, blocks):
-        give_share(r).start()
-    own_share = pltpu.make_async_copy(late_hbm.at[tp], late_all.at[0], late_load)
-    own_share.start()
+    pl.semaphore_wait(barrier, ep - 1 + len(sides))
+
+    for stage in range(2):
+        for side in range(2):
+            share(stage, side).start()
+    for load_own in own_loads():
+        load_own.start()
 
     for w in weights():
         w.wait()
@@ -567,6 +608,17 @@
 
     back[me] = res[0]
     own_back[me] = own_ref[me]
+
+    for load_own in own_loads():
+        load_own.wait()
+    for side in range(2):
+        share(0, side).wait_recv()
+
+        @pl.loop(0, half)
+        def _(k):
+            mid_sum[side, k] = (mid_own[side, k].astype(f32) + mid[side, k].astype(f32)).astype(bf16)
+
+        share(2, side).start()
 
     count = experts * per
     chosen = expert_of(count, 0, per, experts)
@@ -587,16 +639,14 @@
         hit = slot == (at + n * LATE).astype(f32)
         pick_first[n] = jnp.where(hit, weight, 0.0).astype(bf16)
 
-    own_share.wait()
-    for r in range(1, blocks):
-        give_share(r).wait_recv()
+    for stage in (1, 2):
+        for side in range(2):
+            share(stage, side).wait_recv()
 
     @pl.loop(0, ep)
     def _(k):
-        total = late_all[0, k].astype(f32)
-        for r in range(1, blocks):
-            total = total + late_all[r, k].astype(f32)
-        late_sum[k] = total.astype(bf16)
+        total = from_left[k].astype(f32) + from_right[k].astype(f32)
+        late_sum[k] = (total + late_own[k].astype(f32)).astype(bf16)
 
     @pl.loop(1, ep)
     def _(k):
@@ -608,26 +658,32 @@
     def _(k):
         give_back(k).wait_recv()
 
-    for t in range(width // col_tile):
+    for t in range(tiles):
         cols = slice(t * col_tile, (t + 1) * col_tile)
         got = mm(pick[...], back[:, :, cols].reshape(count, col_tile)).astype(bf16)
         part[t] = got.reshape(blocks, tokens, col_tile)
-        for r in range(1, blocks):
-            give_part(t, r).start()
+        give_part(0, t).start()
+        give_part(1, t).start()
+
+    for t in range(tiles):
+        give_part(0, t).wait_recv()
+        own_part = part[t, sides[side_of(t)]].astype(f32)
+        part_sum[t] = (own_part + part_mid[t].astype(f32)).astype(bf16)
+        give_part(2, t).start()
 
     @pl.loop(1, ep)
     def _(k):
         give_own(k).wait_recv()
         give_late(k).wait_recv()
 
-    for t in range(width // col_tile):
+    for t in range(tiles):
         cols = slice(t * col_tile, (t + 1) * col_tile)
         total = part[t, 0].astype(f32)
         for n, ref in enumerate((late_back, own_back)):
             total = total + mm(pick_first[n], ref[:, :, cols].reshape(experts * LATE, col_tile))
-        for r in range(1, blocks):
-            give_part(t, r).wait_recv()
-            total = total + shares[t, r].astype(f32)
+        for stage in (1, 2):
+            give_part(stage, t).wait_recv()
+        total = total + part_left[t].astype(f32) + part_right[t].astype(f32)
         out_ref[:, cols] = total.astype(bf16)
 
     @pl.loop(1, ep)
@@ -636,10 +692,11 @@
         give_own(k).wait_send()
         give_late(k).wait_send()
 
-    for r in range(1, blocks):
-        give_share(r).wait_send()
-        for t in range(width // col_tile):
-            give_part(t, r).wait_send()
+    for stage in range(3):
+        for side in range(2):
+            share(stage, side).wait_send()
+        for t in range(tiles):
+            give_part(stage, t).wait_send()
 
 
 def joint(second_in, late_part, own_part, tags, gate, up, down, tokens):
@@ -662,17 +719,25 @@
             pltpu.VMEM((hidden, width), bf16),
             pltpu.VMEM((ep, per, width), bf16),
             pltpu.VMEM((ep, per, width), bf16),
-            pltpu.VMEM((blocks, ep, LATE, width), bf16),
+            pltpu.VMEM((ep, LATE, width), bf16),
+            pltpu.VMEM((2, ep // 2, LATE, width), bf16),
+            pltpu.VMEM((2, ep // 2, LATE, width), bf16),
+            pltpu.VMEM((2, ep // 2, LATE, width), bf16),
+            pltpu.VMEM((ep, LATE, width), bf16),
+            pltpu.VMEM((ep, LATE, width), bf16),
             pltpu.VMEM((ep, LATE, width), bf16),
             pltpu.VMEM((ep, LATE, width), bf16),
             pltpu.VMEM((ep, LATE, width), bf16),
             pltpu.VMEM((blocks * tokens, ep * per), bf16),
             pltpu.VMEM((FIRST // LATE, tokens, ep * LATE), bf16),
             pltpu.VMEM((tiles, blocks, tokens, 512), bf16),
-            pltpu.VMEM((tiles, blocks, tokens, 512), bf16),
-            dma((ep,)), dma((3,)), dma, dma((ep,)), dma((ep,)), dma((blocks,)), dma((blocks,)),
+            pltpu.VMEM((tiles, tokens, 512), bf16),
+            pltpu.VMEM((tiles, tokens, 512), bf16),
+            pltpu.VMEM((tiles, tokens, 512), bf16),
+            pltpu.VMEM((tiles, tokens, 512), bf16),
+            dma((ep,)), dma((3,)), dma((3,)), dma((ep,)), dma((ep,)), dma((3, 2)), dma((3, 2)),
             dma((ep,)), dma((ep,)), dma((ep,)), dma((ep,)),
-            dma((tiles, blocks)), dma((tiles, blocks)),
+            dma((3, tiles)), dma((3, tiles)),
         ],
         compiler_params=pltpu.CompilerParams(
             collective_id=1, has_side_effects=True, vmem_limit_bytes=60 * 1024 * 1024

time: 324 us -> 321 us (level)
  the two profiles are of different devices: /device:TPU:9 before, /device:TPU:0 now
where the time goes in v5:
time: 321 us; the launch traced here: 317 us
  Pallas kernels  206 us (64%)
  waiting for transfers between devices  46.3 us (14%)
  blocking collectives  36.9 us (11%)
  between operations  13.9 us (4%)
  starting transfers between devices  7.38 us (2%)
  local copies, waits for them, and re-layouts  5.52 us (2%)
    pallas_call x1, Pallas kernels, joint(): pl.pallas_call(joint_kernel, in_specs=[any_ref, any_ref, vmem, vmem, any_...  111 us
    all_to_all x1, waiting for transfers between devices, exchanged(): return lax.all_to_all(value, EP, split_axis=0, concat_axis=0, tiled=True)  46.1 us
    all_to_all x1, blocking collectives, exchanged(): return lax.all_to_all(value, EP, split_axis=0, concat_axis=0, tiled=True)  36.9 us
    pallas_call x1, Pallas kernels, mixer_half(): pl.pallas_call(mixer_kernel, grid=(steps,), in_specs=[block(inner), block...  25.6 us
    pallas_call x1, Pallas kernels, entering_state(): pl.pallas_call(entering_kernel, in_specs=[pl.BlockSpec(memory_space=pltpu...  24.1 us
    pallas_call x2, Pallas kernels, expert(): pl.pallas_call(expert_kernel, grid=(rows // ROW_TILE,), in_specs=[pl.Bloc...  18.1 us
    pallas_call x1, Pallas kernels, mixer_half(): pl.pallas_call(states_kernel, grid=(steps,), in_specs=[block(inner), bloc...  15.9 us
    pallas_call x1, Pallas kernels, experts_half(): pl.pallas_call(functools.partial(second_kernel, experts=experts), grid=(c...  7.44 us
  transfers between devices with their start and end apart: 5, of which 2 were waited for; matrix products, arithmetic and copies ran while one was open for 1% of the time, Pallas kernels for 64%

profile of v5, /device:TPU:0, one launch (start us, length us, event | category | flops | bytes accessed | tf_op | source)
XLA Modules:
  0.0 317.1 jit_solution(15250734193731412510)
XLA Ops:
  7.2 0.0 all-gather.3.cloned.1.call-start
  7.2 3.6 %route.1 = (bf16[128,2176]{1,0:T(8,128)(2,1)}, bf16[512,2048]{1,0:T(8,128)(2,1)}) custom-call(bf16[128,2048]{1,0:T(8,128)(2,1)} %x_ref.3, f32[1,2048]{1,0:T(1,128)} %bitcast.28, s32[4,128]{1,0:T(4,128)} %bitcast.30, f32[4,128]{1,0:T(4,128)} %bitcast.31), custom_call_target="tpu_custom_call" | custom-call | flops 1000000000 | bytes 3000000 | tf_op jit(solution)/shard_map/route/pallas_call | solution.py:759
  10.8 0.0 all-gather.3.cloned.1.call-update
  10.8 0.0 all-gather.5.cloned.1.call-start
  10.9 36.9 %all_to_all.10 = bf16[32,16,2048]{2,1,0:T(8,128)(2,1)S(1)} all-to-all(bf16[32,16,2048]{2,1,0:T(8,128)(2,1)} %bitcast.20), channel_id=1, replica_groups=mesh['ep_0'=4,'ep_1'=4,'ep_2'=2,'tp'=4] {'ep_0','ep_1','ep_2'}, dimensions={0} | all-to-all | bytes 4194304 | tf_op jit(solution)/shard_map/all_to_all | solution.py:751
  47.8 0.0 slice-start
  47.8 0.0 slice-start.1
  47.8 0.0 slice-start.2
  47.8 0.0 copy-start
  47.8 0.0 copy-start.1
  47.8 0.0 copy-start.2
  47.8 1.4 slice_bitcast_fusion
  49.3 0.0 all-gather.5.cloned.1.call-update
  49.3 0.0 reduce-scatter.2.cloned.1.call-start
  49.3 0.0 slice-done
  49.4 0.0 slice-done.1
  49.4 0.0 slice-done.2
  49.4 2.0 collective-permute-start
  51.4 0.0 copy-done
  51.4 0.0 copy-done.1
  51.4 0.0 copy-done.2
  51.4 0.6 pad_maximum_fusion.1.taps_ref
  52.0 0.2 collective-permute-done.halo_ref
  52.2 0.0 copy-start.3
  52.2 0.6 copy-done.3
  52.8 15.9 %states.1 = (bf16[1536,1024]{1,0:T(8,128)(2,1)}, bf16[1536,256]{1,0:T(8,128)(2,1)}, bf16[1536,256]{1,0:T(8,128)(2,1)}, f32[32,1536]{1,0:T(8,128)}, bf16[32,16,512]{2,1,0:T(8,128)(2,1)}) custom-call(bf16[1536,1024]{1,0:T(8,128)(2,1)} %x_ref.2, bf16[1536,256]{1,0:T(8,128)(2,1)} %b_ref.1, bf16[1536,256]{1,0:T(8,128)(2,1)} %c_ref.1, bf16[8,1536]{1,0:T(8,128)(2,1)} %copy-done.3, ...), custom_call_target="tpu_custom_call" | custom-call | flops 8000000000 | bytes 10000000 | tf_op jit(solution)/shard_map/states/pallas_call | solution.py:311
  68.8 24.1 %entering.1.enter_ref = f32[128,1024]{1,0:T(8,128)} custom-call(bf16[32,16,512]{2,1,0:T(8,128)(2,1)} %get-tuple-element.13.msg_ref), custom_call_target="tpu_custom_call" | custom-call | flops 10000000000 | bytes 3000000 | tf_op jit(solution)/shard_map/entering/pallas_call | solution.py:210
  92.8 25.6 %mixer.1 = bf16[1536,2048]{1,0:T(8,128)(2,1)} custom-call(bf16[1536,1024]{1,0:T(8,128)(2,1)} %get-tuple-element.9.xs_ref, bf16[1536,256]{1,0:T(8,128)(2,1)} %get-tuple-element.10.bs_ref, bf16[1536,256]{1,0:T(8,128)(2,1)} %get-tuple-element.11.cs_ref, bf16[1536,1024]{1,0:T(8,128)(2,1)} %z_ref.1, f32[32,1536]{1,0:T(8,128)} %get-tuple-element.12.row_ref, ...), custom_call_target="tpu_custom_call" | custom-call | flops 20000000000 | bytes 20000000 | tf_op jit(solution)/shard_map/mixer/pallas_call | solution.py:342
  118.4 0.0 reduce-scatter.2.cloned.1.call-update
  118.5 0.6 and_select_fusion.apart_ref
  119.0 0.0 all-gather.3.cloned.1.call-done.table_ref
  119.0 7.4 %second.1 = bf16[1280,2048]{1,0:T(8,128)(2,1)} custom-call(bf16[512,2176]{1,0:T(8,128)(2,1)} %all-gather.3.cloned.1.call-done.table_ref, s32[1,512]{1,0:T(1,128)} %and_select_fusion.apart_ref), custom_call_target="tpu_custom_call" | custom-call | flops 3200000000 | bytes 10000000 | tf_op jit(solution)/shard_map/second/pallas_call | solution.py:776
  126.5 5.2 %all-to-all-start = ((bf16[32,40,2048]{2,1,0:T(8,128)(2,1)}), bf16[32,40,2048]{2,1,0:T(8,128)(2,1)}, u32[]{:S(2)}, u32[]{:S(2)}) async-start(bf16[32,40,2048]{2,1,0:T(8,128)(2,1)} %bitcast.19), calls=%async_computation.1 | async-start | bytes 10485760 | tf_op jit(solution)/shard_map/all_to_all | solution.py:751
  131.7 6.1 %expert.3 = bf16[256,2048]{1,0:T(8,128)(2,1)} custom-call(bf16[256,2048]{1,0:T(8,128)(2,1)} %get-tuple-element.16.x_ref, bf16[1,2048,512]{2,1,0:T(8,128)(2,1)} %gate_ref.3, bf16[1,2048,512]{2,1,0:T(8,128)(2,1)} %up_ref.3, bf16[1,512,2048]{2,1,0:T(8,128)(2,1)} %down_ref.3), custom_call_target="tpu_custom_call" | custom-call | flops 1610612736 | bytes 8388608 | tf_op jit(solution)/shard_map/expert/pallas_call | solution.py:437
  137.9 1.6 slice.26.tags_ref
  139.4 0.0 all-gather.5.cloned.1.call-done
  139.4 11.9 %expert.2 = bf16[1024,2048]{1,0:T(8,128)(2,1)} custom-call(bf16[1024,2048]{1,0:T(8,128)(2,1)} %bitcast.25, bf16[1,2048,512]{2,1,0:T(8,128)(2,1)} %gate_ref.3, bf16[1,2048,512]{2,1,0:T(8,128)(2,1)} %up_ref.3, bf16[1,512,2048]{2,1,0:T(8,128)(2,1)} %down_ref.3), custom_call_target="tpu_custom_call" | custom-call | flops 6442450944 | bytes 14680064 | tf_op jit(solution)/shard_map/expert/pallas_call | solution.py:437
  151.4 46.1 %all-to-all-done.rows_hbm = bf16[32,40,2048]{2,1,0:T(8,128)(2,1)} async-done(((bf16[32,40,2048]{2,1,0:T(8,128)(2,1)}), bf16[32,40,2048]{2,1,0:T(8,128)(2,1)}, u32[]{:S(2)}, u32[]{:S(2)}) %all-to-all-start) | async-done | bytes 5242912 | tf_op jit(solution)/shard_map/all_to_all | solution.py:751
  197.4 111.2 %joint.1 = bf16[128,2048]{1,0:T(8,128)(2,1)} custom-call(bf16[32,40,2048]{2,1,0:T(8,128)(2,1)} %all-to-all-done.rows_hbm, bf16[4,32,8,2048]{3,2,1,0:T(8,128)(2,1)} %bitcast.35, bf16[32,8,2048]{2,1,0:T(8,128)(2,1)} %bitcast.24, bf16[512,128]{1,0:T(8,128)(2,1)} %slice.26.tags_ref, bf16[2048,512]{1,0:T(8,128)(2,1)} %bitcast.21, bf16[2048,512]{1,0:T(8,128)(2,1)} %bitcast.22, ...), custom_call_target="tpu_custom_call" | custom-call | flops 40000000000 | bytes 30000000 | tf_op jit(solution)/shard_map/joint/pallas_call | solution.py:710
  308.7 0.0 reduce-scatter.2.cloned.1.call-done
  308.7 1.9 copy.24
  (1 shorter events, 0.0 us)
Async XLA Ops:
  7.2 111.9 %all-gather.3.cloned.1.call-start = ((), (), s32[]{:S(2)}) async-start(), calls=%async_computation.4 | async-start | bytes 2785280 | tf_op jit(solution)/shard_map/all_gather | solution.py:770
  10.8 128.6 %all-gather.5.cloned.1.call-start = ((), (), s32[]{:S(2)}) async-start(), calls=%async_computation.5 | async-start | bytes 5242880 | tf_op jit(solution)/shard_map/all_gather | solution.py:772
  47.8 1.6 slice-start
  47.8 1.6 slice-start.1
  47.8 1.6 slice-start.2
  47.8 3.6 %copy-start = (bf16[4,1024]{1,0:T(4,128)(2,1)S(1)}, bf16[4,1024]{1,0:T(4,128)(2,1)}, u32[]{:S(2)}) copy-start(bf16[4,1024]{1,0:T(4,128)(2,1)} %param.26) | copy-start | bytes 24580
  47.8 3.6 %copy-start.1 = (bf16[4,256]{1,0:T(4,128)(2,1)S(1)}, bf16[4,256]{1,0:T(4,128)(2,1)}, u32[]{:S(2)}) copy-start(bf16[4,256]{1,0:T(4,128)(2,1)} %param.28) | copy-start | bytes 6148
  47.8 3.6 %copy-start.2 = (bf16[4,256]{1,0:T(4,128)(2,1)S(1)}, bf16[4,256]{1,0:T(4,128)(2,1)}, u32[]{:S(2)}) copy-start(bf16[4,256]{1,0:T(4,128)(2,1)} %param.27) | copy-start | bytes 6148
  49.3 259.4 %reduce-scatter.2.cloned.1.call-start = ((), (), s32[]{:S(2)}) async-start(), calls=%async_computation.3 | async-start | bytes 7864320 | tf_op jit(solution)/shard_map/reduce_scatter | solution.py:363
  49.4 2.9 collective-permute-start
  52.2 0.6 copy-start.3
  126.5 70.9 %all-to-all-start = ((bf16[32,40,2048]{2,1,0:T(8,128)(2,1)}), bf16[32,40,2048]{2,1,0:T(8,128)(2,1)}, u32[]{:S(2)}, u32[]{:S(2)}) async-start(bf16[32,40,2048]{2,1,0:T(8,128)(2,1)} %bitcast.19), calls=%async_computation.1 | async-start | bytes 10485760 | tf_op jit(solution)/shard_map/all_to_all | solution.py:751
Sparse Core Ops, SparseCore 0:
  11.0 34.3 all-gather.2
  49.4 45.8 all-gather.4
  118.6 62.9 reduce-scatter.1

commit v6 on v5

--- a/solution.py
+++ b/solution.py
@@ -454,7 +454,7 @@
 def joint_kernel(
     rows_hbm, late_hbm, own_ref, tags_ref, gate_hbm, up_hbm, down_hbm, out_ref,
     rows, gate, up, down, res, back, late_own, mid_own, mid, mid_sum, from_left, from_right,
-    late_sum, late_back, own_back, pick, pick_first, part, part_mid, part_sum, part_left, part_right,
+    late_sum, late_back, own_back, pick, pick_first, mix, part, part_mid, part_sum, part_left, part_right,
     load_sem, weight_sem, late_load, send_sem, recv_sem, share_send, share_recv,
     late_send, late_recv, own_send, own_recv, part_send, part_recv,
 ):
@@ -490,7 +490,7 @@
 
     def give_back(k):
         return pltpu.make_async_remote_copy(
-            src_ref=res.at[k], dst_ref=back.at[me], send_sem=send_sem.at[k], recv_sem=recv_sem.at[k],
+            src_ref=res.at[k], dst_ref=back.at[k], send_sem=send_sem.at[k], recv_sem=recv_sem.at[k],
             device_id=device(k), device_id_type=mesh_ids,
         )
 
@@ -554,10 +554,16 @@
             src, dst = part_sum.at[t], landing.at[t]
         return along(side, src, dst, part_send.at[stage, t], part_recv.at[stage, t])
 
+    group = 8
+
+    @pl.loop(0, group)
+    def _(k):
+        load(k).start()
+
     for w in weights():
         w.start()
 
-    @pl.loop(0, ep)
+    @pl.loop(group, ep)
     def _(k):
         load(k).start()
 
@@ -582,8 +588,6 @@
     for w in weights():
         w.wait()
 
-    group = 8
-
     @pl.loop(0, ep // group)
     def _(c):
         @pl.loop(0, group)
@@ -606,7 +610,7 @@
     def _(k):
         give_own(k).start()
 
-    back[me] = res[0]
+    back[0] = res[0]
     own_back[me] = own_ref[me]
 
     for load_own in own_loads():
@@ -620,16 +624,20 @@
 
         share(2, side).start()
 
-    count = experts * per
-    chosen = expert_of(count, 0, per, experts)
+    count = group * per
     block, wanted = second_slot(lax.broadcasted_iota(jnp.int32, (1, count), 1) % per)
-    for r in range(blocks):
-        q = (tp + r) % blocks
-        table = tags_ref[pl.ds(pl.multiple_of(q * tokens, tokens), tokens), :]
-        slot = mm_last(table[:, 0:experts], chosen)
-        weight = mm_last(table[:, experts : 2 * experts], chosen)
-        hit = (slot == wanted.astype(f32)) & (block == r)
-        pick[r * tokens : (r + 1) * tokens, :] = jnp.where(hit, weight, 0.0).astype(bf16)
+    for c in range(ep // group):
+        sent = lax.broadcasted_iota(jnp.int32, (count, experts), 0) // per + c * group
+        holder = (z + 64 - sent // 2) % 4 * 4 + (y + 64 - sent // 8 - sent // 2) % 4
+        holder = holder * 2 + (core + 64 - sent) % 2
+        chosen = (holder == lax.broadcasted_iota(jnp.int32, (count, experts), 1)).astype(bf16)
+        for r in range(blocks):
+            q = (tp + r) % blocks
+            table = tags_ref[pl.ds(pl.multiple_of(q * tokens, tokens), tokens), :]
+            slot = mm_last(table[:, 0:experts], chosen)
+            weight = mm_last(table[:, experts : 2 * experts], chosen)
+            hit = (slot == wanted.astype(f32)) & (block == r)
+            pick[c, r * tokens : (r + 1) * tokens, :] = jnp.where(hit, weight, 0.0).astype(bf16)
     own = tags_ref[pl.ds(pl.multiple_of(tp * tokens, tokens), tokens), :]
     chosen = expert_of(experts * LATE, 0, LATE, experts)
     slot = mm_last(own[:, 0:experts], chosen)
@@ -639,6 +647,24 @@
         hit = slot == (at + n * LATE).astype(f32)
         pick_first[n] = jnp.where(hit, weight, 0.0).astype(bf16)
 
+    def mixed_in(c, t):
+        cols = slice(t * col_tile, (t + 1) * col_tile)
+        got = back[c * group : (c + 1) * group, :, cols].reshape(count, col_tile)
+        return mm(pick[c], got) if c == 0 else mix[:, cols] + mm(pick[c], got)
+
+    def arrived(c):
+        @pl.loop(max(c * group, 1), (c + 1) * group)
+        def _(k):
+            give_back(k).wait_recv()
+
+    def mix_in(c):
+        arrived(c)
+        for t in range(tiles):
+            mix[:, t * col_tile : (t + 1) * col_tile] = mixed_in(c, t)
+
+    mix_in(0)
+    mix_in(1)
+
     for stage in (1, 2):
         for side in range(2):
             share(stage, side).wait_recv()
@@ -654,13 +680,11 @@
 
     late_back[me] = late_sum[me]
 
-    @pl.loop(1, ep)
-    def _(k):
-        give_back(k).wait_recv()
+    mix_in(2)
+    arrived(3)
 
     for t in range(tiles):
-        cols = slice(t * col_tile, (t + 1) * col_tile)
-        got = mm(pick[...], back[:, :, cols].reshape(count, col_tile)).astype(bf16)
+        got = mixed_in(3, t).astype(bf16)
         part[t] = got.reshape(blocks, tokens, col_tile)
         give_part(0, t).start()
         give_part(1, t).start()
@@ -728,8 +752,9 @@
             pltpu.VMEM((ep, LATE, width), bf16),
             pltpu.VMEM((ep, LATE, width), bf16),
             pltpu.VMEM((ep, LATE, width), bf16),
-            pltpu.VMEM((blocks * tokens, ep * per), bf16),
+            pltpu.VMEM((ep // 8, blocks * tokens, 8 * per), bf16),
             pltpu.VMEM((FIRST // LATE, tokens, ep * LATE), bf16),
+            pltpu.VMEM((blocks * tokens, width), f32),
             pltpu.VMEM((tiles, blocks, tokens, 512), bf16),
             pltpu.VMEM((tiles, tokens, 512), bf16),
             pltpu.VMEM((tiles, tokens, 512), bf16),

time: 321 us -> 322 us (level)
  no operation moved by 1% of the time
where the time goes in v6:
time: 322 us; the launch traced here: 317 us
  Pallas kernels  206 us (64%)
  waiting for transfers between devices  46.3 us (14%)
  blocking collectives  36.9 us (11%)
  between operations  13.9 us (4%)
  starting transfers between devices  7.38 us (2%)
  local copies, waits for them, and re-layouts  5.52 us (2%)
    pallas_call x1, Pallas kernels, joint(): pl.pallas_call(joint_kernel, in_specs=[any_ref, any_ref, vmem, vmem, any_...  111 us
    all_to_all x1, waiting for transfers between devices, exchanged(): return lax.all_to_all(value, EP, split_axis=0, concat_axis=0, tiled=True)  46.1 us
    all_to_all x1, blocking collectives, exchanged(): return lax.all_to_all(value, EP, split_axis=0, concat_axis=0, tiled=True)  36.9 us
    pallas_call x1, Pallas kernels, mixer_half(): pl.pallas_call(mixer_kernel, grid=(steps,), in_specs=[block(inner), block...  25.6 us
    pallas_call x1, Pallas kernels, entering_state(): pl.pallas_call(entering_kernel, in_specs=[pl.BlockSpec(memory_space=pltpu...  24.1 us
    pallas_call x2, Pallas kernels, expert(): pl.pallas_call(expert_kernel, grid=(rows // ROW_TILE,), in_specs=[pl.Bloc...  18.1 us
    pallas_call x1, Pallas kernels, mixer_half(): pl.pallas_call(states_kernel, grid=(steps,), in_specs=[block(inner), bloc...  15.9 us
    pallas_call x1, Pallas kernels, experts_half(): pl.pallas_call(functools.partial(second_kernel, experts=experts), grid=(c...  7.44 us
  transfers between devices with their start and end apart: 5, of which 2 were waited for; matrix products, arithmetic and copies ran while one was open for 1% of the time, Pallas kernels for 64%

profile of v6, /device:TPU:0, one launch (start us, length us, event | category | flops | bytes accessed | tf_op | source)
XLA Modules:
  0.0 317.1 jit_solution(2840687886047770230)
XLA Ops:
  7.2 0.0 all-gather.3.cloned.1.call-start
  7.2 3.6 %route.1 = (bf16[128,2176]{1,0:T(8,128)(2,1)}, bf16[512,2048]{1,0:T(8,128)(2,1)}) custom-call(bf16[128,2048]{1,0:T(8,128)(2,1)} %x_ref.3, f32[1,2048]{1,0:T(1,128)} %bitcast.28, s32[4,128]{1,0:T(4,128)} %bitcast.30, f32[4,128]{1,0:T(4,128)} %bitcast.31), custom_call_target="tpu_custom_call" | custom-call | flops 1000000000 | bytes 3000000 | tf_op jit(solution)/shard_map/route/pallas_call | solution.py:784
  10.8 0.0 all-gather.3.cloned.1.call-update
  10.8 0.0 all-gather.5.cloned.1.call-start
  10.9 36.9 %all_to_all.10 = bf16[32,16,2048]{2,1,0:T(8,128)(2,1)S(1)} all-to-all(bf16[32,16,2048]{2,1,0:T(8,128)(2,1)} %bitcast.20), channel_id=1, replica_groups=mesh['ep_0'=4,'ep_1'=4,'ep_2'=2,'tp'=4] {'ep_0','ep_1','ep_2'}, dimensions={0} | all-to-all | bytes 4194304 | tf_op jit(solution)/shard_map/all_to_all | solution.py:776
  47.8 0.0 slice-start
  47.8 0.0 slice-start.1
  47.8 0.0 slice-start.2
  47.8 0.0 copy-start
  47.8 0.0 copy-start.1
  47.8 0.0 copy-start.2
  47.8 1.4 slice_bitcast_fusion
  49.3 0.0 all-gather.5.cloned.1.call-update
  49.3 0.0 reduce-scatter.2.cloned.1.call-start
  49.3 0.0 slice-done
  49.4 0.0 slice-done.1
  49.4 0.0 slice-done.2
  49.4 2.0 collective-permute-start
  51.4 0.0 copy-done
  51.4 0.0 copy-done.1
  51.4 0.0 copy-done.2
  51.4 0.6 pad_maximum_fusion.1.taps_ref
  52.0 0.2 collective-permute-done.halo_ref
  52.2 0.0 copy-start.3
  52.2 0.6 copy-done.3
  52.8 15.9 %states.1 = (bf16[1536,1024]{1,0:T(8,128)(2,1)}, bf16[1536,256]{1,0:T(8,128)(2,1)}, bf16[1536,256]{1,0:T(8,128)(2,1)}, f32[32,1536]{1,0:T(8,128)}, bf16[32,16,512]{2,1,0:T(8,128)(2,1)}) custom-call(bf16[1536,1024]{1,0:T(8,128)(2,1)} %x_ref.2, bf16[1536,256]{1,0:T(8,128)(2,1)} %b_ref.1, bf16[1536,256]{1,0:T(8,128)(2,1)} %c_ref.1, bf16[8,1536]{1,0:T(8,128)(2,1)} %copy-done.3, ...), custom_call_target="tpu_custom_call" | custom-call | flops 8000000000 | bytes 10000000 | tf_op jit(solution)/shard_map/states/pallas_call | solution.py:311
  68.8 24.1 %entering.1.enter_ref = f32[128,1024]{1,0:T(8,128)} custom-call(bf16[32,16,512]{2,1,0:T(8,128)(2,1)} %get-tuple-element.13.msg_ref), custom_call_target="tpu_custom_call" | custom-call | flops 10000000000 | bytes 3000000 | tf_op jit(solution)/shard_map/entering/pallas_call | solution.py:210
  92.8 25.6 %mixer.1 = bf16[1536,2048]{1,0:T(8,128)(2,1)} custom-call(bf16[1536,1024]{1,0:T(8,128)(2,1)} %get-tuple-element.9.xs_ref, bf16[1536,256]{1,0:T(8,128)(2,1)} %get-tuple-element.10.bs_ref, bf16[1536,256]{1,0:T(8,128)(2,1)} %get-tuple-element.11.cs_ref, bf16[1536,1024]{1,0:T(8,128)(2,1)} %z_ref.1, f32[32,1536]{1,0:T(8,128)} %get-tuple-element.12.row_ref, ...), custom_call_target="tpu_custom_call" | custom-call | flops 20000000000 | bytes 20000000 | tf_op jit(solution)/shard_map/mixer/pallas_call | solution.py:342
  118.4 0.0 reduce-scatter.2.cloned.1.call-update
  118.5 0.6 and_select_fusion.apart_ref
  119.0 0.0 all-gather.3.cloned.1.call-done.table_ref
  119.0 7.4 %second.1 = bf16[1280,2048]{1,0:T(8,128)(2,1)} custom-call(bf16[512,2176]{1,0:T(8,128)(2,1)} %all-gather.3.cloned.1.call-done.table_ref, s32[1,512]{1,0:T(1,128)} %and_select_fusion.apart_ref), custom_call_target="tpu_custom_call" | custom-call | flops 3200000000 | bytes 10000000 | tf_op jit(solution)/shard_map/second/pallas_call | solution.py:801
  126.5 5.2 %all-to-all-start = ((bf16[32,40,2048]{2,1,0:T(8,128)(2,1)}), bf16[32,40,2048]{2,1,0:T(8,128)(2,1)}, u32[]{:S(2)}, u32[]{:S(2)}) async-start(bf16[32,40,2048]{2,1,0:T(8,128)(2,1)} %bitcast.19), calls=%async_computation.1 | async-start | bytes 10485760 | tf_op jit(solution)/shard_map/all_to_all | solution.py:776
  131.7 6.1 %expert.3 = bf16[256,2048]{1,0:T(8,128)(2,1)} custom-call(bf16[256,2048]{1,0:T(8,128)(2,1)} %get-tuple-element.16.x_ref, bf16[1,2048,512]{2,1,0:T(8,128)(2,1)} %gate_ref.3, bf16[1,2048,512]{2,1,0:T(8,128)(2,1)} %up_ref.3, bf16[1,512,2048]{2,1,0:T(8,128)(2,1)} %down_ref.3), custom_call_target="tpu_custom_call" | custom-call | flops 1610612736 | bytes 8388608 | tf_op jit(solution)/shard_map/expert/pallas_call | solution.py:437
  137.9 1.6 slice.26.tags_ref
  139.4 0.0 all-gather.5.cloned.1.call-done
  139.4 11.9 %expert.2 = bf16[1024,2048]{1,0:T(8,128)(2,1)} custom-call(bf16[1024,2048]{1,0:T(8,128)(2,1)} %bitcast.25, bf16[1,2048,512]{2,1,0:T(8,128)(2,1)} %gate_ref.3, bf16[1,2048,512]{2,1,0:T(8,128)(2,1)} %up_ref.3, bf16[1,512,2048]{2,1,0:T(8,128)(2,1)} %down_ref.3), custom_call_target="tpu_custom_call" | custom-call | flops 6442450944 | bytes 14680064 | tf_op jit(solution)/shard_map/expert/pallas_call | solution.py:437
  151.4 46.1 %all-to-all-done.rows_hbm = bf16[32,40,2048]{2,1,0:T(8,128)(2,1)} async-done(((bf16[32,40,2048]{2,1,0:T(8,128)(2,1)}), bf16[32,40,2048]{2,1,0:T(8,128)(2,1)}, u32[]{:S(2)}, u32[]{:S(2)}) %all-to-all-start) | async-done | bytes 5242912 | tf_op jit(solution)/shard_map/all_to_all | solution.py:776
  197.4 111.2 %joint.1 = bf16[128,2048]{1,0:T(8,128)(2,1)} custom-call(bf16[32,40,2048]{2,1,0:T(8,128)(2,1)} %all-to-all-done.rows_hbm, bf16[4,32,8,2048]{3,2,1,0:T(8,128)(2,1)} %bitcast.35, bf16[32,8,2048]{2,1,0:T(8,128)(2,1)} %bitcast.24, bf16[512,128]{1,0:T(8,128)(2,1)} %slice.26.tags_ref, bf16[2048,512]{1,0:T(8,128)(2,1)} %bitcast.21, bf16[2048,512]{1,0:T(8,128)(2,1)} %bitcast.22, ...), custom_call_target="tpu_custom_call" | custom-call | flops 40000000000 | bytes 30000000 | tf_op jit(solution)/shard_map/joint/pallas_call | solution.py:734
  308.7 0.0 reduce-scatter.2.cloned.1.call-done
  308.7 1.9 copy.24
  (1 shorter events, 0.0 us)
Async XLA Ops:
  7.2 111.9 %all-gather.3.cloned.1.call-start = ((), (), s32[]{:S(2)}) async-start(), calls=%async_computation.4 | async-start | bytes 2785280 | tf_op jit(solution)/shard_map/all_gather | solution.py:795
  10.8 128.6 %all-gather.5.cloned.1.call-start = ((), (), s32[]{:S(2)}) async-start(), calls=%async_computation.5 | async-start | bytes 5242880 | tf_op jit(solution)/shard_map/all_gather | solution.py:797
  47.8 1.6 slice-start
  47.8 1.6 slice-start.1
  47.8 1.6 slice-start.2
  47.8 3.6 %copy-start = (bf16[4,1024]{1,0:T(4,128)(2,1)S(1)}, bf16[4,1024]{1,0:T(4,128)(2,1)}, u32[]{:S(2)}) copy-start(bf16[4,1024]{1,0:T(4,128)(2,1)} %param.26) | copy-start | bytes 24580
  47.8 3.6 %copy-start.1 = (bf16[4,256]{1,0:T(4,128)(2,1)S(1)}, bf16[4,256]{1,0:T(4,128)(2,1)}, u32[]{:S(2)}) copy-start(bf16[4,256]{1,0:T(4,128)(2,1)} %param.28) | copy-start | bytes 6148
  47.8 3.6 %copy-start.2 = (bf16[4,256]{1,0:T(4,128)(2,1)S(1)}, bf16[4,256]{1,0:T(4,128)(2,1)}, u32[]{:S(2)}) copy-start(bf16[4,256]{1,0:T(4,128)(2,1)} %param.27) | copy-start | bytes 6148
  49.3 259.4 %reduce-scatter.2.cloned.1.call-start = ((), (), s32[]{:S(2)}) async-start(), calls=%async_computation.3 | async-start | bytes 7864320 | tf_op jit(solution)/shard_map/reduce_scatter | solution.py:363
  49.4 2.9 collective-permute-start
  52.2 0.6 copy-start.3
  126.5 70.9 %all-to-all-start = ((bf16[32,40,2048]{2,1,0:T(8,128)(2,1)}), bf16[32,40,2048]{2,1,0:T(8,128)(2,1)}, u32[]{:S(2)}, u32[]{:S(2)}) async-start(bf16[32,40,2048]{2,1,0:T(8,128)(2,1)} %bitcast.19), calls=%async_computation.1 | async-start | bytes 10485760 | tf_op jit(solution)/shard_map/all_to_all | solution.py:776
Sparse Core Ops, SparseCore 0:
  11.0 34.3 all-gather.2
  49.4 45.8 all-gather.4
  118.6 62.9 reduce-scatter.1
